TPU v7x, 32 devices: a whole 2x2x4 slice. The times are simulated.
32 devices in a mesh: grp: 2 (over y), sp: 4 (over z), fs: 2 (over x), tp: 2 (over core).
Axes of the slice: x: 2, y: 2, z: 4, core: 2. Of those that a mesh axis runs over, the one named last changes fastest.
Arguments:
- tokens: bfloat16 [8, 256, 2048], P(('grp', 'fs'), 'sp'), parts along dimension 0, may hold values from -6 to 6
- pre_gain: float32 [2048], replicated, may hold values from 0.1 to 1.9
- query_weight: bfloat16 [2048, 1024], P(('sp', 'fs'), 'tp'), may hold values from -0.125 to 0.125
- key_weight: bfloat16 [2048, 1024], P(('sp', 'fs'), 'tp'), may hold values from -0.125 to 0.125
- value_weight: bfloat16 [2048, 1024], P(('sp', 'fs'), 'tp'), may hold values from -0.125 to 0.125
- beta_weight: bfloat16 [2048, 8], replicated, may hold values from -0.125 to 0.125
- decay_weight: bfloat16 [2048, 8], replicated, may hold values from -0.125 to 0.125
- decay_rate: float32 [8], replicated, may hold values from 0 to 1
- delta_gain: float32 [128], replicated, may hold values from 0.1 to 1.9
- query_down: bfloat16 [2048, 512], P(('sp', 'fs')), may hold values from -0.125 to 0.125
- latent_down: bfloat16 [2048, 256], P(('sp', 'fs')), may hold values from -0.125 to 0.125
- rope_weight: bfloat16 [2048, 32], replicated, may hold values from -0.125 to 0.125
- query_gain: float32 [512], replicated, may hold values from 0.1 to 1.9
- latent_gain: float32 [256], replicated, may hold values from 0.1 to 1.9
- query_up: bfloat16 [512, 1536], P(None, 'tp'), may hold values from -4 to 4
- latent_up: bfloat16 [256, 2048], P(None, 'tp'), may hold values from -4 to 4
- delta_out: bfloat16 [1024, 2048], P('tp', ('sp', 'fs')), may hold values from -8 to 8
- latent_out: bfloat16 [1024, 2048], P('tp', ('sp', 'fs')), may hold values from -8 to 8
- post_gain: float32 [2048], P('tp'), may hold values from 0.1 to 1.9
Outputs:
- mixed_out: bfloat16 [8, 256, 2048], P(('grp', 'fs'), 'sp', 'tp'), parts along dimension 0
There are 2 independent parts, one for each index of `grp`. A program takes and returns all parts, laid end to end along the dimension named above; an argument that names none is the same for every part. Nothing has to cross between parts.
All inputs are finite; a program needn't handle non-finite values.
Results may differ from a plain program's by a relative error of at most 0.018.
The roundings to bfloat16 on the way count: a program that leaves them out, or rounds other values in their place, can miss the bound.
Values may be sent and summed in bfloat16 or wider, within the bound.
No kernel may reach another device: no remote copies, remote signals or barrier semaphores. Data moves between devices by JAX's collectives and lax.ppermute only.
A program may use at most 128 MiB of HBM per device.

v0:
```python
import math

import jax
import jax.numpy as jnp
from jax import lax
from jax.sharding import PartitionSpec as P

D = 2048
HEAD = 128
NOPE = 64
ROPE = 32
VDIM = 64
BLOCK = 64


NORM_EPS = 1e-06
ROPE_THETA = 10000.0
HIGHEST = lax.Precision.HIGHEST


def prefix(array, axis, join, neutral):
    place = lax.axis_index(axis)
    gathered = jax.tree.map(
        lambda a, kind: lax.all_gather(a.astype(kind), axis), array, (jnp.bfloat16, jnp.bfloat16)
    )
    state = jax.tree.map(lambda a, e: jnp.zeros_like(a) + jnp.asarray(e, a.dtype), array, neutral)

    def one(step, state):
        return join(
            state,
            jax.tree.map(
                lambda a, own: lax.dynamic_index_in_dim(a, step, 0, False).astype(own.dtype),
                gathered,
                array,
            ),
        )

    return lax.fori_loop(0, place, one, state)


def stored(values):
    return lax.optimization_barrier(values.astype(jnp.bfloat16))


def rms_scale(values):
    return lax.rsqrt(jnp.mean(values * values, axis=-1, keepdims=True) + NORM_EPS)


def unit_rows(values):
    return values * lax.rsqrt(jnp.sum(values * values, axis=-1, keepdims=True) + NORM_EPS)


def rope_tables(positions, rope_width):
    frequency = ROPE_THETA ** (-jnp.arange(0, rope_width, 2, dtype=jnp.float32) / rope_width)
    angles = positions.astype(jnp.float32)[:, None] * frequency[None, :]
    return (jnp.cos(angles), jnp.sin(angles))


def rotate(values, cosine_table, sine_table):
    lower_half, upper_half = jnp.split(values, 2, axis=-1)
    return jnp.concatenate(
        [
            lower_half * cosine_table - upper_half * sine_table,
            upper_half * cosine_table + lower_half * sine_table,
        ],
        axis=-1,
    )


def delta_terms(query_vectors, key_vectors, value_vectors, beta_gate, log_decay):
    length, head_count, head_width = query_vectors.shape
    nblocks = length // BLOCK

    def split_blocks(tensor):
        return jnp.moveaxis(tensor.reshape((nblocks, BLOCK, head_count) + tensor.shape[2:]), 2, 0)

    query_vectors = split_blocks(query_vectors)
    key_vectors = split_blocks(key_vectors)
    value_vectors = split_blocks(value_vectors)
    beta_gate = split_blocks(beta_gate)
    gate_sum = jnp.cumsum(split_blocks(log_decay), axis=-1)
    position = jnp.arange(BLOCK)
    strict = position[:, None] > position[None, :]
    causal = position[:, None] >= position[None, :]
    gate_gap = gate_sum[..., :, None] - gate_sum[..., None, :]
    strict_decay = jnp.where(strict, jnp.exp(jnp.where(strict, gate_gap, 0.0)), 0.0)
    causal_decay = jnp.where(causal, jnp.exp(jnp.where(causal, gate_gap, 0.0)), 0.0)
    keys_scaled = key_vectors * beta_gate[..., None]
    lower_mat = (
        jnp.einsum("hnid,hnjd->hnij", keys_scaled, key_vectors, precision=HIGHEST) * strict_decay
    )
    identity = jnp.eye(BLOCK, dtype=jnp.float32)
    inverse = jax.scipy.linalg.solve_triangular(
        identity + lower_mat, jnp.broadcast_to(identity, lower_mat.shape), lower=True
    )
    new_values = jnp.einsum(
        "hnij,hnjd->hnid", inverse, value_vectors * beta_gate[..., None], precision=HIGHEST
    )
    key_weights = jnp.einsum(
        "hnij,hnjd->hnid", inverse, keys_scaled * jnp.exp(gate_sum)[..., None], precision=HIGHEST
    )
    scores = (
        jnp.einsum("hnid,hnjd->hnij", query_vectors, key_vectors, precision=HIGHEST) * causal_decay
    )
    last_gate = gate_sum[..., -1]
    query_decay = query_vectors * jnp.exp(gate_sum)[..., None]
    key_decay = key_vectors * jnp.exp(last_gate[..., None] - gate_sum)[..., None]
    return (query_decay, key_decay, new_values, key_weights, scores, last_gate)


def compose(earlier, following):
    return (
        jnp.einsum("hij,hjk->hik", following[0], earlier[0], precision=HIGHEST),
        jnp.einsum("hij,hjk->hik", following[0], earlier[1], precision=HIGHEST) + following[1],
    )


def keep_same(current):
    return current


def local(
    tokens,
    pre_gain,
    query_weight,
    key_weight,
    value_weight,
    beta_weight,
    decay_weight,
    decay_rate,
    delta_gain,
    query_down,
    latent_down,
    rope_weight,
    query_gain,
    latent_gain,
    query_up,
    latent_up,
    delta_out,
    latent_out,
    post_gain,
):
    f32 = jnp.float32
    seq_count, token_count = (tokens.shape[0], tokens.shape[1])
    row_total = seq_count * token_count
    sequence = tokens.reshape(row_total, tokens.shape[2]).astype(f32)
    query_start = lax.axis_index("sp") * token_count
    positions = query_start + jnp.arange(token_count)
    normed = (sequence * rms_scale(sequence) * pre_gain).astype(jnp.bfloat16)
    head_group = lax.axis_index("tp")
    q_width = query_down.shape[1] // lax.axis_size("tp")
    kv_width = latent_down.shape[1] // lax.axis_size("tp")
    q_own = lax.dynamic_slice_in_dim(query_down, head_group * q_width, q_width, 1)
    kv_own = lax.dynamic_slice_in_dim(latent_down, head_group * kv_width, kv_width, 1)
    weights = (query_weight, key_weight, value_weight, q_own, kv_own)
    portion = (
        lax.all_gather(query_weight, ("sp", "fs"), axis=0, tiled=True),
        lax.all_gather(key_weight, ("sp", "fs"), axis=0, tiled=True),
        lax.all_gather(value_weight, ("sp", "fs"), axis=0, tiled=True),
        lax.all_gather(q_own, ("sp", "fs"), axis=0, tiled=True),
        lax.all_gather(kv_own, ("sp", "fs"), axis=0, tiled=True),
    )
    row_count = portion[0].shape[0]
    projected = tuple((jnp.dot(normed, weight, preferred_element_type=f32) for weight in portion))
    raw_query, raw_key, raw_value, q_half, kv_half = tuple((stored(member) for member in projected))
    q_latent, kv_latent = (
        lax.all_gather(q_half, "tp", axis=1, tiled=True),
        lax.all_gather(kv_half, "tp", axis=1, tiled=True),
    )
    head_count = query_weight.shape[1] // HEAD
    lane_count = seq_count * head_count
    beta_full = jax.nn.sigmoid(jnp.dot(normed, beta_weight, preferred_element_type=f32))
    beta_gate = lax.dynamic_slice_in_dim(beta_full, head_group * head_count, head_count, 1)
    decay_full = jnp.dot(normed, decay_weight, preferred_element_type=f32)
    decay_pre = lax.dynamic_slice_in_dim(decay_full, head_group * head_count, head_count, 1)
    decay_local = lax.dynamic_slice_in_dim(decay_rate, head_group * head_count, head_count, 0)
    log_decay = -decay_local[None, :] * jax.nn.softplus(decay_pre)

    def by_position(values):
        shaped = values.reshape((seq_count, token_count) + values.shape[1:])
        shaped = jnp.moveaxis(shaped, 0, 1)
        return shaped.reshape((token_count, seq_count * values.shape[1]) + values.shape[2:])

    query_vectors = by_position(
        unit_rows(jax.nn.silu(raw_query.astype(f32)).reshape(row_total, head_count, HEAD))
        * HEAD ** (-0.5)
    )
    key_vectors = by_position(
        unit_rows(jax.nn.silu(raw_key.astype(f32)).reshape(row_total, head_count, HEAD))
    )
    value_vectors = by_position(
        jax.nn.silu(raw_value.astype(f32)).reshape(row_total, head_count, HEAD)
    )
    block_terms = delta_terms(
        query_vectors, key_vectors, value_vectors, by_position(beta_gate), by_position(log_decay)
    )
    inputs = tuple((jnp.moveaxis(tensor, 1, 0) for tensor in block_terms))

    def advance(totals, block_in):
        carried, transfer = totals
        query_decay, key_decay, new_values, key_weights, scores, last_gate = block_in
        corrected = new_values - jnp.einsum("hcd,hde->hce", key_weights, carried, precision=HIGHEST)
        output = jnp.einsum("hcd,hde->hce", query_decay, carried, precision=HIGHEST) + jnp.einsum(
            "hij,hje->hie", scores, corrected, precision=HIGHEST
        )
        reader_rows = query_decay - jnp.einsum(
            "hij,hjd->hid", scores, key_weights, precision=HIGHEST
        )
        reader = jnp.einsum("hcd,hde->hce", reader_rows, transfer, precision=HIGHEST)
        factor = jnp.exp(last_gate)[:, None, None]
        carried = carried * factor + jnp.einsum(
            "hcd,hce->hde", key_decay, corrected, precision=HIGHEST
        )
        moved = jnp.einsum("hcd,hde->hce", key_weights, transfer, precision=HIGHEST)
        transfer = transfer * factor - jnp.einsum(
            "hcd,hce->hde", key_decay, moved, precision=HIGHEST
        )
        return ((carried, transfer), (output, reader))

    eye_stack = jnp.broadcast_to(jnp.eye(HEAD, dtype=f32), (lane_count, HEAD, HEAD))
    zero_state = jnp.zeros((lane_count, HEAD, HEAD), f32)
    (state_end, transfer_end), (outputs, readers) = lax.scan(
        advance, (zero_state, eye_stack), inputs
    )
    _, incoming = prefix((transfer_end, state_end), "sp", compose, (eye_stack, zero_state))
    outputs = outputs + jnp.einsum("nhcd,hde->nhce", readers, incoming, precision=HIGHEST)
    delta_raw = jnp.transpose(outputs, (0, 2, 1, 3)).reshape(
        token_count, seq_count, head_count, HEAD
    )
    delta_raw = jnp.moveaxis(delta_raw, 1, 0).reshape(row_total, head_count, HEAD)
    delta_heads = (
        (delta_raw * rms_scale(delta_raw) * delta_gain)
        .astype(jnp.bfloat16)
        .reshape(row_total, head_count * HEAD)
    )
    q_lat32 = q_latent.astype(f32)
    kv_lat32 = kv_latent.astype(f32)
    q_normed = (q_lat32 * rms_scale(q_lat32) * query_gain).astype(jnp.bfloat16)
    kv_normed = (kv_lat32 * rms_scale(kv_lat32) * latent_gain).astype(jnp.bfloat16)
    rope_raw = stored(jnp.dot(normed, rope_weight, preferred_element_type=f32))
    cosine_table, sine_table = rope_tables(positions, rope_raw.shape[1])
    rope_keys = rotate(
        rope_raw.astype(f32).reshape(seq_count, token_count, rope_raw.shape[1]),
        cosine_table,
        sine_table,
    ).astype(jnp.bfloat16)
    latent_count = query_up.shape[1] // (NOPE + ROPE)
    query_all = stored(jnp.dot(q_normed, query_up, preferred_element_type=f32)).reshape(
        seq_count, token_count, latent_count, NOPE + ROPE
    )
    query_plain = query_all[..., :NOPE]
    query_turned = rotate(
        query_all[..., NOPE:].astype(f32), cosine_table[:, None, :], sine_table[:, None, :]
    ).astype(jnp.bfloat16)
    score_scale = (NOPE + ROPE) ** (-0.5)
    query_block = positions // BLOCK
    kv_seq = kv_normed.reshape(seq_count, token_count, kv_normed.shape[1])

    def attend_block(totals, key_plain, value_rows, rope_rows, key_start):
        row_max, row_sum, weighted = totals
        key_block = (key_start + jnp.arange(key_plain.shape[1])) // BLOCK
        allowed = key_block[None, :] <= query_block[:, None]
        logits = (
            jnp.einsum("sqhd,skhd->shqk", query_plain, key_plain, preferred_element_type=f32)
            + jnp.einsum("sqhd,skd->shqk", query_turned, rope_rows, preferred_element_type=f32)
        ) * score_scale
        logits = jnp.where(allowed[None, None], logits, -jnp.inf)
        new_max = jnp.maximum(row_max, jnp.max(logits, axis=-1))
        shift = jnp.where(jnp.isfinite(new_max), new_max, 0.0)
        weights = jnp.where(allowed[None, None], jnp.exp(logits - shift[..., None]), 0.0)
        rescale = jnp.exp(row_max - shift)
        row_sum = row_sum * rescale + jnp.sum(weights, axis=-1)
        weighted = weighted * rescale[..., None] + jnp.einsum(
            "shqk,skhd->shqd", weights.astype(jnp.bfloat16), value_rows, preferred_element_type=f32
        )
        return (new_max, row_sum, weighted)

    start_stats = (
        jnp.full((seq_count, latent_count, token_count), -jnp.inf, f32),
        jnp.zeros((seq_count, latent_count, token_count), f32),
        jnp.zeros((seq_count, latent_count, token_count, VDIM), f32),
    )

    def expand_latent(portion, row_start, span_rows):
        latent_rows = lax.dynamic_slice_in_dim(portion[0], row_start, span_rows, 1)
        expanded = jnp.dot(
            latent_rows.reshape(seq_count * span_rows, latent_rows.shape[2]),
            latent_up,
            preferred_element_type=f32,
        ).astype(jnp.bfloat16)
        expanded = expanded.reshape(seq_count, span_rows, latent_count, NOPE + VDIM)
        return (
            expanded[..., :NOPE],
            expanded[..., NOPE:],
            lax.dynamic_slice_in_dim(portion[1], row_start, span_rows, 1),
        )

    portion = (
        lax.all_gather(kv_seq, "sp", axis=1, tiled=True),
        lax.all_gather(rope_keys, "sp", axis=1, tiled=True),
    )
    row_count = portion[0].shape[1]
    span_rows = math.gcd(row_count, token_count * max(1, 512 // token_count))

    def visit_rows(current):

        def visit_block(block_index, stats):
            row_start = block_index * span_rows
            key_plain, value_rows, rope_rows = expand_latent(portion, row_start, span_rows)
            return attend_block(stats, key_plain, value_rows, rope_rows, row_start)

        return lax.fori_loop(0, row_count // span_rows, visit_block, current)

    row_max, row_sum, weighted = lax.cond(
        jnp.int32(0) < query_start + token_count, visit_rows, keep_same, start_stats
    )
    latent_heads = (
        jnp.transpose(weighted / row_sum[..., None], (0, 2, 1, 3))
        .reshape(row_total, latent_count * VDIM)
        .astype(jnp.bfloat16)
    )
    heads_joined = jnp.concatenate([delta_heads, latent_heads], axis=1)
    out_rows = jnp.concatenate([delta_out, latent_out], axis=0)
    partial_value = jnp.dot(
        heads_joined,
        lax.all_gather(out_rows, ("sp", "fs"), axis=1, tiled=True),
        preferred_element_type=f32,
    )
    mixed_half = lax.psum_scatter(
        partial_value.astype(jnp.bfloat16), "tp", scatter_dimension=1, tiled=True
    ).astype(jnp.float32)
    squares = lax.psum(jnp.sum(mixed_half * mixed_half, axis=1), "tp")
    row_scale = lax.rsqrt(squares / D + NORM_EPS)
    result = mixed_half * row_scale[:, None] * post_gain
    return result.astype(jnp.bfloat16).reshape(seq_count, token_count, result.shape[1])


def solution(mesh):
    return jax.shard_map(
        local,
        mesh=mesh,
        in_specs=(
            P(("grp", "fs"), "sp", None),
            P(),
            P(("sp", "fs"), "tp"),
            P(("sp", "fs"), "tp"),
            P(("sp", "fs"), "tp"),
            P(),
            P(),
            P(),
            P(),
            P(("sp", "fs"), None),
            P(("sp", "fs"), None),
            P(),
            P(),
            P(),
            P(None, "tp"),
            P(None, "tp"),
            P("tp", ("sp", "fs")),
            P("tp", ("sp", "fs")),
            P("tp"),
        ),
        out_specs=P(("grp", "fs"), "sp", "tp"),
        check_vma=False,
    )
```

profile of v0, /device:TPU:0, one launch (start us, length us, event | category | flops | bytes accessed | tf_op | source)
XLA Modules:
  0.0 364.7 jit_solution(9441882675673515229)
XLA Ops:
  6.6 0.7 all-gather.12.cloned.1.call-update
  7.3 0.7 all-gather.14.cloned.1.call-update
  8.1 1.6 constant_dynamic-slice_fusion
  9.7 0.5 all-gather.10.cloned.1.call-update
  10.3 1.2 multiply_reduce_fusion
  11.7 0.9 fusion.30
  13.9 47.4 %all-gather.12.cloned.1.call-done = bf16[2048,512]{1,0:T(8,128)(2,1)} async-done(((bf16[256,512]{1,0:T(8,128)(2,1)}), bf16[2048,512]{1,0:T(8,128)(2,1)}) %all-gather.12.cloned.1.call-update) | async-done | bytes 2097168 | tf_op jit(solution)/shard_map/all_gather | solution.py:158
  61.3 2.0 convolution_convert_fusion.4
  64.1 47.0 %all-gather.14.cloned.1.call-done = bf16[2048,512]{1,0:T(8,128)(2,1)} async-done(((bf16[256,512]{1,0:T(8,128)(2,1)}), bf16[2048,512]{1,0:T(8,128)(2,1)}) %all-gather.14.cloned.1.call-update) | async-done | bytes 2097168 | tf_op jit(solution)/shard_map/all_gather | solution.py:159
  111.1 2.0 convolution_convert_fusion.3
  113.6 0.6 fusion.24
  114.1 39.3 %custom-call.4 = f32[8,1,64,64]{2,3,1,0:T(8,128)S(1)} custom-call(f32[8,1,64,64]{3,2,1,0:T(8,128)S(1)} %fusion.24), custom_call_target="InvertDiagBlocksLowerTriangular" | custom-call | tf_op jit(solution)/shard_map/jit(_solve_triangular)/vmap()/triangular_solve | solution.py:93
  153.5 0.6 fusion.62
  154.1 0.4 fusion.60
  154.5 0.4 fusion.58
  155.3 1.8 fusion.20
  157.2 0.5 fusion.69
  157.7 1.7 fusion.19
  159.6 0.8 pad_maximum_fusion
  160.9 32.9 %all_gather.49 = bf16[2048,128]{1,0:T(8,128)(2,1)S(1)} all-gather(bf16[256,128]{1,0:T(8,128)(2,1)S(1)} %constant_dynamic-slice_fusion.1), channel_id=1, replica_groups=mesh['grp'=2,'sp'=4,'fs'=2,'tp'=2] {'sp','fs'}, dimensions={0}, use_global_device_ids=true | all-gather | bytes 589824 | tf_op jit(solution)/shard_map/all_gather | solution.py:161
  194.9 15.0 %all_gather.54 = bf16[2,256,32]{2,0,1:T(2,128)(2,1)} all-gather(bf16[2,64,32]{2,0,1:T(2,128)(2,1)S(1)} %pad_maximum_fusion.2), channel_id=1, replica_groups=mesh['grp'=2,'sp'=4,'fs'=2,'tp'=2] {'sp'}, dimensions={1}, use_global_device_ids=true | all-gather | bytes 40960 | tf_op jit(solution)/shard_map/all_gather | solution.py:300
  209.9 1.9 all_gather.50
  212.0 16.2 %all_gather.51 = bf16[2,256,256]{2,1,0:T(8,128)(2,1)S(1)} all-gather(bf16[2,64,256]{2,1,0:T(8,128)(2,1)S(1)} %bitcast.189), channel_id=1, replica_groups=mesh['grp'=2,'sp'=4,'fs'=2,'tp'=2] {'sp'}, dimensions={1}, use_global_device_ids=true | all-gather | bytes 327680 | tf_op jit(solution)/shard_map/all_gather | solution.py:299
  228.2 1.5 convolution_convert_fusion.6
  229.8 2.2 all_gather.53
  232.9 0.9 copy.102
  233.8 0.9 convert_element_type.164
  234.8 3.4 conditional.1
  234.9 0.4 fusion.3
  235.6 0.4 fusion.92
  236.1 0.5 convolution_bitcast_fusion
  236.9 0.4 fusion.93
  237.4 0.4 fusion.10
  237.8 0.4 convolution_add_fusion.1
  238.8 2.0 convolution_convert_fusion.5
  241.8 0.4 fusion.65
  242.2 0.5 convolution_multiply_fusion.1
  242.7 0.4 fusion.21
  243.1 0.4 convolution_subtract_fusion.1
  243.5 0.5 fusion.67
  244.1 22.4 %all-gather.20.cloned.1.call-done = bf16[32,128,128]{2,1,0:T(8,128)(2,1)} async-done(((bf16[8,128,128]{2,1,0:T(8,128)(2,1)}), bf16[32,128,128]{2,1,0:T(8,128)(2,1)}) %all-gather.20.cloned.1.call-update) | async-done | bytes 1048592 | tf_op jit(solution)/shard_map/all_gather | solution.py:24
  266.5 0.6 fusion.25
  267.8 74.7 %all-gather.18.cloned.1.call-done = bf16[1024,2048]{1,0:T(8,128)(2,1)} async-done(((bf16[1024,256]{1,0:T(8,128)(2,1)}), bf16[1024,2048]{1,0:T(8,128)(2,1)}) %all-gather.18.cloned.1.call-update) | async-done | bytes 4194320 | tf_op jit(solution)/shard_map/all_gather | solution.py:326
  342.5 3.7 %convolution_convert_fusion.1 = bf16[128,2048]{1,0:T(8,128)(2,1)} fusion(bf16[1024,2048]{1,0:T(8,128)(2,1)} %all-gather.18.cloned.1.call-done, bf16[128,512]{1,0:T(8,128)(2,1)S(1)} %convert_element_type.167, bf16[128,512]{1,0:T(8,128)(2,1)S(1)} %fusion.51), kind=kOutput, calls=%fused_computation.35 | convolution fusion | flops 537657344 | bytes 4980736 | tf_op jit(solution)/shard_map/dot_general | solution.py:324
  346.2 6.3 %reduce-scatter.2.cloned.1.call-done = bf16[128,1024]{1,0:T(8,128)(2,1)} async-done(((bf16[128,2048]{1,0:T(8,128)(2,1)}), bf16[128,1024]{1,0:T(8,128)(2,1)}) %reduce-scatter.2.cloned.1.call-update) | async-done | bytes 262160 | tf_op jit(solution)/shard_map/reduce_scatter | solution.py:329
  352.5 1.1 fusion.31
  353.6 2.5 psum.7
  356.1 1.8 fusion.33
  (127 shorter events, 8.9 us)
Async XLA Ops:
  6.5 225.6 %copy-start = (bf16[512,768]{1,0:T(8,128)(2,1)S(1)}, bf16[512,768]{1,0:T(8,128)(2,1)}, u32[]{:S(2)}) copy-start(bf16[512,768]{1,0:T(8,128)(2,1)} %param.37) | copy-start | bytes 2359300
  6.5 5.1 %copy-start.1 = (bf16[2,64,2048]{2,1,0:T(8,128)(2,1)S(1)}, bf16[2,64,2048]{2,1,0:T(8,128)(2,1)}, u32[]{:S(2)}) copy-start(bf16[2,64,2048]{2,1,0:T(8,128)(2,1)} %param.23) | copy-start | bytes 1572868
  6.5 6.0 %copy-start.7 = (bf16[2048,8]{0,1:T(8,128)(2,1)S(1)}, bf16[2048,8]{0,1:T(8,128)(2,1)}, u32[]{:S(2)}) copy-start(bf16[2048,8]{0,1:T(8,128)(2,1)} %param.28) | copy-start | bytes 98308
  6.5 6.3 %copy-start.8 = (bf16[2048,8]{0,1:T(8,128)(2,1)S(1)}, bf16[2048,8]{0,1:T(8,128)(2,1)}, u32[]{:S(2)}) copy-start(bf16[2048,8]{0,1:T(8,128)(2,1)} %param.29) | copy-start | bytes 98308
  6.5 6.5 %copy-start.14 = (f32[8]{0:T(128)S(1)}, f32[8]{0:T(128)}, u32[]{:S(2)}) copy-start(f32[8]{0:T(128)} %param.30) | copy-start | bytes 100
  6.5 54.8 %all-gather.12.cloned.1.call-start = ((), (), s32[]{:S(2)}) async-start(), calls=%async_computation.2 | async-start | bytes 2359296 | tf_op jit(solution)/shard_map/all_gather | solution.py:158
  7.3 103.8 %all-gather.14.cloned.1.call-start = ((), (), s32[]{:S(2)}) async-start(), calls=%async_computation.3 | async-start | bytes 2359296 | tf_op jit(solution)/shard_map/all_gather | solution.py:159
  8.0 220.2 %all-gather.16.cloned.1.call-start = ((), (), s32[]{:S(2)}) async-start(), calls=%async_computation.4 | async-start | bytes 1179648 | tf_op jit(solution)/shard_map/all_gather | solution.py:160
  9.7 229.2 %all-gather.10.cloned.1.call-start = ((), (), s32[]{:S(2)}) async-start(), calls=%async_computation.1 | async-start | bytes 2359296 | tf_op jit(solution)/shard_map/all_gather | solution.py:157
  10.3 233.8 %all-gather.22.cloned.1.call-start = ((), (), s32[]{:S(2)}) async-start(), calls=%async_computation.8 | async-start | bytes 1310720 | tf_op jit(solution)/shard_map/all_gather | solution.py:24
  154.5 5.1 %copy-start.4 = (bf16[512,256]{1,0:T(8,128)(2,1)S(1)}, bf16[512,256]{1,0:T(8,128)(2,1)}, u32[]{:S(2)}) copy-start(bf16[512,256]{1,0:T(8,128)(2,1)} %param.40) | copy-start | bytes 786436
  154.5 5.1 %copy-start.5 = (bf16[512,256]{1,0:T(8,128)(2,1)S(1)}, bf16[512,256]{1,0:T(8,128)(2,1)}, u32[]{:S(2)}) copy-start(bf16[512,256]{1,0:T(8,128)(2,1)} %param.39) | copy-start | bytes 786436
  155.3 5.2 %copy-start.6 = (bf16[2048,32]{0,1:T(8,128)(2,1)S(1)}, bf16[2048,32]{0,1:T(8,128)(2,1)}, u32[]{:S(2)}) copy-start(bf16[2048,32]{0,1:T(8,128)(2,1)} %param.34) | copy-start | bytes 393220
  157.1 3.8 %copy-start.9 = (bf16[256,256]{1,0:T(8,128)(2,1)S(1)}, bf16[256,256]{1,0:T(8,128)(2,1)}, u32[]{:S(2)}) copy-start(bf16[256,256]{1,0:T(8,128)(2,1)} %param.33) | copy-start | bytes 393220
  157.1 109.3 %all-gather.20.cloned.1.call-start = ((), (), s32[]{:S(2)}) async-start(), calls=%async_computation.7 | async-start | bytes 1310720 | tf_op jit(solution)/shard_map/all_gather | solution.py:24
  159.5 183.0 %all-gather.18.cloned.1.call-start = ((), (), s32[]{:S(2)}) async-start(), calls=%async_computation.5 | async-start | bytes 4718592 | tf_op jit(solution)/shard_map/all_gather | solution.py:326
  160.4 51.5 %copy-start.12 = (f32[256]{0:T(256)S(1)}, f32[256]{0:T(256)}, u32[]{:S(2)}) copy-start(f32[256]{0:T(256)} %param.36) | copy-start | bytes 3076
  160.4 67.8 %copy-start.13 = (f32[128]{0:T(128)S(1)}, f32[128]{0:T(128)}, u32[]{:S(2)}) copy-start(f32[128]{0:T(128)} %param.31) | copy-start | bytes 1540
  160.4 192.1 %reduce-scatter.2.cloned.1.call-start = ((), (), s32[]{:S(2)}) async-start(), calls=%async_computation.6 | async-start | bytes 786432 | tf_op jit(solution)/shard_map/reduce_scatter | solution.py:329
  194.4 37.7 %copy-start.11 = (f32[512]{0:T(512)S(1)}, f32[512]{0:T(512)}, u32[]{:S(2)}) copy-start(f32[512]{0:T(512)} %param.35) | copy-start | bytes 6148
  229.8 5.0 %copy-start.2 = (bf16[256,1024]{1,0:T(8,128)(2,1)S(1)}, bf16[256,1024]{1,0:T(8,128)(2,1)}, u32[]{:S(2)}) copy-start(bf16[256,1024]{1,0:T(8,128)(2,1)} %param.38) | copy-start | bytes 1572868
  236.0 0.9 copy-start.3
  267.8 88.3 %copy-start.10 = (f32[1024]{0:T(1024)S(1)}, f32[1024]{0:T(1024)}, u32[]{:S(2)}) copy-start(f32[1024]{0:T(1024)} %param.41) | copy-start | bytes 12292
Sparse Core Ops, SparseCore 0:
  9.5 51.7 all-gather.11
  63.4 47.6 all-gather.13
  113.2 39.2 all-gather.15
  154.5 51.2 all-gather.9
  207.2 31.1 all-gather.21
  239.8 26.5 all-gather.19
  268.5 73.9 all-gather.17
  346.4 6.0 reduce-scatter.1
where the time goes:
time: 365 us
  waiting for transfers between devices  200 us (55%)
  blocking collectives  70.7 us (19%)
  other arithmetic  49.8 us (14%)
  matrix products  23.7 us (6%)
  between operations  14.1 us (4%)
  local copies, waits for them, and re-layouts  6.24 us (2%)
    all_gather x1, waiting for transfers between devices, local(): lax.all_gather(out_rows, ('sp', 'fs'), axis=1, tiled=True)  74.7 us
    all_gather x1, waiting for transfers between devices, local(): lax.all_gather(key_weight, ('sp', 'fs'), axis=0, tiled=True)  47.4 us
    all_gather x1, waiting for transfers between devices, local(): lax.all_gather(value_weight, ('sp', 'fs'), axis=0, tiled=True)  47 us
    another operation x1, other arithmetic, delta_terms(): jax.scipy.linalg.solve_triangular(identity + lower_mat, jnp.broadcast_to(...  39.3 us
    all_gather x1, blocking collectives, local(): lax.all_gather(kv_own, ('sp', 'fs'), axis=0, tiled=True)  32.9 us
    all_gather x2, waiting for transfers between devices, prefix(): lax.all_gather(a.astype(kind), axis)  22.4 us
    all_gather x1, blocking collectives, local(): lax.all_gather(kv_seq, 'sp', axis=1, tiled=True)  16.2 us
    all_gather x1, blocking collectives, local(): lax.all_gather(rope_keys, 'sp', axis=1, tiled=True)  15 us
  transfers between devices with their start and end apart: 8, of which 5 were waited for; matrix products, arithmetic and copies ran while one was open for 20% of the time, Pallas kernels for 0%

commit v1 on v0

--- a/solution.py
+++ b/solution.py
@@ -3,6 +3,8 @@
 import jax
 import jax.numpy as jnp
 from jax import lax
+from jax.experimental import pallas as pl
+from jax.experimental.pallas import tpu as pltpu
 from jax.sharding import PartitionSpec as P
 
 D = 2048
@@ -335,9 +337,471 @@
     return result.astype(jnp.bfloat16).reshape(seq_count, token_count, result.shape[1])
 
 
+def pick(array, index):
+    return lax.dynamic_index_in_dim(array, index, 0, False)
+
+
+def dot32(left, right):
+    return jnp.dot(left, right, preferred_element_type=jnp.float32)
+
+
+def dot_t(left, right):
+    return lax.dot_general(
+        left, right, (((1,), (1,)), ((), ())), preferred_element_type=jnp.float32
+    )
+
+
+def two_parts(values):
+    high = values.astype(jnp.bfloat16)
+    return high, (values - high.astype(jnp.float32)).astype(jnp.bfloat16)
+
+
+def fine_dot(left, right, product=dot32):
+    left_high, left_low = two_parts(left)
+    right_high, right_low = two_parts(right)
+    return product(left_high, right_high) + (
+        product(left_high, right_low) + product(left_low, right_high)
+    )
+
+
+def kernel_call(body, out_shapes, args, scratch=(), scalars=1, name=None):
+    specs = [
+        pl.BlockSpec(memory_space=pltpu.SMEM if i < scalars else pltpu.VMEM)
+        for i in range(len(args))
+    ]
+    return pl.pallas_call(
+        body,
+        out_shape=out_shapes,
+        in_specs=specs,
+        out_specs=jax.tree.map(lambda _: pl.BlockSpec(memory_space=pltpu.VMEM), out_shapes),
+        scratch_shapes=scratch,
+        name=name,
+        compiler_params=pltpu.CompilerParams(vmem_limit_bytes=56 * 1024 * 1024),
+    )(*args)
+
+
+def outgoing_weights(ids, mixers, lats, sp_size):
+    half = mixers[0].shape[0] // 2
+    per_mixer = mixers[0].shape[1] // sp_size
+    per_lat = [w.shape[1] // sp_size // 2 for w in lats]
+    columns = len(mixers) * per_mixer + sum(per_lat)
+
+    def body(ids_ref, *refs):
+        rows = pl.ds(pl.multiple_of(ids_ref[2] * half, half), half)
+        first = ids_ref[3] == 0
+        out_ref = refs[-1]
+        for s in range(sp_size):
+            begin = 0
+            for ref in refs[: len(mixers)]:
+                out_ref[s, :, begin : begin + per_mixer] = ref[
+                    rows, s * per_mixer : (s + 1) * per_mixer
+                ]
+                begin += per_mixer
+            for ref, per in zip(refs[len(mixers) : -1], per_lat):
+                pair = ref[rows, 2 * s * per : 2 * (s + 1) * per]
+                out_ref[s, :, begin : begin + per] = jnp.where(first, pair[:, :per], pair[:, per:])
+                begin += per
+
+    return kernel_call(
+        body,
+        jax.ShapeDtypeStruct((sp_size, half, columns), jnp.bfloat16),
+        (ids, *mixers, *lats),
+        name="outgoing_weights",
+    )
+
+
+def outgoing_tokens(ids, tokens, gain, sp_size):
+    rows, width = tokens.shape
+    block = width // (sp_size * 4)
+
+    def body(ids_ref, token_ref, gain_ref, out_ref):
+        values = token_ref[...].astype(jnp.float32)
+        normed = (values * rms_scale(values) * gain_ref[...]).astype(jnp.bfloat16)
+        first = ids_ref[3] == 0
+        for f in range(2):
+            for s in range(sp_size):
+                begin = (s * 2 + f) * 2 * block
+                piece = jnp.where(
+                    first,
+                    normed[:, begin : begin + block],
+                    normed[:, begin + block : begin + 2 * block],
+                )
+                at = (f * sp_size + s) * block
+                for n in range(sp_size):
+                    out_ref[n, :, at : at + block] = piece
+
+    return kernel_call(
+        body,
+        jax.ShapeDtypeStruct((sp_size, rows, width // 2), jnp.bfloat16),
+        (ids, tokens, gain),
+        name="outgoing_tokens",
+    )
+
+
+def project(ids, mine, theirs, weights, extra, sizes):
+    seq_count, token_count, fine, q_cols, kv_cols = sizes
+    sp_size, rows, part = mine.shape
+    span = sp_size * token_count
+    extra_width = extra.shape[1]
+
+    def body(ids_ref, mine_ref, their_ref, weight_ref, extra_ref, fine_ref, lat_ref, ext_ref):
+        mine_at = pl.ds(pl.multiple_of(ids_ref[3] * part, part), part)
+        their_at = pl.ds(pl.multiple_of((1 - ids_ref[3]) * part, part), part)
+        for s in range(sp_size):
+            value = dot32(mine_ref[s], weight_ref[mine_at, :])
+            value = (value + dot32(their_ref[s], weight_ref[their_at, :])).astype(jnp.bfloat16)
+            outer = dot32(mine_ref[s], extra_ref[mine_at, :])
+            outer = outer + dot32(their_ref[s], extra_ref[their_at, :])
+            for n in range(seq_count):
+                cut = slice(n * token_count, (n + 1) * token_count)
+                at = slice(s * token_count, (s + 1) * token_count)
+                fine_ref[n, at, :] = value[cut, :fine]
+                ext_ref[n, at, :] = outer[cut]
+                for j in range(sp_size):
+                    lat_ref[j, n, at, :] = value[cut, fine:]
+
+    return kernel_call(
+        body,
+        (
+            jax.ShapeDtypeStruct((seq_count, span, fine), jnp.bfloat16),
+            jax.ShapeDtypeStruct((sp_size, seq_count, span, q_cols + kv_cols), jnp.bfloat16),
+            jax.ShapeDtypeStruct((seq_count, span, extra_width), jnp.float32),
+        ),
+        (ids, mine, theirs, weights, extra),
+        name="project",
+    )
+
+
+def lower_inverses(lowers, base):
+    size = lowers[0].shape[0]
+    row = lax.broadcasted_iota(jnp.int32, (size, size), 0)
+    col = lax.broadcasted_iota(jnp.int32, (size, size), 1)
+    unit = jnp.where(row == col, 1.0, 0.0)
+    powers = [jnp.where(row // base == col // base, low, 0.0) for low in lowers]
+    inverses = [unit - p for p in powers]
+    reach = 2
+    while reach < base:
+        powers = [fine_dot(p, p) for p in powers]
+        inverses = [i + fine_dot(i, p) for i, p in zip(inverses, powers)]
+        reach *= 2
+    block = base
+    while block < size:
+        joint = (row // (2 * block) == col // (2 * block)) & (row // block != col // block)
+        moved = [fine_dot(i, jnp.where(joint, low, 0.0)) for i, low in zip(inverses, lowers)]
+        inverses = [i - fine_dot(m, i) for i, m in zip(inverses, moved)]
+        block *= 2
+    return inverses
+
+
+def delta_mix(scalars, fine, ext, gain, rates, gate_at, heads, copies):
+    seq_count, span, _ = fine.shape
+    tile = math.gcd(span, 128)
+    tiles = span // tile
+    gates = rates.shape[1]
+
+    def terms(raw_query, raw_key, raw_value, beta_pre, decay_pre, rate):
+        query = unit_rows(jax.nn.silu(raw_query)) * HEAD ** (-0.5)
+        key = unit_rows(jax.nn.silu(raw_key))
+        value = jax.nn.silu(raw_value)
+        beta = jax.nn.sigmoid(beta_pre)
+        log_decay = -rate * jax.nn.softplus(decay_pre)
+        row = lax.broadcasted_iota(jnp.int32, (span, span), 0)
+        col = lax.broadcasted_iota(jnp.int32, (span, span), 1)
+        as_row = jnp.sum(jnp.where(row == col, log_decay, 0.0), axis=0, keepdims=True)
+        gate = jnp.sum(jnp.where(row >= col, as_row, 0.0), axis=1, keepdims=True)
+        gate_row = jnp.sum(jnp.where(row == col, gate, 0.0), axis=0, keepdims=True)
+        decay = jnp.where(row >= col, jnp.exp(jnp.where(row >= col, gate - gate_row, 0.0)), 0.0)
+        lower = fine_dot(key * beta, key, dot_t) * jnp.where(row > col, decay, 0.0)
+        scores = fine_dot(query, key, dot_t) * decay
+        return lower, scores, value * beta
+
+    def body(ids_ref, fine_ref, ext_ref, gain_ref, rate_ref, out_ref):
+        lane = lax.broadcasted_iota(jnp.int32, (span, ext.shape[2]), 1)
+        rate_lane = lax.broadcasted_iota(jnp.int32, (1, gates), 1)
+        chains = []
+        for n in range(seq_count):
+            for h in range(heads):
+                raw = [
+                    fine_ref[n, :, (k * heads + h) * HEAD : (k * heads + h + 1) * HEAD].astype(
+                        jnp.float32
+                    )
+                    for k in range(3)
+                ]
+                head = ids_ref[4] + h
+                outer = ext_ref[n]
+                beta_pre, decay_pre = (
+                    jnp.sum(
+                        jnp.where(lane == gate_at + k * gates + head, outer, 0.0),
+                        axis=1,
+                        keepdims=True,
+                    )
+                    for k in range(2)
+                )
+                rate = jnp.sum(
+                    jnp.where(rate_lane == head, rate_ref[...], 0.0), axis=1, keepdims=True
+                )
+                chains.append(terms(*raw, beta_pre, decay_pre, rate))
+        cuts = [slice(j * tile, (j + 1) * tile) for j in range(tiles)]
+        inverses = lower_inverses([c[0][cut, cut] for c in chains for cut in cuts], 8)
+        solved = [[] for _ in chains]
+        for j, cut in enumerate(cuts):
+            for i, (lower, _, wanted) in enumerate(chains):
+                rest = wanted[cut]
+                if j:
+                    rest = rest - fine_dot(
+                        lower[cut, : j * tile], jnp.concatenate(solved[i], axis=0)
+                    )
+                solved[i].append(fine_dot(inverses[i * tiles + j], rest))
+        for i, (_, scores, _) in enumerate(chains):
+            n, h = divmod(i, heads)
+            out = fine_dot(scores, jnp.concatenate(solved[i], axis=0))
+            out = (out * rms_scale(out) * gain_ref[...]).astype(jnp.bfloat16)
+            for j in range(copies):
+                out_ref[j, n * span : (n + 1) * span, h * HEAD : (h + 1) * HEAD] = out
+
+    return kernel_call(
+        body,
+        jax.ShapeDtypeStruct((copies, seq_count * span, heads * HEAD), jnp.bfloat16),
+        (scalars, fine, ext, gain, rates),
+        name="delta_mix",
+    )
+
+
+def latent_mix(ids, mine, theirs, ext, tables, gains, ups, q_cols, heads):
+    sp_size, seq_count, span, _ = mine.shape
+    scale = (NOPE + ROPE) ** (-0.5)
+
+    def body(ids_ref, mine_ref, their_ref, ext_ref, cos_ref, sin_ref, *refs):
+        qg_ref, kg_ref, qup_ref, kup_ref, out_ref = refs
+        first = ids_ref[3] == 0
+        row = lax.broadcasted_iota(jnp.int32, (span, span), 0) // BLOCK
+        col = lax.broadcasted_iota(jnp.int32, (span, span), 1) // BLOCK
+        allowed = col <= row
+        cosine, sine = cos_ref[...], sin_ref[...]
+        for n in range(seq_count):
+            q_parts, kv_parts = [], []
+            for s in range(sp_size):
+                own, other = mine_ref[s, n], their_ref[s, n]
+                pair = (jnp.where(first, own, other), jnp.where(first, other, own))
+                q_parts += [p[:, :q_cols] for p in pair]
+                kv_parts += [p[:, q_cols:] for p in pair]
+            q_lat = jnp.concatenate(q_parts, axis=1).astype(jnp.float32)
+            kv_lat = jnp.concatenate(kv_parts, axis=1).astype(jnp.float32)
+            q_norm = (q_lat * rms_scale(q_lat) * qg_ref[...]).astype(jnp.bfloat16)
+            kv_norm = (kv_lat * rms_scale(kv_lat) * kg_ref[...]).astype(jnp.bfloat16)
+            q_all = dot32(q_norm, qup_ref[...]).astype(jnp.bfloat16)
+            kv_all = dot32(kv_norm, kup_ref[...]).astype(jnp.bfloat16)
+            plain_width, turn_width = heads * NOPE, heads * ROPE
+            plain = q_all[:, :plain_width]
+            turn = q_all[:, plain_width : plain_width + turn_width].astype(jnp.float32)
+            swapped = q_all[:, plain_width + turn_width :].astype(jnp.float32)
+            turned = (turn * cosine + swapped * sine).astype(jnp.bfloat16)
+            raw = ext_ref[n, :, :ROPE].astype(jnp.bfloat16).astype(jnp.float32)
+            back = jnp.concatenate([raw[:, ROPE // 2 :], raw[:, : ROPE // 2]], axis=1)
+            key_turn = (raw * cosine[:, :ROPE] + back * sine[:, :ROPE]).astype(jnp.bfloat16)
+            results = []
+            for h in range(heads):
+                key_plain = kv_all[:, h * (NOPE + VDIM) : h * (NOPE + VDIM) + NOPE]
+                values = kv_all[:, h * (NOPE + VDIM) + NOPE : (h + 1) * (NOPE + VDIM)]
+                logits = (
+                    dot_t(plain[:, h * NOPE : (h + 1) * NOPE], key_plain)
+                    + dot_t(turned[:, h * ROPE : (h + 1) * ROPE], key_turn)
+                ) * scale
+                logits = jnp.where(allowed, logits, -jnp.inf)
+                peak = jnp.max(logits, axis=-1, keepdims=True)
+                weights = jnp.exp(logits - peak)
+                total = jnp.sum(weights, axis=-1, keepdims=True)
+                results.append(dot32(weights.astype(jnp.bfloat16), values) / total)
+            joined = jnp.concatenate(results, axis=1).astype(jnp.bfloat16)
+            for j in range(sp_size):
+                out_ref[j, n * span : (n + 1) * span, :] = joined
+
+    return kernel_call(
+        body,
+        jax.ShapeDtypeStruct((sp_size, seq_count * span, heads * VDIM), jnp.bfloat16),
+        (ids, mine, theirs, ext, *tables, *gains, *ups),
+        name="latent_mix",
+    )
+
+
+def output_partial(ids, delta_all, latent_all, weights, sizes):
+    seq_count, token_count = sizes
+    sp_size, rows, d_width = delta_all.shape
+    l_width = latent_all.shape[2]
+    span = sp_size * token_count
+    d_total, l_total = d_width * sp_size, l_width * sp_size
+    columns = weights[0].shape[1]
+
+    def body(ids_ref, d_ref, l_ref, d_own, d_other, l_own, l_other, keep_ref, pass_ref, lhs_ref):
+        for s in range(sp_size):
+            lhs_ref[:, s * d_width : (s + 1) * d_width] = d_ref[s]
+            lhs_ref[:, d_total + s * l_width : d_total + (s + 1) * l_width] = l_ref[s]
+        own = dot32(lhs_ref[:, :d_total], d_own[...]) + dot32(lhs_ref[:, d_total:], l_own[...])
+        other = dot32(lhs_ref[:, :d_total], d_other[...]) + dot32(
+            lhs_ref[:, d_total:], l_other[...]
+        )
+        own, other = own.astype(jnp.bfloat16), other.astype(jnp.bfloat16)
+        straight = ids_ref[1] == ids_ref[3]
+        keep, onward = jnp.where(straight, own, other), jnp.where(straight, other, own)
+        for n in range(seq_count):
+            for s in range(sp_size):
+                first = n * span + s * token_count
+                at = slice(n * token_count, (n + 1) * token_count)
+                keep_ref[s, at, :] = keep[first : first + token_count]
+                pass_ref[s, at, :] = onward[first : first + token_count]
+
+    shape = jax.ShapeDtypeStruct((sp_size, seq_count * token_count, columns), jnp.bfloat16)
+    return kernel_call(
+        body,
+        (shape, shape),
+        (ids, delta_all, latent_all, *weights),
+        scratch=(pltpu.VMEM((rows, d_total + l_total), jnp.bfloat16),),
+        name="output_partial",
+    )
+
+
+def whole_sequences(
+    tokens,
+    pre_gain,
+    query_weight,
+    key_weight,
+    value_weight,
+    beta_weight,
+    decay_weight,
+    decay_rate,
+    delta_gain,
+    query_down,
+    latent_down,
+    rope_weight,
+    query_gain,
+    latent_gain,
+    query_up,
+    latent_up,
+    delta_out,
+    latent_out,
+    post_gain,
+):
+    f32, bf16 = jnp.float32, jnp.bfloat16
+    sp_size, tp_size = lax.axis_size("sp"), lax.axis_size("tp")
+    place, fs_at = lax.axis_index("sp"), lax.axis_index("fs")
+    grp_at, tp_at = lax.axis_index("grp"), lax.axis_index("tp")
+    seq_count, token_count, width = tokens.shape
+    rows = seq_count * token_count
+    heads = query_weight.shape[1] // HEAD // sp_size
+    first_head = (tp_at * sp_size + place) * heads
+    ids = jnp.stack([place, fs_at, grp_at, tp_at, first_head]).astype(jnp.int32)
+    shares = sp_size * tp_size
+    q_cols, kv_cols = query_down.shape[1] // shares, latent_down.shape[1] // shares
+
+    def exchange(values, axis):
+        return lax.all_to_all(values, axis, 0, 0, tiled=True)
+
+    def swap(values, axis):
+        return lax.ppermute(values, axis, [(0, 1), (1, 0)])
+
+    outgoing = outgoing_weights(
+        ids, (query_weight, key_weight, value_weight), (query_down, latent_down), sp_size
+    )
+    block = exchange(outgoing, "sp")
+    block = jnp.broadcast_to(block.reshape(1, -1, outgoing.shape[2]), (4,) + (block.shape[0] * block.shape[1], outgoing.shape[2]))
+    weights = exchange(block, ("grp", "fs")).reshape(width, outgoing.shape[2])
+
+    token_rows, outgoing = lax.optimization_barrier((tokens.reshape(rows, width), outgoing))
+    mine = exchange(outgoing_tokens(ids, token_rows, pre_gain[None, :], sp_size), "sp")
+    theirs = swap(mine, "tp")
+
+    delta_other, latent_other = swap(delta_out, "fs"), swap(latent_out, "fs")
+
+    gate_at = rope_weight.shape[1]
+    filler = -(gate_at + 2 * beta_weight.shape[1]) % 128
+    extra = jnp.concatenate(
+        [rope_weight, beta_weight, decay_weight, jnp.zeros((width, filler), bf16)], axis=1
+    )
+    extra = extra.reshape(sp_size, 2, 2, width // (4 * sp_size), extra.shape[1])
+    extra = jnp.transpose(extra, (2, 1, 0, 3, 4)).reshape(width, extra.shape[4])
+
+    fine, lat, ext = project(
+        ids,
+        mine,
+        theirs,
+        weights,
+        extra,
+        (seq_count, token_count, 3 * heads * HEAD, q_cols, kv_cols),
+    )
+    lat_mine = exchange(lat, "sp")
+    lat_theirs = swap(lat_mine, "tp")
+
+    delta_heads = delta_mix(
+        ids, fine, ext, delta_gain[None, :], decay_rate[None, :], gate_at, heads, sp_size
+    )
+    delta_all = exchange(delta_heads, "sp")
+
+    latent_heads = query_up.shape[1] // (NOPE + ROPE) // sp_size
+    up = query_up.reshape(query_up.shape[0], sp_size, latent_heads, NOPE + ROPE)
+    up = lax.dynamic_index_in_dim(up, place, 1, False)
+    turn = up[..., NOPE:]
+    back = jnp.concatenate([turn[..., ROPE // 2 :], turn[..., : ROPE // 2]], axis=-1)
+    q_up = jnp.concatenate(
+        [a.reshape(up.shape[0], -1) for a in (up[..., :NOPE], turn, back)], axis=1
+    )
+    kv_width = latent_up.shape[1] // sp_size
+    kv_up = lax.dynamic_slice_in_dim(latent_up, place * kv_width, kv_width, 1)
+    cosine, sine = rope_tables(jnp.arange(sp_size * token_count), ROPE)
+    tables = (
+        jnp.tile(jnp.concatenate([cosine, cosine], axis=1), (1, latent_heads)),
+        jnp.tile(jnp.concatenate([-sine, sine], axis=1), (1, latent_heads)),
+    )
+    latent = latent_mix(
+        ids,
+        lat_mine,
+        lat_theirs,
+        ext,
+        tables,
+        (query_gain[None, :], latent_gain[None, :]),
+        (q_up, kv_up),
+        q_cols,
+        latent_heads,
+    )
+    latent_all = exchange(latent, "sp")
+
+    keep, onward = output_partial(
+        ids,
+        delta_all,
+        latent_all,
+        (delta_out, delta_other, latent_out, latent_other),
+        (seq_count, token_count),
+    )
+    mixed = (keep.astype(f32) + swap(onward, "tp").astype(f32)).astype(bf16)
+    landed = exchange(mixed, "sp")
+    per_tp = sp_size // tp_size
+    squares = jnp.sum(landed.astype(f32) * landed.astype(f32), axis=(0, 2))[:, None]
+    squares = squares + swap(squares, "tp")
+    here = lax.dynamic_slice_in_dim(landed, tp_at * per_tp, per_tp, 0)
+    there = swap(lax.dynamic_slice_in_dim(landed, (1 - tp_at) * per_tp, per_tp, 0), "tp")
+    low, high = jnp.where(tp_at == 0, here, there), jnp.where(tp_at == 0, there, here)
+    final = jnp.concatenate(
+        [half[k] for k in range(per_tp) for half in (low, high)], axis=1
+    ).astype(f32)
+    result = final * lax.rsqrt(squares / D + NORM_EPS) * post_gain
+    return result.astype(bf16).reshape(seq_count, token_count, final.shape[1])
+
+
+def fits_whole(mesh):
+    shape = mesh.shape
+    pairs = all(shape[name] == 2 for name in ("grp", "fs", "tp"))
+    return pairs and shape["sp"] % shape["tp"] == 0
+
+
 def solution(mesh):
+    def chosen(*args):
+        head_count = args[2].shape[1] // HEAD
+        latent_count = args[14].shape[1] // (NOPE + ROPE)
+        sp_size = mesh.shape["sp"]
+        whole = fits_whole(mesh) and head_count % sp_size == 0 and latent_count % sp_size == 0
+        return (whole_sequences if whole else local)(*args)
+
     return jax.shard_map(
-        local,
+        chosen,
         mesh=mesh,
         in_specs=(
             P(("grp", "fs"), "sp", None),

time: 365 us -> 166 us (0.45)
  waiting for transfers between devices: 200 us -> 83.9 us
  blocking collectives: 70.7 us -> 0 us
  other arithmetic: 49.8 us -> 5.59 us
  starting transfers between devices: 0.32 us -> 31.2 us
  matrix products: 23.7 us -> 0 us
  Pallas kernels: 0 us -> 23.7 us
  between operations: 14.1 us -> 0.28 us
  local copies, waits for them, and re-layouts: 6.24 us -> 20 us
    all_gather x7 -> x0, waiting for transfers between devices: 192 us -> none  [the longest x1 74.7 us: local(): lax.all_gather(out_rows, ('sp', 'fs'), axis=1, tiled=True)]
    all_to_all x0 -> x7, waiting for transfers between devices: none -> 70.5 us  [exchange(): return lax.all_to_all(values, axis, 0, 0, tiled=True)]
    all_gather x5 -> x0, blocking collectives: 68.2 us -> none  [the longest x1 32.9 us: local(): lax.all_gather(kv_own, ('sp', 'fs'), axis=0, tiled=True)]
    another operation x4 -> x0, other arithmetic: 39.7 us -> none  [the longest x1 39.3 us: delta_terms(): jax.scipy.linalg.solve_triangular(identity + lower_mat, jnp.broadcast_to(...]
    all_to_all x0 -> x7, starting transfers between devices: none -> 28.4 us  [exchange(): return lax.all_to_all(values, axis, 0, 0, tiled=True)]
    pallas_call x0 -> x6, Pallas kernels: none -> 23.7 us  [kernel_call(): pl.pallas_call(body, out_shape=out_shapes, in_specs=specs, out_specs=jax....]
    dot_general x27 -> x0, matrix products: 23.1 us -> none  [the longest x5 7.94 us: local(): jnp.dot(normed, weight, preferred_element_type=f32)]
    ppermute x0 -> x7, waiting for transfers between devices: none -> 13.5 us  [swap(): return lax.ppermute(values, axis, [(0, 1), (1, 0)])]
  transfers between devices with their start and end apart: 8 -> 14, of which waited for: 5 -> 11; matrix products, arithmetic and copies ran while one was open for 20% -> 9% of each run, Pallas kernels for 0% -> 8%
where the time goes in v1:
time: 166 us; the launch traced here: 165 us
  waiting for transfers between devices  83.9 us (51%)
  starting transfers between devices  31.2 us (19%)
  Pallas kernels  23.7 us (14%)
  local copies, waits for them, and re-layouts  20 us (12%)
  other arithmetic  5.59 us (3%)
    all_to_all x7, waiting for transfers between devices, exchange(): return lax.all_to_all(values, axis, 0, 0, tiled=True)  70.5 us
    all_to_all x7, starting transfers between devices, exchange(): return lax.all_to_all(values, axis, 0, 0, tiled=True)  28.4 us
    pallas_call x6, Pallas kernels, kernel_call(): pl.pallas_call(body, out_shape=out_shapes, in_specs=specs, out_specs=jax....  23.7 us
    ppermute x7, waiting for transfers between devices, swap(): return lax.ppermute(values, axis, [(0, 1), (1, 0)])  13.5 us
    unnamed x28, local copies, waits for them, and re-layouts  7.38 us
    pallas_call x2, local copies, waits for them, and re-layouts, kernel_call(): pl.pallas_call(body, out_shape=out_shapes, in_specs=specs, out_specs=jax....  4.1 us
  transfers between devices with their start and end apart: 14, of which 11 were waited for; matrix products, arithmetic and copies ran while one was open for 9% of the time, Pallas kernels for 8%

profile of v1, /device:TPU:0, one launch (start us, length us, event | category | flops | bytes accessed | tf_op | source)
XLA Modules:
  0.0 164.7 jit_solution(14066836864536433562)
XLA Ops:
  0.0 0.7 stack.23.ids_ref
  0.7 2.3 %outgoing_weights.1 = bf16[4,128,480]{2,1,0:T(8,128)(2,1)} custom-call(s32[5]{0:T(128)} %stack.23.ids_ref, bf16[256,512]{1,0:T(8,128)(2,1)} %refs_0_.1, bf16[256,512]{1,0:T(8,128)(2,1)} %refs_1_.1, bf16[256,512]{1,0:T(8,128)(2,1)} %refs_2_.1, bf16[256,512]{1,0:T(8,128)(2,1)} %refs_3_.1, bf16[256,256]{1,0:T(8,128)(2,1)} %refs_4_.1), custom_call_target="tpu_custom_call" | custom-call | tf_op jit(solution)/shard_map/outgoing_weights/pallas_call | solution.py:372
  3.0 2.0 %copy.48 = bf16[4,128,480]{1,2,0:T(8,128)(2,1)} copy(bf16[4,128,480]{2,1,0:T(8,128)(2,1)} %outgoing_weights.1) | data formatting | bytes 983040 | tf_op jit(solution)/shard_map/outgoing_weights/pallas_call | solution.py:372
  5.0 6.3 %all-to-all-start.1 = ((bf16[4,128,480]{1,2,0:T(8,128)(2,1)}), bf16[4,128,480]{1,2,0:T(8,128)(2,1)S(1)}, u32[]{:S(2)}, u32[]{:S(2)}) async-start(bf16[4,128,480]{1,2,0:T(8,128)(2,1)} %copy.48), calls=%async_computation.1 | async-start | bytes 983040 | tf_op jit(solution)/shard_map/all_to_all | solution.py:697
  11.4 2.5 %outgoing_tokens.1 = bf16[4,128,1024]{2,1,0:T(8,128)(2,1)} custom-call(s32[5]{0:T(128)} %stack.23.ids_ref, bf16[128,2048]{1,0:T(8,128)(2,1)} %bitcast.39, f32[1,2048]{1,0:T(1,128)} %bitcast.49), custom_call_target="tpu_custom_call" | custom-call | tf_op jit(solution)/shard_map/outgoing_tokens/pallas_call | solution.py:372
  13.9 11.3 %all-to-all-done.1 = bf16[4,128,480]{1,2,0:T(8,128)(2,1)S(1)} async-done(((bf16[4,128,480]{1,2,0:T(8,128)(2,1)}), bf16[4,128,480]{1,2,0:T(8,128)(2,1)S(1)}, u32[]{:S(2)}, u32[]{:S(2)}) %all-to-all-start.1) | async-done | bytes 491552 | tf_op jit(solution)/shard_map/all_to_all | solution.py:697
  25.2 3.5 %all-to-all-start = ((bf16[4,128,1024]{2,1,0:T(8,128)(2,1)}), bf16[4,128,1024]{2,1,0:T(8,128)(2,1)S(1)}, u32[]{:S(2)}, u32[]{:S(2)}) async-start(bf16[4,128,1024]{2,1,0:T(8,128)(2,1)} %outgoing_tokens.1), calls=%async_computation | async-start | bytes 2097152 | tf_op jit(solution)/shard_map/all_to_all | solution.py:697
  28.7 25.2 %all-to-all-done.mine_ref = bf16[4,128,1024]{2,1,0:T(8,128)(2,1)S(1)} async-done(((bf16[4,128,1024]{2,1,0:T(8,128)(2,1)}), bf16[4,128,1024]{2,1,0:T(8,128)(2,1)S(1)}, u32[]{:S(2)}, u32[]{:S(2)}) %all-to-all-start) | async-done | bytes 1048608 | tf_op jit(solution)/shard_map/all_to_all | solution.py:697
  54.0 1.5 broadcast_in_dim.33
  55.5 3.7 %all-to-all-start.2 = ((bf16[4,512,480]{1,2,0:T(8,128)(2,1)}), bf16[4,512,480]{1,2,0:T(8,128)(2,1)S(1)}, u32[]{:S(2)}, u32[]{:S(2)}) async-start(bf16[4,512,480]{1,2,0:T(8,128)(2,1)} %broadcast_in_dim.33), calls=%async_computation.2 | async-start | bytes 3932160 | tf_op jit(solution)/shard_map/all_to_all | solution.py:697
  59.2 1.9 %copy.51 = bf16[2048,32]{1,0:T(8,128)(2,1)} copy(bf16[2048,32]{0,1:T(8,128)(2,1)} %param.30) | data formatting | bytes 262144 | tf_op args[11]
  61.1 1.8 %copy.52 = bf16[2048,8]{1,0:T(8,128)(2,1)} copy(bf16[2048,8]{0,1:T(8,128)(2,1)} %param.24) | data formatting | bytes 65536 | tf_op args[5]
  62.9 1.8 %copy.53 = bf16[2048,8]{1,0:T(8,128)(2,1)} copy(bf16[2048,8]{0,1:T(8,128)(2,1)} %param.25) | data formatting | bytes 65536 | tf_op args[6]
  64.8 1.9 %maximum_maximum_fusion = bf16[2048,128]{1,0:T(8,128)(2,1)S(1)} fusion(bf16[2048,8]{1,0:T(8,128)(2,1)} %copy.53, bf16[2048,8]{1,0:T(8,128)(2,1)} %copy.52, bf16[2048,32]{1,0:T(8,128)(2,1)} %copy.51, bf16[128]{0:T(256)(128)(2,1)S(1)} %pad.16.clone), kind=kLoop, calls=%fused_computation | loop fusion | flops 2097152 | bytes 721152 | tf_op jit(solution)/shard_map/concatenate | solution.py:717
  66.7 0.9 copy.54
  67.5 14.6 %all-to-all-done.2 = bf16[4,512,480]{1,2,0:T(8,128)(2,1)S(1)} async-done(((bf16[4,512,480]{1,2,0:T(8,128)(2,1)}), bf16[4,512,480]{1,2,0:T(8,128)(2,1)S(1)}, u32[]{:S(2)}, u32[]{:S(2)}) %all-to-all-start.2) | async-done | bytes 1966112 | tf_op jit(solution)/shard_map/all_to_all | solution.py:697
  82.1 2.4 %copy.50 = bf16[4,512,480]{2,1,0:T(8,128)(2,1)} copy(bf16[4,512,480]{1,2,0:T(8,128)(2,1)S(1)} %all-to-all-done.2) | data formatting | bytes 3932160 | tf_op jit(solution)/shard_map/all_to_all | solution.py:697
  84.5 5.0 %project.1 = (bf16[2,256,384]{2,1,0:T(8,128)(2,1)}, bf16[4,2,256,96]{3,2,1,0:T(8,128)(2,1)}, f32[2,256,128]{2,1,0:T(8,128)}) custom-call(s32[5]{0:T(128)} %stack.23.ids_ref, bf16[4,128,1024]{2,1,0:T(8,128)(2,1)} %copy-done.1, bf16[4,128,1024]{2,1,0:T(8,128)(2,1)} %collective-permute-done.their_ref, bf16[2048,480]{1,0:T(8,128)(2,1)} %bitcast.35, ...), custom_call_target="tpu_custom_call" | custom-call | tf_op jit(solution)/shard_map/project/pallas_call | solution.py:372
  89.5 2.1 %copy.55 = bf16[4,2,256,96]{2,3,1,0:T(8,128)(2,1)} copy(bf16[4,2,256,96]{3,2,1,0:T(8,128)(2,1)} %get-tuple-element.14) | data formatting | bytes 786432 | tf_op jit(solution)/shard_map/project/pallas_call | solution.py:372
  91.5 3.5 %all-to-all-start.4 = ((bf16[4,2,256,96]{2,3,1,0:T(8,128)(2,1)}), bf16[4,2,256,96]{2,3,1,0:T(8,128)(2,1)S(1)}, u32[]{:S(2)}, u32[]{:S(2)}) async-start(bf16[4,2,256,96]{2,3,1,0:T(8,128)(2,1)} %copy.55), calls=%async_computation.4 | async-start | bytes 786432 | tf_op jit(solution)/shard_map/all_to_all | solution.py:697
  95.0 0.3 copy.57
  95.3 0.1 fusion
  95.5 5.5 %delta_mix.1 = bf16[4,512,128]{2,1,0:T(8,128)(2,1)} custom-call(s32[5]{0:T(128)} %stack.23.ids_ref, bf16[2,256,384]{2,1,0:T(8,128)(2,1)} %get-tuple-element.12.fine_ref, f32[2,256,128]{2,1,0:T(8,128)} %get-tuple-element.13.ext_ref, f32[1,128]{1,0:T(1,128)} %bitcast.52, f32[1,8]{1,0:T(1,128)} %bitcast.53), custom_call_target="tpu_custom_call" | custom-call | tf_op jit(solution)/shard_map/delta_mix/pallas_call | solution.py:372
  101.0 5.2 %all-to-all-done.4 = bf16[4,2,256,96]{2,3,1,0:T(8,128)(2,1)S(1)} async-done(((bf16[4,2,256,96]{2,3,1,0:T(8,128)(2,1)}), bf16[4,2,256,96]{2,3,1,0:T(8,128)(2,1)S(1)}, u32[]{:S(2)}, u32[]{:S(2)}) %all-to-all-start.4) | async-done | bytes 393248 | tf_op jit(solution)/shard_map/all_to_all | solution.py:697
  106.2 3.5 %all-to-all-start.3 = ((bf16[4,512,128]{2,1,0:T(8,128)(2,1)}), bf16[4,512,128]{2,1,0:T(8,128)(2,1)S(1)}, u32[]{:S(2)}, u32[]{:S(2)}) async-start(bf16[4,512,128]{2,1,0:T(8,128)(2,1)} %delta_mix.1), calls=%async_computation.3 | async-start | bytes 1048576 | tf_op jit(solution)/shard_map/all_to_all | solution.py:697
  109.7 0.3 copy.61.mine_ref
  110.5 0.8 copy.62.cos_ref
  111.3 0.8 copy.63.sin_ref
  112.0 0.7 constant_dynamic-slice_fusion.1.refs_3_
  112.7 0.8 pad_maximum_fusion.refs_2_
  113.5 0.8 copy-done.6
  114.3 5.3 %latent_mix.1 = bf16[4,512,128]{2,1,0:T(8,128)(2,1)} custom-call(s32[5]{0:T(128)} %stack.23.ids_ref, bf16[4,2,256,96]{3,2,1,0:T(8,128)(2,1)} %copy-done.4, bf16[4,2,256,96]{3,2,1,0:T(8,128)(2,1)} %copy-done.6, f32[2,256,128]{2,1,0:T(8,128)} %get-tuple-element.13.ext_ref, f32[256,64]{1,0:T(8,128)} %copy.62.cos_ref, f32[256,64]{1,0:T(8,128)} %copy.63.sin_ref, ...), custom_call_target="tpu_custom_call" | custom-call | tf_op jit(solution)/shard_map/latent_mix/pallas_call | solution.py:372
  119.7 4.0 %all-to-all-done.3.d_ref = bf16[4,512,128]{2,1,0:T(8,128)(2,1)S(1)} async-done(((bf16[4,512,128]{2,1,0:T(8,128)(2,1)}), bf16[4,512,128]{2,1,0:T(8,128)(2,1)S(1)}, u32[]{:S(2)}, u32[]{:S(2)}) %all-to-all-start.3) | async-done | bytes 524320 | tf_op jit(solution)/shard_map/all_to_all | solution.py:697
  123.7 3.5 %all-to-all-start.5 = ((bf16[4,512,128]{2,1,0:T(8,128)(2,1)}), bf16[4,512,128]{2,1,0:T(8,128)(2,1)S(1)}, u32[]{:S(2)}, u32[]{:S(2)}) async-start(bf16[4,512,128]{2,1,0:T(8,128)(2,1)} %latent_mix.1), calls=%async_computation.5 | async-start | bytes 1048576 | tf_op jit(solution)/shard_map/all_to_all | solution.py:697
  127.2 2.0 %collective-permute-start.3 = (bf16[512,256]{1,0:T(8,128)(2,1)S(1)}, bf16[512,256]{1,0:T(8,128)(2,1)S(1)}, u32[]{:S(2)}, u32[]{:S(2)}) collective-permute-start(bf16[512,256]{1,0:T(8,128)(2,1)S(1)} %copy-done.8), channel_id=1, source_target_pairs={{0,2},{2,0},{1,3},{3,1},{4,6},{6,4},{5,7},{7,5},{8,10},{10,8},{9,1... | collective-permute-start | bytes 786440 | tf_op jit(solution)/shard_map/ppermute | solution.py:700
  129.2 7.1 %collective-permute-done.2.d_other = bf16[512,256]{1,0:T(8,128)(2,1)S(1)} collective-permute-done((bf16[512,256]{1,0:T(8,128)(2,1)S(1)}, bf16[512,256]{1,0:T(8,128)(2,1)S(1)}, u32[]{:S(2)}, u32[]{:S(2)}) %collective-permute-start.2) | collective-permute-done | bytes 262176 | tf_op jit(solution)/shard_map/ppermute | solution.py:700
  136.4 3.8 %collective-permute-done.3.l_other = bf16[512,256]{1,0:T(8,128)(2,1)S(1)} collective-permute-done((bf16[512,256]{1,0:T(8,128)(2,1)S(1)}, bf16[512,256]{1,0:T(8,128)(2,1)S(1)}, u32[]{:S(2)}, u32[]{:S(2)}) %collective-permute-start.3) | collective-permute-done | bytes 262176 | tf_op jit(solution)/shard_map/ppermute | solution.py:700
  140.1 1.0 all-to-all-done.5.l_ref
  141.2 0.8 copy-done.3
  142.0 3.1 %output_partial.1 = (bf16[4,128,256]{2,1,0:T(8,128)(2,1)}, bf16[4,128,256]{2,1,0:T(8,128)(2,1)}) custom-call(s32[5]{0:T(128)} %stack.23.ids_ref, bf16[4,512,128]{2,1,0:T(8,128)(2,1)} %copy-done.2, bf16[4,512,128]{2,1,0:T(8,128)(2,1)} %copy-done.3, bf16[512,256]{1,0:T(8,128)(2,1)} %d_own.1, bf16[512,256]{1,0:T(8,128)(2,1)} %copy-done.9, ...), custom_call_target="tpu_custom_call" | custom-call | tf_op jit(solution)/shard_map/output_partial/pallas_call | solution.py:372
  145.0 1.7 %collective-permute-done.4 = bf16[4,128,256]{2,1,0:T(8,128)(2,1)S(1)} collective-permute-done((bf16[4,128,256]{2,1,0:T(8,128)(2,1)}, bf16[4,128,256]{2,1,0:T(8,128)(2,1)S(1)}, u32[]{:S(2)}, u32[]{:S(2)}) %collective-permute-start.4) | collective-permute-done | bytes 262176 | tf_op jit(solution)/shard_map/ppermute | solution.py:700
  146.8 1.7 %add_convert_fusion = bf16[4,128,256]{2,1,0:T(8,128)(2,1)} fusion(bf16[4,128,256]{2,1,0:T(8,128)(2,1)S(1)} %collective-permute-done.4, bf16[4,128,256]{2,1,0:T(8,128)(2,1)} %get-tuple-element.15), kind=kLoop, calls=%fused_computation.3 | loop fusion | flops 524288 | bytes 786432 | tf_op jit(solution)/shard_map/convert_element_type | solution.py:774
  148.5 4.4 %all-to-all-start.6 = ((bf16[4,128,256]{2,1,0:T(8,128)(2,1)}), bf16[4,128,256]{2,1,0:T(8,128)(2,1)S(1)}, u32[]{:S(2)}, u32[]{:S(2)}) async-start(bf16[4,128,256]{2,1,0:T(8,128)(2,1)} %add_convert_fusion), calls=%async_computation.6 | async-start | bytes 524288 | tf_op jit(solution)/shard_map/all_to_all | solution.py:697
  152.9 9.2 %all-to-all-done.6 = bf16[4,128,256]{2,1,0:T(8,128)(2,1)S(1)} async-done(((bf16[4,128,256]{2,1,0:T(8,128)(2,1)}), bf16[4,128,256]{2,1,0:T(8,128)(2,1)S(1)}, u32[]{:S(2)}, u32[]{:S(2)}) %all-to-all-start.6) | async-done | bytes 262176 | tf_op jit(solution)/shard_map/all_to_all | solution.py:697
  162.2 0.1 multiply_reduce_fusion
  162.3 0.6 collective-permute-start.6
  162.9 0.8 collective-permute-done.6
  163.9 0.8 multiply_convert_fusion
  (52 shorter events, 1.0 us)
Async XLA Ops:
  0.0 112.0 %copy-start = (bf16[256,1024]{1,0:T(8,128)(2,1)S(1)}, bf16[256,1024]{1,0:T(8,128)(2,1)}, u32[]{:S(2)}) copy-start(bf16[256,1024]{1,0:T(8,128)(2,1)} %param.34) | copy-start | bytes 1572868
  5.0 20.1 %all-to-all-start.1 = ((bf16[4,128,480]{1,2,0:T(8,128)(2,1)}), bf16[4,128,480]{1,2,0:T(8,128)(2,1)S(1)}, u32[]{:S(2)}, u32[]{:S(2)}) async-start(bf16[4,128,480]{1,2,0:T(8,128)(2,1)} %copy.48), calls=%async_computation.1 | async-start | bytes 983040 | tf_op jit(solution)/shard_map/all_to_all | solution.py:697
  25.2 28.8 %all-to-all-start = ((bf16[4,128,1024]{2,1,0:T(8,128)(2,1)}), bf16[4,128,1024]{2,1,0:T(8,128)(2,1)S(1)}, u32[]{:S(2)}, u32[]{:S(2)}) async-start(bf16[4,128,1024]{2,1,0:T(8,128)(2,1)} %outgoing_tokens.1), calls=%async_computation | async-start | bytes 2097152 | tf_op jit(solution)/shard_map/all_to_all | solution.py:697
  54.0 5.3 %copy-start.1 = (bf16[4,128,1024]{2,1,0:T(8,128)(2,1)}, bf16[4,128,1024]{2,1,0:T(8,128)(2,1)S(1)}, u32[]{:S(2)}) copy-start(bf16[4,128,1024]{2,1,0:T(8,128)(2,1)S(1)} %all-to-all-done.mine_ref) | copy-start | bytes 3145732
  55.5 26.6 %all-to-all-start.2 = ((bf16[4,512,480]{1,2,0:T(8,128)(2,1)}), bf16[4,512,480]{1,2,0:T(8,128)(2,1)S(1)}, u32[]{:S(2)}, u32[]{:S(2)}) async-start(bf16[4,512,480]{1,2,0:T(8,128)(2,1)} %broadcast_in_dim.33), calls=%async_computation.2 | async-start | bytes 3932160 | tf_op jit(solution)/shard_map/all_to_all | solution.py:697
  59.2 25.2 %collective-permute-start = (bf16[4,128,1024]{2,1,0:T(8,128)(2,1)S(1)}, bf16[4,128,1024]{2,1,0:T(8,128)(2,1)}, u32[]{:S(2)}, u32[]{:S(2)}) collective-permute-start(bf16[4,128,1024]{2,1,0:T(8,128)(2,1)S(1)} %all-to-all-done.mine_ref), channel_id=1, source_target_pairs={{0,1},{1,0},{2,3},{3,2},{4,5},{5,4},{6,7},{7,6},{8,9},{9,8},{10,11... | collective-permute-start | bytes 3145736 | tf_op jit(solution)/shard_map/ppermute | solution.py:700
  89.5 5.5 %copy-start.5 = (bf16[512,768]{1,0:T(8,128)(2,1)S(1)}, bf16[512,768]{1,0:T(8,128)(2,1)}, u32[]{:S(2)}) copy-start(bf16[512,768]{1,0:T(8,128)(2,1)} %param.33) | copy-start | bytes 2359300
  91.5 14.6 %all-to-all-start.4 = ((bf16[4,2,256,96]{2,3,1,0:T(8,128)(2,1)}), bf16[4,2,256,96]{2,3,1,0:T(8,128)(2,1)S(1)}, u32[]{:S(2)}, u32[]{:S(2)}) async-start(bf16[4,2,256,96]{2,3,1,0:T(8,128)(2,1)} %copy.55), calls=%async_computation.4 | async-start | bytes 786432 | tf_op jit(solution)/shard_map/all_to_all | solution.py:697
  106.2 17.5 %all-to-all-start.3 = ((bf16[4,512,128]{2,1,0:T(8,128)(2,1)}), bf16[4,512,128]{2,1,0:T(8,128)(2,1)S(1)}, u32[]{:S(2)}, u32[]{:S(2)}) async-start(bf16[4,512,128]{2,1,0:T(8,128)(2,1)} %delta_mix.1), calls=%async_computation.3 | async-start | bytes 1048576 | tf_op jit(solution)/shard_map/all_to_all | solution.py:697
  110.0 3.5 %copy-start.4 = (bf16[4,2,256,96]{3,2,1,0:T(8,128)(2,1)}, bf16[4,2,256,96]{3,2,1,0:T(8,128)(2,1)S(1)}, u32[]{:S(2)}) copy-start(bf16[4,2,256,96]{3,2,1,0:T(8,128)(2,1)S(1)} %copy.61.mine_ref) | copy-start | bytes 1179652
  110.0 3.5 %collective-permute-start.1 = (bf16[4,2,256,96]{3,2,1,0:T(8,128)(2,1)S(1)}, bf16[4,2,256,96]{3,2,1,0:T(8,128)(2,1)S(1)}, u32[]{:S(2)}, u32[]{:S(2)}) collective-permute-start(bf16[4,2,256,96]{3,2,1,0:T(8,128)(2,1)S(1)} %copy.61.mine_ref), channel_id=1, source_target_pairs={{0,1},{1,0},{2,3},{3,2},{4,5},{5,4},{6,7},{7,6},{8,9},{9,8},{10,11... | collective-permute-start | bytes 1179656 | tf_op jit(solution)/shard_map/ppermute | solution.py:700
  112.7 14.4 %copy-start.7 = (bf16[512,256]{1,0:T(8,128)(2,1)S(1)}, bf16[512,256]{1,0:T(8,128)(2,1)}, u32[]{:S(2)}) copy-start(bf16[512,256]{1,0:T(8,128)(2,1)} %d_own.1) | copy-start | bytes 786436
  112.7 14.5 %copy-start.8 = (bf16[512,256]{1,0:T(8,128)(2,1)S(1)}, bf16[512,256]{1,0:T(8,128)(2,1)}, u32[]{:S(2)}) copy-start(bf16[512,256]{1,0:T(8,128)(2,1)} %l_own.1) | copy-start | bytes 786436
  113.5 0.8 copy-start.6
  123.7 17.5 %copy-start.2 = (bf16[4,512,128]{2,1,0:T(8,128)(2,1)}, bf16[4,512,128]{2,1,0:T(8,128)(2,1)S(1)}, u32[]{:S(2)}) copy-start(bf16[4,512,128]{2,1,0:T(8,128)(2,1)S(1)} %all-to-all-done.3.d_ref) | copy-start | bytes 1572868
  123.7 17.5 %all-to-all-start.5 = ((bf16[4,512,128]{2,1,0:T(8,128)(2,1)}), bf16[4,512,128]{2,1,0:T(8,128)(2,1)S(1)}, u32[]{:S(2)}, u32[]{:S(2)}) async-start(bf16[4,512,128]{2,1,0:T(8,128)(2,1)} %latent_mix.1), calls=%async_computation.5 | async-start | bytes 1048576 | tf_op jit(solution)/shard_map/all_to_all | solution.py:697
  127.1 9.2 %collective-permute-start.2 = (bf16[512,256]{1,0:T(8,128)(2,1)S(1)}, bf16[512,256]{1,0:T(8,128)(2,1)S(1)}, u32[]{:S(2)}, u32[]{:S(2)}) collective-permute-start(bf16[512,256]{1,0:T(8,128)(2,1)S(1)} %copy-done.7), channel_id=1, source_target_pairs={{0,2},{2,0},{1,3},{3,1},{4,6},{6,4},{5,7},{7,5},{8,10},{10,8},{9,1... | collective-permute-start | bytes 786440 | tf_op jit(solution)/shard_map/ppermute | solution.py:700
  127.2 12.9 %collective-permute-start.3 = (bf16[512,256]{1,0:T(8,128)(2,1)S(1)}, bf16[512,256]{1,0:T(8,128)(2,1)S(1)}, u32[]{:S(2)}, u32[]{:S(2)}) collective-permute-start(bf16[512,256]{1,0:T(8,128)(2,1)S(1)} %copy-done.8), channel_id=1, source_target_pairs={{0,2},{2,0},{1,3},{3,1},{4,6},{6,4},{5,7},{7,5},{8,10},{10,8},{9,1... | collective-permute-start | bytes 786440 | tf_op jit(solution)/shard_map/ppermute | solution.py:700
  136.4 4.8 %copy-start.9 = (bf16[512,256]{1,0:T(8,128)(2,1)}, bf16[512,256]{1,0:T(8,128)(2,1)S(1)}, u32[]{:S(2)}) copy-start(bf16[512,256]{1,0:T(8,128)(2,1)S(1)} %collective-permute-done.2.d_other) | copy-start | bytes 786436
  140.1 1.0 copy-start.10
  141.2 0.8 copy-start.3
  145.0 18.9 %copy-start.11 = (f32[1024]{0:T(1024)S(1)}, f32[1024]{0:T(1024)}, u32[]{:S(2)}) copy-start(f32[1024]{0:T(1024)} %param.37) | copy-start | bytes 12292
  145.0 1.7 %collective-permute-start.4 = (bf16[4,128,256]{2,1,0:T(8,128)(2,1)}, bf16[4,128,256]{2,1,0:T(8,128)(2,1)S(1)}, u32[]{:S(2)}, u32[]{:S(2)}) collective-permute-start(bf16[4,128,256]{2,1,0:T(8,128)(2,1)} %get-tuple-element.16), channel_id=1, source_target_pairs={{0,1},{1,0},{2,3},{3,2},{4,5},{5,4},{6,7},{7,6},{8,9},{9,8},{10,11... | collective-permute-start | bytes 786440 | tf_op jit(solution)/shard_map/ppermute | solution.py:700
  148.5 13.6 %all-to-all-start.6 = ((bf16[4,128,256]{2,1,0:T(8,128)(2,1)}), bf16[4,128,256]{2,1,0:T(8,128)(2,1)S(1)}, u32[]{:S(2)}, u32[]{:S(2)}) async-start(bf16[4,128,256]{2,1,0:T(8,128)(2,1)} %add_convert_fusion), calls=%async_computation.6 | async-start | bytes 524288 | tf_op jit(solution)/shard_map/all_to_all | solution.py:697
  162.1 1.7 %collective-permute-start.5 = (bf16[2,128,256]{2,1,0:T(8,128)(2,1)S(1)}, bf16[2,128,256]{2,1,0:T(8,128)(2,1)S(1)}, u32[]{:S(2)}, u32[]{:S(2)}) collective-permute-start(bf16[2,128,256]{2,1,0:T(8,128)(2,1)S(1)} %constant_dynamic-slice_fusion), channel_id=1, source_target_pairs={{0,1},{1,0},{2,3},{3,2},{4,5},{5,4},{6,7},{7,6},{8,9},{9,8},{10,11... | collective-permute-start | bytes 393224 | tf_op jit(solution)/shard_map/ppermute | solution.py:700
  162.3 1.4 collective-permute-start.6

commit v2 on v1

--- a/solution.py
+++ b/solution.py
@@ -2,6 +2,7 @@
 
 import jax
 import jax.numpy as jnp
+import numpy as np
 from jax import lax
 from jax.experimental import pallas as pl
 from jax.experimental.pallas import tpu as pltpu
@@ -364,11 +365,8 @@
     )
 
 
-def kernel_call(body, out_shapes, args, scratch=(), scalars=1, name=None):
-    specs = [
-        pl.BlockSpec(memory_space=pltpu.SMEM if i < scalars else pltpu.VMEM)
-        for i in range(len(args))
-    ]
+def kernel_call(body, out_shapes, args, scratch=(), name=None):
+    specs = [pl.BlockSpec(memory_space=pltpu.VMEM) for _ in args]
     return pl.pallas_call(
         body,
         out_shape=out_shapes,
@@ -380,15 +378,16 @@
     )(*args)
 
 
-def outgoing_weights(ids, mixers, lats, sp_size):
+def outgoing_weights(mixers, lats, sp_size):
     half = mixers[0].shape[0] // 2
     per_mixer = mixers[0].shape[1] // sp_size
     per_lat = [w.shape[1] // sp_size // 2 for w in lats]
     columns = len(mixers) * per_mixer + sum(per_lat)
-
-    def body(ids_ref, *refs):
-        rows = pl.ds(pl.multiple_of(ids_ref[2] * half, half), half)
-        first = ids_ref[3] == 0
+    padded = -(-columns // 128) * 128
+
+    def body(*refs):
+        rows = pl.ds(pl.multiple_of(lax.axis_index("grp") * half, half), half)
+        first = lax.axis_index("tp") == 0
         out_ref = refs[-1]
         for s in range(sp_size):
             begin = 0
@@ -397,79 +396,132 @@
                     rows, s * per_mixer : (s + 1) * per_mixer
                 ]
                 begin += per_mixer
+            rest = []
             for ref, per in zip(refs[len(mixers) : -1], per_lat):
                 pair = ref[rows, 2 * s * per : 2 * (s + 1) * per]
-                out_ref[s, :, begin : begin + per] = jnp.where(first, pair[:, :per], pair[:, per:])
-                begin += per
+                rest.append(jnp.where(first, pair[:, :per], pair[:, per:]))
+            rest.append(jnp.zeros((half, padded - columns), jnp.bfloat16))
+            out_ref[s, :, begin:] = jnp.concatenate(rest, axis=1)
 
     return kernel_call(
         body,
-        jax.ShapeDtypeStruct((sp_size, half, columns), jnp.bfloat16),
-        (ids, *mixers, *lats),
+        jax.ShapeDtypeStruct((sp_size, half, padded), jnp.bfloat16),
+        (*mixers, *lats),
         name="outgoing_weights",
     )
 
 
-def outgoing_tokens(ids, tokens, gain, sp_size):
+def outgoing_tokens(tokens, gain, sp_size):
     rows, width = tokens.shape
     block = width // (sp_size * 4)
 
-    def body(ids_ref, token_ref, gain_ref, out_ref):
+    def body(token_ref, gain_ref, mine_ref, their_ref):
         values = token_ref[...].astype(jnp.float32)
         normed = (values * rms_scale(values) * gain_ref[...]).astype(jnp.bfloat16)
-        first = ids_ref[3] == 0
+        first = lax.axis_index("tp") == 0
         for f in range(2):
             for s in range(sp_size):
                 begin = (s * 2 + f) * 2 * block
-                piece = jnp.where(
-                    first,
-                    normed[:, begin : begin + block],
-                    normed[:, begin + block : begin + 2 * block],
+                low = normed[:, begin : begin + block]
+                high = normed[:, begin + block : begin + 2 * block]
+                at = (f * sp_size + s) * block
+                mine_ref[:, at : at + block] = jnp.where(first, low, high)
+                their_ref[:, at : at + block] = jnp.where(first, high, low)
+
+    shape = jax.ShapeDtypeStruct((rows, width // 2), jnp.bfloat16)
+    return kernel_call(body, (shape, shape), (tokens, gain), name="outgoing_tokens")
+
+
+def project(mine, theirs, blocks, extra, sizes):
+    seq_count, token_count, fine, q_cols, kv_cols = sizes
+    sp_size = len(mine)
+    span = sp_size * token_count
+    rows = seq_count * span
+    part = mine[0].shape[1]
+    middle = part // 2
+    extra_width = extra.shape[1]
+    q_stack, kv_stack = 128 // q_cols, 128 // kv_cols
+    packed = rows // q_stack + rows // kv_stack
+    lat_width = q_cols + kv_cols
+
+    def body(*refs):
+        mine_refs, refs = refs[:sp_size], refs[sp_size:]
+        their_refs, refs = refs[:sp_size], refs[sp_size:]
+        block_refs, extra_ref, fine_ref, pack_ref, ext_ref, lat_ref = refs[:5], *refs[5:]
+        place, fs_at = lax.axis_index("sp"), lax.axis_index("fs")
+        tp_at = lax.axis_index("tp")
+        straight = tp_at == lax.axis_index("grp")
+
+        def lanes(fs_from):
+            return pl.ds(pl.multiple_of(fs_from * middle, middle), middle)
+
+        for o in range(sp_size):
+            def half_of(same_grp, same_fs):
+                at = lanes(fs_at if same_fs else 1 - fs_at)
+                one, two = mine_refs[o][:, at], their_refs[o][:, at]
+                if not same_grp:
+                    one, two = two, one
+                return jnp.where(straight, one, two)
+
+            far = half_of(False, False)
+            cut = block_refs[3].shape[0]
+            value = (
+                dot32(half_of(True, True), block_refs[0][...])
+                + dot32(half_of(True, False), block_refs[1][...])
+                + dot32(half_of(False, True), block_refs[2][...])
+                + dot32(far[:, :cut], block_refs[3][...])
+                + dot32(far[:, cut:], block_refs[4][...])
+            ).astype(jnp.bfloat16)
+            mine_at = pl.ds(pl.multiple_of(tp_at * part, part), part)
+            their_at = pl.ds(pl.multiple_of((1 - tp_at) * part, part), part)
+            outer = dot32(mine_refs[o][...], extra_ref[mine_at, :])
+            outer = outer + dot32(their_refs[o][...], extra_ref[their_at, :])
+            source = lax.rem(place + o, sp_size)
+            for n in range(seq_count):
+                of = slice(n * token_count, (n + 1) * token_count)
+                at = pl.ds(pl.multiple_of(source * token_count, token_count), token_count)
+                fine_ref[n, at, :] = value[of, :fine]
+                ext_ref[n, at, :] = outer[of]
+                at = pl.ds(
+                    pl.multiple_of(n * span + source * token_count, token_count), token_count
                 )
-                at = (f * sp_size + s) * block
-                for n in range(sp_size):
-                    out_ref[n, :, at : at + block] = piece
-
-    return kernel_call(
-        body,
-        jax.ShapeDtypeStruct((sp_size, rows, width // 2), jnp.bfloat16),
-        (ids, tokens, gain),
-        name="outgoing_tokens",
-    )
-
-
-def project(ids, mine, theirs, weights, extra, sizes):
-    seq_count, token_count, fine, q_cols, kv_cols = sizes
-    sp_size, rows, part = mine.shape
-    span = sp_size * token_count
-    extra_width = extra.shape[1]
-
-    def body(ids_ref, mine_ref, their_ref, weight_ref, extra_ref, fine_ref, lat_ref, ext_ref):
-        mine_at = pl.ds(pl.multiple_of(ids_ref[3] * part, part), part)
-        their_at = pl.ds(pl.multiple_of((1 - ids_ref[3]) * part, part), part)
-        for s in range(sp_size):
-            value = dot32(mine_ref[s], weight_ref[mine_at, :])
-            value = (value + dot32(their_ref[s], weight_ref[their_at, :])).astype(jnp.bfloat16)
-            outer = dot32(mine_ref[s], extra_ref[mine_at, :])
-            outer = outer + dot32(their_ref[s], extra_ref[their_at, :])
-            for n in range(seq_count):
-                cut = slice(n * token_count, (n + 1) * token_count)
-                at = slice(s * token_count, (s + 1) * token_count)
-                fine_ref[n, at, :] = value[cut, :fine]
-                ext_ref[n, at, :] = outer[cut]
-                for j in range(sp_size):
-                    lat_ref[j, n, at, :] = value[cut, fine:]
+                lat_ref[at, :] = value[of, fine : fine + 128]
+        group = rows // q_stack
+        for base, first, width, count in (
+            (0, 0, q_cols, q_stack),
+            (rows // q_stack, q_cols, kv_cols, kv_stack),
+        ):
+            group = rows // count
+            joined = jnp.concatenate(
+                [
+                    lat_ref[k * group : (k + 1) * group, first : first + width]
+                    for k in range(count)
+                ],
+                axis=1,
+            )
+            for j in range(sp_size):
+                pack_ref[j, base : base + group, :] = joined
 
     return kernel_call(
         body,
         (
             jax.ShapeDtypeStruct((seq_count, span, fine), jnp.bfloat16),
-            jax.ShapeDtypeStruct((sp_size, seq_count, span, q_cols + kv_cols), jnp.bfloat16),
+            jax.ShapeDtypeStruct((sp_size, packed, 128), jnp.bfloat16),
             jax.ShapeDtypeStruct((seq_count, span, extra_width), jnp.float32),
         ),
-        (ids, mine, theirs, weights, extra),
+        (*mine, *theirs, *blocks, extra),
+        scratch=(pltpu.VMEM((rows, 128), jnp.bfloat16),),
         name="project",
     )
+
+
+def send_by_pair(out_refs, pieces, sp_size, token_count):
+    place = lax.axis_index("sp")
+    for step, out_ref in enumerate(out_refs):
+        second = lax.rem(place + step, sp_size) >= sp_size // 2
+        for n, (low, high) in enumerate(pieces):
+            rows = low.shape[0]
+            out_ref[n * rows : (n + 1) * rows, :] = jnp.where(second, high, low)
 
 
 def lower_inverses(lowers, base):
@@ -493,7 +545,7 @@
     return inverses
 
 
-def delta_mix(scalars, fine, ext, gain, rates, gate_at, heads, copies):
+def delta_mix(fine, ext, gain, rates, gate_at, heads, sp_size):
     seq_count, span, _ = fine.shape
     tile = math.gcd(span, 128)
     tiles = span // tile
@@ -515,7 +567,8 @@
         scores = fine_dot(query, key, dot_t) * decay
         return lower, scores, value * beta
 
-    def body(ids_ref, fine_ref, ext_ref, gain_ref, rate_ref, out_ref):
+    def body(fine_ref, ext_ref, gain_ref, rate_ref, *out_refs):
+        first_head = (lax.axis_index("tp") * sp_size + lax.axis_index("sp")) * heads
         lane = lax.broadcasted_iota(jnp.int32, (span, ext.shape[2]), 1)
         rate_lane = lax.broadcasted_iota(jnp.int32, (1, gates), 1)
         chains = []
@@ -527,7 +580,7 @@
                     )
                     for k in range(3)
                 ]
-                head = ids_ref[4] + h
+                head = first_head + h
                 outer = ext_ref[n]
                 beta_pre, decay_pre = (
                     jnp.sum(
@@ -552,39 +605,55 @@
                         lower[cut, : j * tile], jnp.concatenate(solved[i], axis=0)
                     )
                 solved[i].append(fine_dot(inverses[i * tiles + j], rest))
+        pieces = []
         for i, (_, scores, _) in enumerate(chains):
-            n, h = divmod(i, heads)
             out = fine_dot(scores, jnp.concatenate(solved[i], axis=0))
             out = (out * rms_scale(out) * gain_ref[...]).astype(jnp.bfloat16)
-            for j in range(copies):
-                out_ref[j, n * span : (n + 1) * span, h * HEAD : (h + 1) * HEAD] = out
-
+            pieces.append((out[: span // 2], out[span // 2 :]))
+        for h in range(heads):
+            columns = slice(h * HEAD, (h + 1) * HEAD)
+            views = [ref.at[:, columns] for ref in out_refs] if heads > 1 else out_refs
+            send_by_pair(views, pieces[h::heads], sp_size, span // sp_size)
+
+    shape = jax.ShapeDtypeStruct((seq_count * span // 2, heads * HEAD), jnp.bfloat16)
     return kernel_call(
-        body,
-        jax.ShapeDtypeStruct((copies, seq_count * span, heads * HEAD), jnp.bfloat16),
-        (scalars, fine, ext, gain, rates),
-        name="delta_mix",
-    )
-
-
-def latent_mix(ids, mine, theirs, ext, tables, gains, ups, q_cols, heads):
-    sp_size, seq_count, span, _ = mine.shape
+        body, (shape,) * sp_size, (fine, ext, gain, rates), name="delta_mix"
+    )
+
+
+def latent_mix(mine, theirs, ext, tables, gains, ups, q_cols, kv_cols, heads):
+    sp_size = mine.shape[0]
+    seq_count, span, _ = ext.shape
+    rows = seq_count * span
     scale = (NOPE + ROPE) ** (-0.5)
 
-    def body(ids_ref, mine_ref, their_ref, ext_ref, cos_ref, sin_ref, *refs):
-        qg_ref, kg_ref, qup_ref, kup_ref, out_ref = refs
-        first = ids_ref[3] == 0
+    def unpack(value, n, base, width):
+        group = rows * width // 128
+        pieces = []
+        for k in range(128 // width):
+            if n * span < (k + 1) * group and k * group < (n + 1) * span:
+                low = max(n * span - k * group, 0)
+                high = min((n + 1) * span - k * group, group)
+                pieces.append(
+                    value[base + low : base + high, k * width : (k + 1) * width]
+                )
+        return jnp.concatenate(pieces, axis=0) if len(pieces) > 1 else pieces[0]
+
+    def body(mine_ref, their_ref, ext_ref, cos_ref, sin_ref, *refs):
+        qg_ref, kg_ref, qup_ref, kup_ref, *out_refs = refs
+        first = lax.axis_index("tp") == 0
         row = lax.broadcasted_iota(jnp.int32, (span, span), 0) // BLOCK
         col = lax.broadcasted_iota(jnp.int32, (span, span), 1) // BLOCK
         allowed = col <= row
         cosine, sine = cos_ref[...], sin_ref[...]
+        pairs = []
+        for s in range(sp_size):
+            own, other = mine_ref[s], their_ref[s]
+            pairs += [jnp.where(first, own, other), jnp.where(first, other, own)]
+        joins = []
         for n in range(seq_count):
-            q_parts, kv_parts = [], []
-            for s in range(sp_size):
-                own, other = mine_ref[s, n], their_ref[s, n]
-                pair = (jnp.where(first, own, other), jnp.where(first, other, own))
-                q_parts += [p[:, :q_cols] for p in pair]
-                kv_parts += [p[:, q_cols:] for p in pair]
+            q_parts = [unpack(p, n, 0, q_cols) for p in pairs]
+            kv_parts = [unpack(p, n, rows * q_cols // 128, kv_cols) for p in pairs]
             q_lat = jnp.concatenate(q_parts, axis=1).astype(jnp.float32)
             kv_lat = jnp.concatenate(kv_parts, axis=1).astype(jnp.float32)
             q_norm = (q_lat * rms_scale(q_lat) * qg_ref[...]).astype(jnp.bfloat16)
@@ -613,50 +682,83 @@
                 total = jnp.sum(weights, axis=-1, keepdims=True)
                 results.append(dot32(weights.astype(jnp.bfloat16), values) / total)
             joined = jnp.concatenate(results, axis=1).astype(jnp.bfloat16)
-            for j in range(sp_size):
-                out_ref[j, n * span : (n + 1) * span, :] = joined
-
+            joins.append((joined[: span // 2], joined[span // 2 :]))
+        send_by_pair(out_refs, joins, sp_size, span // sp_size)
+
+    shape = jax.ShapeDtypeStruct((rows // 2, heads * VDIM), jnp.bfloat16)
     return kernel_call(
         body,
-        jax.ShapeDtypeStruct((sp_size, seq_count * span, heads * VDIM), jnp.bfloat16),
-        (ids, mine, theirs, ext, *tables, *gains, *ups),
+        (shape,) * sp_size,
+        (mine, theirs, ext, *tables, *gains, *ups),
         name="latent_mix",
     )
 
 
-def output_partial(ids, delta_all, latent_all, weights, sizes):
+def output_partial(delta_all, latent_all, near, near_fs, far, far_fs, sizes):
     seq_count, token_count = sizes
-    sp_size, rows, d_width = delta_all.shape
-    l_width = latent_all.shape[2]
-    span = sp_size * token_count
-    d_total, l_total = d_width * sp_size, l_width * sp_size
-    columns = weights[0].shape[1]
-
-    def body(ids_ref, d_ref, l_ref, d_own, d_other, l_own, l_other, keep_ref, pass_ref, lhs_ref):
-        for s in range(sp_size):
-            lhs_ref[:, s * d_width : (s + 1) * d_width] = d_ref[s]
-            lhs_ref[:, d_total + s * l_width : d_total + (s + 1) * l_width] = l_ref[s]
-        own = dot32(lhs_ref[:, :d_total], d_own[...]) + dot32(lhs_ref[:, d_total:], l_own[...])
-        other = dot32(lhs_ref[:, :d_total], d_other[...]) + dot32(
-            lhs_ref[:, d_total:], l_other[...]
-        )
-        own, other = own.astype(jnp.bfloat16), other.astype(jnp.bfloat16)
-        straight = ids_ref[1] == ids_ref[3]
-        keep, onward = jnp.where(straight, own, other), jnp.where(straight, other, own)
-        for n in range(seq_count):
-            for s in range(sp_size):
-                first = n * span + s * token_count
-                at = slice(n * token_count, (n + 1) * token_count)
-                keep_ref[s, at, :] = keep[first : first + token_count]
-                pass_ref[s, at, :] = onward[first : first + token_count]
-
-    shape = jax.ShapeDtypeStruct((sp_size, seq_count * token_count, columns), jnp.bfloat16)
+    sp_size = len(delta_all)
+    rows, d_width = delta_all[0].shape
+    l_width = latent_all[0].shape[1]
+    total, columns = near.shape
+    half = total // 2
+    per_half = sp_size // 2
+
+    def body(*refs):
+        d_refs, refs = refs[:sp_size], refs[sp_size:]
+        l_refs, refs = refs[:sp_size], refs[sp_size:]
+        near_ref, near_fs_ref, far_ref, far_fs_ref, keep_ref, pass_ref, lhs_ref = refs
+        place, fs_at = lax.axis_index("sp"), lax.axis_index("fs")
+        grp_at = lax.axis_index("grp")
+        for o in range(sp_size):
+            source = lax.rem(place + o, sp_size)
+            base = (source // per_half) * half
+            within = lax.rem(source, per_half)
+            at = pl.multiple_of(base + within * d_width, 128)
+            lhs_ref[:, pl.ds(at, d_width)] = d_refs[o][...]
+            at = pl.multiple_of(base + per_half * d_width + within * l_width, 128)
+            lhs_ref[:, pl.ds(at, l_width)] = l_refs[o][...]
+        lhs = lhs_ref[...]
+        own = lhs_ref[:, pl.ds(pl.multiple_of(grp_at * half, half), half)]
+        other = lhs_ref[:, pl.ds(pl.multiple_of((1 - grp_at) * half, half), half)]
+        close = (
+            dot32(lhs, near_ref[...]).astype(jnp.bfloat16),
+            dot32(lhs, near_fs_ref[...]).astype(jnp.bfloat16),
+        )
+        away = tuple(
+            (dot32(own, ref[:half, :]) + dot32(other, ref[half:, :])).astype(jnp.bfloat16)
+            for ref in (far_ref, far_fs_ref)
+        )
+        straight = place // per_half == lax.axis_index("tp")
+        for k in range(2):
+            begin = (1 - fs_at) if k else fs_at
+            at = pl.ds(pl.multiple_of(begin * columns, columns), columns)
+            keep = jnp.where(straight, close[k], away[k])
+            onward = jnp.where(straight, away[k], close[k])
+            pair_rows = 2 * token_count
+            for n in range(seq_count):
+                for p in range(2):
+                    of = slice(n * pair_rows + p * token_count, n * pair_rows + (p + 1) * token_count)
+                    to = slice(n * token_count, (n + 1) * token_count)
+                    keep_ref[p, to, at] = keep[of]
+                    pass_ref[p, to, at] = onward[of]
+
+    shape = jax.ShapeDtypeStruct((2, rows // 2, 2 * columns), jnp.bfloat16)
     return kernel_call(
         body,
         (shape, shape),
-        (ids, delta_all, latent_all, *weights),
-        scratch=(pltpu.VMEM((rows, d_total + l_total), jnp.bfloat16),),
+        (*delta_all, *latent_all, near, near_fs, far, far_fs),
+        scratch=(pltpu.VMEM((rows, total), jnp.bfloat16),),
         name="output_partial",
+    )
+
+
+def whole_tables(length, repeats):
+    frequency = ROPE_THETA ** (-np.arange(0, ROPE, 2, dtype=np.float32) / np.float32(ROPE))
+    angles = np.arange(length, dtype=np.float32)[:, None] * frequency[None, :].astype(np.float32)
+    cosine, sine = np.cos(angles), np.sin(angles)
+    return tuple(
+        jnp.asarray(np.tile(np.concatenate(pair, axis=1), (1, repeats)), jnp.float32)
+        for pair in ((cosine, cosine), (-sine, sine))
     )
 
 
@@ -683,13 +785,10 @@
 ):
     f32, bf16 = jnp.float32, jnp.bfloat16
     sp_size, tp_size = lax.axis_size("sp"), lax.axis_size("tp")
-    place, fs_at = lax.axis_index("sp"), lax.axis_index("fs")
-    grp_at, tp_at = lax.axis_index("grp"), lax.axis_index("tp")
+    place, grp_at = lax.axis_index("sp"), lax.axis_index("grp")
     seq_count, token_count, width = tokens.shape
     rows = seq_count * token_count
     heads = query_weight.shape[1] // HEAD // sp_size
-    first_head = (tp_at * sp_size + place) * heads
-    ids = jnp.stack([place, fs_at, grp_at, tp_at, first_head]).astype(jnp.int32)
     shares = sp_size * tp_size
     q_cols, kv_cols = query_down.shape[1] // shares, latent_down.shape[1] // shares
 
@@ -699,18 +798,41 @@
     def swap(values, axis):
         return lax.ppermute(values, axis, [(0, 1), (1, 0)])
 
-    outgoing = outgoing_weights(
-        ids, (query_weight, key_weight, value_weight), (query_down, latent_down), sp_size
-    )
-    block = exchange(outgoing, "sp")
-    block = jnp.broadcast_to(block.reshape(1, -1, outgoing.shape[2]), (4,) + (block.shape[0] * block.shape[1], outgoing.shape[2]))
-    weights = exchange(block, ("grp", "fs")).reshape(width, outgoing.shape[2])
-
+    def along(values, step):
+        return lax.ppermute(values, "sp", [(i, (i + step) % sp_size) for i in range(sp_size)])
+
+    def from_sp(sends):
+        return [sends[0]] + [along(sends[step], step) for step in range(sp_size - 1, 0, -1)]
+
+    with jax.named_scope("weights_out"):
+        outgoing = outgoing_weights(
+            (query_weight, key_weight, value_weight), (query_down, latent_down), sp_size
+        )
+        block = exchange(outgoing, "sp").reshape(-1, outgoing.shape[2])
     token_rows, outgoing = lax.optimization_barrier((tokens.reshape(rows, width), outgoing))
-    mine = exchange(outgoing_tokens(ids, token_rows, pre_gain[None, :], sp_size), "sp")
-    theirs = swap(mine, "tp")
-
-    delta_other, latent_other = swap(delta_out, "fs"), swap(latent_out, "fs")
+
+    quarter = delta_out.shape[0] // 2
+    near = jnp.concatenate(
+        [w[k * quarter : (k + 1) * quarter] for k in range(2) for w in (delta_out, latent_out)]
+    )
+    with jax.named_scope("near_out"):
+        near_fs = swap(near, "fs")
+
+    own_half, other_half = outgoing_tokens(token_rows, pre_gain[None, :], sp_size)
+    with jax.named_scope("tokens_out"):
+        mine = from_sp([own_half] * sp_size)
+    theirs = [other_half] + [swap(piece, "tp") for piece in mine[1:]]
+
+    with jax.named_scope("far_out"):
+        far_half = lax.dynamic_slice_in_dim(near, grp_at * 2 * quarter, 2 * quarter, 0)
+        far_half = along(far_half, sp_size // 2)
+
+    middle = block.shape[0] // 2
+    by_fs, by_grp = swap(block, "fs"), swap(block, "grp")
+    blocks = (block, by_fs, by_grp, swap(by_grp[:middle], "fs"), swap(by_fs[middle:], "grp"))
+
+    far = jnp.concatenate([far_half, swap(far_half, "grp")])
+    far_fs = swap(far, "fs")
 
     gate_at = rope_weight.shape[1]
     filler = -(gate_at + 2 * beta_weight.shape[1]) % 128
@@ -719,22 +841,6 @@
     )
     extra = extra.reshape(sp_size, 2, 2, width // (4 * sp_size), extra.shape[1])
     extra = jnp.transpose(extra, (2, 1, 0, 3, 4)).reshape(width, extra.shape[4])
-
-    fine, lat, ext = project(
-        ids,
-        mine,
-        theirs,
-        weights,
-        extra,
-        (seq_count, token_count, 3 * heads * HEAD, q_cols, kv_cols),
-    )
-    lat_mine = exchange(lat, "sp")
-    lat_theirs = swap(lat_mine, "tp")
-
-    delta_heads = delta_mix(
-        ids, fine, ext, delta_gain[None, :], decay_rate[None, :], gate_at, heads, sp_size
-    )
-    delta_all = exchange(delta_heads, "sp")
 
     latent_heads = query_up.shape[1] // (NOPE + ROPE) // sp_size
     up = query_up.reshape(query_up.shape[0], sp_size, latent_heads, NOPE + ROPE)
@@ -746,50 +852,56 @@
     )
     kv_width = latent_up.shape[1] // sp_size
     kv_up = lax.dynamic_slice_in_dim(latent_up, place * kv_width, kv_width, 1)
-    cosine, sine = rope_tables(jnp.arange(sp_size * token_count), ROPE)
-    tables = (
-        jnp.tile(jnp.concatenate([cosine, cosine], axis=1), (1, latent_heads)),
-        jnp.tile(jnp.concatenate([-sine, sine], axis=1), (1, latent_heads)),
-    )
-    latent = latent_mix(
-        ids,
-        lat_mine,
-        lat_theirs,
-        ext,
-        tables,
-        (query_gain[None, :], latent_gain[None, :]),
-        (q_up, kv_up),
-        q_cols,
-        latent_heads,
-    )
-    latent_all = exchange(latent, "sp")
+    tables = whole_tables(sp_size * token_count, latent_heads)
+    mine[1], extra, q_up, kv_up, far_half = lax.optimization_barrier(
+        (mine[1], extra, q_up, kv_up, far_half)
+    )
+
+    fine, lat, ext = project(
+        mine, theirs, blocks, extra, (seq_count, token_count, 3 * heads * HEAD, q_cols, kv_cols)
+    )
+    lat_mine = exchange(lat, "sp")
+    lat_theirs = swap(lat_mine, "tp")
+
+    delta_all = from_sp(
+        delta_mix(fine, ext, delta_gain[None, :], decay_rate[None, :], gate_at, heads, sp_size)
+    )
+    latent_all = from_sp(
+        latent_mix(
+            lat_mine,
+            lat_theirs,
+            ext,
+            tables,
+            (query_gain[None, :], latent_gain[None, :]),
+            (q_up, kv_up),
+            q_cols,
+            kv_cols,
+            latent_heads,
+        )
+    )
 
     keep, onward = output_partial(
-        ids,
-        delta_all,
-        latent_all,
-        (delta_out, delta_other, latent_out, latent_other),
-        (seq_count, token_count),
+        delta_all, latent_all, near, near_fs, far, far_fs, (seq_count, token_count)
     )
     mixed = (keep.astype(f32) + swap(onward, "tp").astype(f32)).astype(bf16)
-    landed = exchange(mixed, "sp")
-    per_tp = sp_size // tp_size
-    squares = jnp.sum(landed.astype(f32) * landed.astype(f32), axis=(0, 2))[:, None]
+    side = lax.rem(place, 2)
+    here = pick(mixed, side)
+    there = lax.ppermute(pick(mixed, 1 - side), "sp", [(i, i ^ 1) for i in range(sp_size)])
+    here, there = here.astype(f32), there.astype(f32)
+    squares = jnp.sum(here * here, axis=1, keepdims=True) + jnp.sum(
+        there * there, axis=1, keepdims=True
+    )
     squares = squares + swap(squares, "tp")
-    here = lax.dynamic_slice_in_dim(landed, tp_at * per_tp, per_tp, 0)
-    there = swap(lax.dynamic_slice_in_dim(landed, (1 - tp_at) * per_tp, per_tp, 0), "tp")
-    low, high = jnp.where(tp_at == 0, here, there), jnp.where(tp_at == 0, there, here)
     final = jnp.concatenate(
-        [half[k] for k in range(per_tp) for half in (low, high)], axis=1
-    ).astype(f32)
+        [jnp.where(side == 0, here, there), jnp.where(side == 0, there, here)], axis=1
+    )
     result = final * lax.rsqrt(squares / D + NORM_EPS) * post_gain
     return result.astype(bf16).reshape(seq_count, token_count, final.shape[1])
 
 
 def fits_whole(mesh):
     shape = mesh.shape
-    pairs = all(shape[name] == 2 for name in ("grp", "fs", "tp"))
-    return pairs and shape["sp"] % shape["tp"] == 0
+    return all(shape[name] == 2 for name in ("grp", "fs", "tp")) and shape["sp"] == 4
 
 
 def solution(mesh):

time: 166 us -> 126 us (0.76)
  waiting for transfers between devices: 83.9 us -> 41.9 us
  starting transfers between devices: 31.2 us -> 44.3 us
  local copies, waits for them, and re-layouts: 20 us -> 11.6 us
  other arithmetic: 5.59 us -> 3.38 us
    all_to_all x7 -> x2, waiting for transfers between devices: 70.5 us -> 8.06 us  [exchange(): return lax.all_to_all(values, axis, 0, 0, tiled=True)]
    ppermute x0 -> x11, starting transfers between devices: none -> 24 us  [the longest x10 23.9 us: along(): lax.ppermute(values, 'sp', [(i, (i + step) % sp_size) for i in range(sp_s...]
    ppermute x0 -> x11, waiting for transfers between devices: none -> 22.8 us  [the longest x10 17.3 us: along(): lax.ppermute(values, 'sp', [(i, (i + step) % sp_size) for i in range(sp_s...]
    all_to_all x7 -> x2, starting transfers between devices: 28.4 us -> 9.94 us  [exchange(): return lax.all_to_all(values, axis, 0, 0, tiled=True)]
    ppermute x7 -> x13, starting transfers between devices: 2.78 us -> 10.4 us  [swap(): return lax.ppermute(values, axis, [(0, 1), (1, 0)])]
    pallas_call x2 -> x0, local copies, waits for them, and re-layouts: 4.1 us -> none  [kernel_call(): pl.pallas_call(body, out_shape=out_shapes, in_specs=specs, out_specs=jax....]
    all_to_all x2 -> x0, local copies, waits for them, and re-layouts: 2.64 us -> none  [exchange(): return lax.all_to_all(values, axis, 0, 0, tiled=True)]
    slice x2 -> x3, local copies, waits for them, and re-layouts: 0.02 us -> 2.55 us  [the longest x1 1.69 us: whole_sequences(): by_grp[:middle]]
  transfers between devices with their start and end apart: 14 -> 26, of which waited for: 11 -> 11; matrix products, arithmetic and copies ran while one was open for 9% -> 7% of each run, Pallas kernels for 8% -> 10%
where the time goes in v2:
time: 126 us; the launch traced here: 125 us
  starting transfers between devices  44.3 us (35%)
  waiting for transfers between devices  41.9 us (33%)
  Pallas kernels  23.8 us (19%)
  local copies, waits for them, and re-layouts  11.6 us (9%)
  other arithmetic  3.38 us (3%)
    ppermute x10, starting transfers between devices, along(): lax.ppermute(values, 'sp', [(i, (i + step) % sp_size) for i in range(sp_s...  23.9 us
    pallas_call x6, Pallas kernels, kernel_call(): pl.pallas_call(body, out_shape=out_shapes, in_specs=specs, out_specs=jax....  23.8 us
    ppermute x10, waiting for transfers between devices, along(): lax.ppermute(values, 'sp', [(i, (i + step) % sp_size) for i in range(sp_s...  17.3 us
    ppermute x13, waiting for transfers between devices, swap(): return lax.ppermute(values, axis, [(0, 1), (1, 0)])  11 us
    ppermute x13, starting transfers between devices, swap(): return lax.ppermute(values, axis, [(0, 1), (1, 0)])  10.4 us
    all_to_all x2, starting transfers between devices, exchange(): return lax.all_to_all(values, axis, 0, 0, tiled=True)  9.94 us
    all_to_all x2, waiting for transfers between devices, exchange(): return lax.all_to_all(values, axis, 0, 0, tiled=True)  8.06 us
    ppermute x1, waiting for transfers between devices, whole_sequences(): lax.ppermute(pick(mixed, 1 - side), 'sp', [(i, i ^ 1) for i in range(sp_s...  5.52 us
  transfers between devices with their start and end apart: 26, of which 11 were waited for; matrix products, arithmetic and copies ran while one was open for 7% of the time, Pallas kernels for 10%

profile of v2, /device:TPU:0, one launch (start us, length us, event | category | flops | bytes accessed | tf_op | source)
XLA Modules:
  0.0 125.3 jit_solution(16637392704903299866)
XLA Ops:
  0.0 2.4 %outgoing_weights.1 = bf16[4,128,512]{2,1,0:T(8,128)(2,1)} custom-call(bf16[256,512]{1,0:T(8,128)(2,1)} %refs_0_.1, bf16[256,512]{1,0:T(8,128)(2,1)} %refs_1_.1, bf16[256,512]{1,0:T(8,128)(2,1)} %refs_2_.1, bf16[256,512]{1,0:T(8,128)(2,1)} %refs_3_.1, bf16[256,256]{1,0:T(8,128)(2,1)} %refs_4_.1), custom_call_target="tpu_custom_call" | custom-call | tf_op jit(solution)/shard_map/weights_out/outgoing_weights/pallas_call | solution.py:370
  2.4 6.3 %all-to-all-start = ((bf16[4,128,512]{2,1,0:T(8,128)(2,1)}), bf16[4,128,512]{2,1,0:T(8,128)(2,1)S(1)}, u32[]{:S(2)}, u32[]{:S(2)}) async-start(bf16[4,128,512]{2,1,0:T(8,128)(2,1)} %outgoing_weights.1), calls=%async_computation | async-start | bytes 1048576 | tf_op jit(solution)/shard_map/weights_out/all_to_all | solution.py:796
  8.7 2.2 %outgoing_tokens.1 = (bf16[128,1024]{1,0:T(8,128)(2,1)}, bf16[128,1024]{1,0:T(8,128)(2,1)}) custom-call(bf16[128,2048]{1,0:T(8,128)(2,1)} %bitcast.38, f32[1,2048]{1,0:T(1,128)} %bitcast.40), custom_call_target="tpu_custom_call" | custom-call | tf_op jit(solution)/shard_map/outgoing_tokens/pallas_call | solution.py:370
  10.9 3.8 %collective-permute-start = (bf16[128,1024]{1,0:T(8,128)(2,1)}, bf16[128,1024]{1,0:T(8,128)(2,1)}, u32[]{:S(2)}, u32[]{:S(2)}) collective-permute-start(bf16[128,1024]{1,0:T(8,128)(2,1)} %get-tuple-element.26.refs_0_), channel_id=1, source_target_pairs={{0,12},{4,0},{8,4},{12,8},{1,13},{5,1},{9,5},{13,9},{2,14},{6,2},{... | collective-permute-start | bytes 786440 | tf_op jit(solution)/shard_map/tokens_out/ppermute | solution.py:802
  14.8 1.1 collective-permute-start.3
  17.3 0.5 maximum_maximum_fusion
  18.4 5.8 %all-to-all-done = bf16[4,128,512]{2,1,0:T(8,128)(2,1)S(1)} async-done(((bf16[4,128,512]{2,1,0:T(8,128)(2,1)}), bf16[4,128,512]{2,1,0:T(8,128)(2,1)S(1)}, u32[]{:S(2)}, u32[]{:S(2)}) %all-to-all-start) | async-done | bytes 524320 | tf_op jit(solution)/shard_map/weights_out/all_to_all | solution.py:796
  24.2 1.5 %collective-permute-start.7 = (bf16[512,512]{1,0:T(8,128)(2,1)S(1)}, bf16[512,512]{1,0:T(8,128)(2,1)S(1)}, u32[]{:S(2)}, u32[]{:S(2)}) collective-permute-start(bf16[512,512]{1,0:T(8,128)(2,1)S(1)} %bitcast.28), channel_id=1, source_target_pairs={{0,2},{2,0},{1,3},{3,1},{4,6},{6,4},{5,7},{7,5},{8,10},{10,8},{9,1... | collective-permute-start | bytes 1572872 | tf_op jit(solution)/shard_map/ppermute | solution.py:799
  25.7 1.5 %collective-permute-start.8 = (bf16[512,512]{1,0:T(8,128)(2,1)S(1)}, bf16[512,512]{1,0:T(8,128)(2,1)}, u32[]{:S(2)}, u32[]{:S(2)}) collective-permute-start(bf16[512,512]{1,0:T(8,128)(2,1)S(1)} %bitcast.29), channel_id=1, source_target_pairs={{0,16},{16,0},{1,17},{17,1},{2,18},{18,2},{3,19},{19,3},{4,20},{20... | collective-permute-start | bytes 1572872 | tf_op jit(solution)/shard_map/ppermute | solution.py:799
  27.3 1.6 %copy.29 = bf16[512,768]{0,1:T(8,128)(2,1)S(1)} copy(bf16[512,768]{1,0:T(8,128)(2,1)} %param.35) | data formatting | bytes 1572864 | tf_op args[14]
  28.9 11.8 %collective-permute-start.1 = (bf16[512,256]{1,0:T(8,128)(2,1)S(1)}, bf16[512,256]{1,0:T(8,128)(2,1)S(1)}, u32[]{:S(2)}, u32[]{:S(2)}) collective-permute-start(bf16[512,256]{1,0:T(8,128)(2,1)S(1)} %constant_dynamic-slice_fusion), channel_id=1, source_target_pairs={{0,8},{4,12},{8,0},{12,4},{1,9},{5,13},{9,1},{13,5},{2,10},{6,14},... | collective-permute-start | bytes 786440 | tf_op jit(solution)/shard_map/far_out/ppermute | solution.py:802
  40.7 11.6 %collective-permute-done.2.refs_2_ = bf16[128,1024]{1,0:T(8,128)(2,1)} collective-permute-done((bf16[128,1024]{1,0:T(8,128)(2,1)}, bf16[128,1024]{1,0:T(8,128)(2,1)}, u32[]{:S(2)}, u32[]{:S(2)}) %collective-permute-start.2) | collective-permute-done | bytes 262176 | tf_op jit(solution)/shard_map/tokens_out/ppermute | solution.py:802
  53.0 0.8 slice.47
  53.8 1.5 %collective-permute-start.10 = (bf16[256,512]{1,0:T(8,128)(2,1)}, bf16[256,512]{1,0:T(8,128)(2,1)}, u32[]{:S(2)}, u32[]{:S(2)}) collective-permute-start(bf16[256,512]{1,0:T(8,128)(2,1)} %slice.47), channel_id=1, source_target_pairs={{0,16},{16,0},{1,17},{17,1},{2,18},{18,2},{3,19},{19,3},{4,20},{20... | collective-permute-start | bytes 786440 | tf_op jit(solution)/shard_map/ppermute | solution.py:799
  55.3 1.7 %slice.46 = bf16[256,512]{1,0:T(8,128)(2,1)} slice(bf16[512,512]{1,0:T(8,128)(2,1)} %collective-permute-done.8.refs_10_), slice={[0:256], [0:512]} | slice | bytes 524288 | tf_op jit(solution)/shard_map/slice | solution.py:832
  57.0 1.6 %collective-permute-start.9 = (bf16[256,512]{1,0:T(8,128)(2,1)}, bf16[256,512]{1,0:T(8,128)(2,1)S(1)}, u32[]{:S(2)}, u32[]{:S(2)}) collective-permute-start(bf16[256,512]{1,0:T(8,128)(2,1)} %slice.46), channel_id=1, source_target_pairs={{0,2},{2,0},{1,3},{3,1},{4,6},{6,4},{5,7},{7,5},{8,10},{10,8},{9,1... | collective-permute-start | bytes 786440 | tf_op jit(solution)/shard_map/ppermute | solution.py:799
  58.8 0.8 slice-done
  59.7 0.7 slice-done.1
  60.5 0.8 copy.28
  61.3 0.7 constant_dynamic-slice_fusion.1.refs_3_
  62.0 0.8 pad_maximum_fusion.1.refs_2_
  62.9 2.7 %collective-permute-done.9.refs_11_ = bf16[256,512]{1,0:T(8,128)(2,1)S(1)} collective-permute-done((bf16[256,512]{1,0:T(8,128)(2,1)}, bf16[256,512]{1,0:T(8,128)(2,1)S(1)}, u32[]{:S(2)}, u32[]{:S(2)}) %collective-permute-start.9) | collective-permute-done | bytes 262176 | tf_op jit(solution)/shard_map/ppermute | solution.py:799
  65.6 0.7 copy-done.13
  66.3 5.0 %project.1 = (bf16[2,256,384]{2,1,0:T(8,128)(2,1)}, bf16[4,384,128]{2,1,0:T(8,128)(2,1)}, f32[2,256,128]{2,1,0:T(8,128)}) custom-call(bf16[128,1024]{1,0:T(8,128)(2,1)} %get-tuple-element.26.refs_0_, bf16[128,1024]{1,0:T(8,128)(2,1)} %collective-permute-done.refs_1_, bf16[128,1024]{1,0:T(8,128)(2,1)} %collective-permute-done.2.refs_2_, ...), custom_call_target="tpu_custom_call" | custom-call | tf_op jit(solution)/shard_map/project/pallas_call | solution.py:370
  71.3 3.6 %all-to-all-start.1 = ((bf16[4,384,128]{2,1,0:T(8,128)(2,1)}), bf16[4,384,128]{2,1,0:T(8,128)(2,1)S(1)}, u32[]{:S(2)}, u32[]{:S(2)}) async-start(bf16[4,384,128]{2,1,0:T(8,128)(2,1)} %get-tuple-element.36), calls=%async_computation.1 | async-start | bytes 786432 | tf_op jit(solution)/shard_map/all_to_all | solution.py:796
  74.9 0.6 collective-permute-start.19
  75.5 1.5 %collective-permute-start.18 = (bf16[1024,256]{1,0:T(8,128)(2,1)S(1)}, bf16[1024,256]{1,0:T(8,128)(2,1)S(1)}, u32[]{:S(2)}, u32[]{:S(2)}) collective-permute-start(bf16[1024,256]{1,0:T(8,128)(2,1)S(1)} %pad_maximum_fusion.refs_8_), channel_id=1, source_target_pairs={{0,2},{2,0},{1,3},{3,1},{4,6},{6,4},{5,7},{7,5},{8,10},{10,8},{9,1... | collective-permute-start | bytes 1572872 | tf_op jit(solution)/shard_map/near_out/ppermute | solution.py:799
  77.0 5.4 %collective-permute-done.19 = bf16[512,256]{1,0:T(8,128)(2,1)S(1)} collective-permute-done((bf16[512,256]{1,0:T(8,128)(2,1)S(1)}, bf16[512,256]{1,0:T(8,128)(2,1)S(1)}, u32[]{:S(2)}, u32[]{:S(2)}) %collective-permute-start.19) | collective-permute-done | bytes 262176 | tf_op jit(solution)/shard_map/ppermute | solution.py:799
  82.4 1.6 %collective-permute-start.20 = (bf16[1024,256]{1,0:T(8,128)(2,1)S(1)}, bf16[1024,256]{1,0:T(8,128)(2,1)S(1)}, u32[]{:S(2)}, u32[]{:S(2)}) collective-permute-start(bf16[1024,256]{1,0:T(8,128)(2,1)S(1)} %constant_dynamic-update-slice_fusion.refs_10_), channel_id=1, source_target_pairs={{0,2},{2,0},{1,3},{3,1},{4,6},{6,4},{5,7},{7,5},{8,10},{10,8},{9,1... | collective-permute-start | bytes 1572872 | tf_op jit(solution)/shard_map/ppermute | solution.py:799
  84.0 2.2 %all-to-all-done.1.mine_ref = bf16[4,384,128]{2,1,0:T(8,128)(2,1)S(1)} async-done(((bf16[4,384,128]{2,1,0:T(8,128)(2,1)}), bf16[4,384,128]{2,1,0:T(8,128)(2,1)S(1)}, u32[]{:S(2)}, u32[]{:S(2)}) %all-to-all-start.1) | async-done | bytes 393248 | tf_op jit(solution)/shard_map/all_to_all | solution.py:796
  86.2 5.5 %delta_mix.1 = (bf16[256,128]{1,0:T(8,128)(2,1)}, bf16[256,128]{1,0:T(8,128)(2,1)}, bf16[256,128]{1,0:T(8,128)(2,1)}, bf16[256,128]{1,0:T(8,128)(2,1)}) custom-call(bf16[2,256,384]{2,1,0:T(8,128)(2,1)} %get-tuple-element.30.fine_ref, f32[2,256,128]{2,1,0:T(8,128)} %get-tuple-element.31.ext_ref, f32[1,128]{1,0:T(1,128)} %bitcast.43, f32[1,8]{1,0:T(1,128)} %bitcast.44), custom_call_target="tpu_custom_call" | custom-call | tf_op jit(solution)/shard_map/delta_mix/pallas_call | solution.py:370
  91.7 1.5 %collective-permute-start.11 = (bf16[256,128]{1,0:T(8,128)(2,1)}, bf16[256,128]{1,0:T(8,128)(2,1)S(1)}, u32[]{:S(2)}, u32[]{:S(2)}) collective-permute-start(bf16[256,128]{1,0:T(8,128)(2,1)} %get-tuple-element.33), channel_id=1, source_target_pairs={{0,12},{4,0},{8,4},{12,8},{1,13},{5,1},{9,5},{13,9},{2,14},{6,2},{... | collective-permute-start | bytes 196616 | tf_op jit(solution)/shard_map/ppermute | solution.py:802
  93.2 0.9 collective-permute-start.13
  94.1 5.3 %latent_mix.1 = (bf16[256,128]{1,0:T(8,128)(2,1)}, bf16[256,128]{1,0:T(8,128)(2,1)}, bf16[256,128]{1,0:T(8,128)(2,1)}, bf16[256,128]{1,0:T(8,128)(2,1)}) custom-call(bf16[4,384,128]{2,1,0:T(8,128)(2,1)} %copy-done.3, bf16[4,384,128]{2,1,0:T(8,128)(2,1)} %copy-done.9, f32[2,256,128]{2,1,0:T(8,128)} %get-tuple-element.31.ext_ref, ...), custom_call_target="tpu_custom_call" | custom-call | tf_op jit(solution)/shard_map/latent_mix/pallas_call | solution.py:370
  99.4 3.0 %collective-permute-start.15 = (bf16[256,128]{1,0:T(8,128)(2,1)}, bf16[256,128]{1,0:T(8,128)(2,1)S(1)}, u32[]{:S(2)}, u32[]{:S(2)}) collective-permute-start(bf16[256,128]{1,0:T(8,128)(2,1)} %get-tuple-element.40), channel_id=1, source_target_pairs={{0,12},{4,0},{8,4},{12,8},{1,13},{5,1},{9,5},{13,9},{2,14},{6,2},{... | collective-permute-start | bytes 196616 | tf_op jit(solution)/shard_map/ppermute | solution.py:802
  102.4 1.1 collective-permute-start.16
  103.5 0.7 collective-permute-start.17
  104.3 1.0 collective-permute-done.15.refs_5_
  105.2 3.9 %collective-permute-done.16.refs_6_ = bf16[256,128]{1,0:T(8,128)(2,1)S(1)} collective-permute-done((bf16[256,128]{1,0:T(8,128)(2,1)}, bf16[256,128]{1,0:T(8,128)(2,1)S(1)}, u32[]{:S(2)}, u32[]{:S(2)}) %collective-permute-start.16) | collective-permute-done | bytes 65568 | tf_op jit(solution)/shard_map/ppermute | solution.py:802
  109.2 0.7 collective-permute-done.17.refs_7_
  109.9 0.6 copy-done.24
  110.5 3.4 %output_partial.1 = (bf16[2,128,512]{2,1,0:T(8,128)(2,1)}, bf16[2,128,512]{2,1,0:T(8,128)(2,1)}) custom-call(bf16[256,128]{1,0:T(8,128)(2,1)} %get-tuple-element.32.refs_0_, bf16[256,128]{1,0:T(8,128)(2,1)} %copy-done.19, bf16[256,128]{1,0:T(8,128)(2,1)} %copy-done.20, bf16[256,128]{1,0:T(8,128)(2,1)} %copy-done.21, ...), custom_call_target="tpu_custom_call" | custom-call | tf_op jit(solution)/shard_map/output_partial/pallas_call | solution.py:370
  113.9 1.7 %collective-permute-done.21 = bf16[2,128,512]{2,1,0:T(8,128)(2,1)S(1)} collective-permute-done((bf16[2,128,512]{2,1,0:T(8,128)(2,1)}, bf16[2,128,512]{2,1,0:T(8,128)(2,1)S(1)}, u32[]{:S(2)}, u32[]{:S(2)}) %collective-permute-start.21) | collective-permute-done | bytes 262176 | tf_op jit(solution)/shard_map/ppermute | solution.py:799
  115.6 1.0 add_convert_fusion
  116.8 5.5 %collective-permute-done.22 = bf16[128,512]{1,0:T(8,128)(2,1)S(1)} collective-permute-done((bf16[128,512]{1,0:T(8,128)(2,1)S(1)}, bf16[128,512]{1,0:T(8,128)(2,1)S(1)}, u32[]{:S(2)}, u32[]{:S(2)}) %collective-permute-start.22) | collective-permute-done | bytes 131104 | tf_op jit(solution)/shard_map/ppermute | solution.py:889
  122.5 1.1 collective-permute-done.23
  123.8 0.7 copy-done.27
  124.5 0.8 fusion.1
  (100 shorter events, 3.5 us)
Async XLA Ops:
  0.0 61.3 %copy-start = (bf16[256,1024]{1,0:T(8,128)(2,1)S(1)}, bf16[256,1024]{1,0:T(8,128)(2,1)}, u32[]{:S(2)}) copy-start(bf16[256,1024]{1,0:T(8,128)(2,1)} %param.36) | copy-start | bytes 1572868
  2.4 21.8 %all-to-all-start = ((bf16[4,128,512]{2,1,0:T(8,128)(2,1)}), bf16[4,128,512]{2,1,0:T(8,128)(2,1)S(1)}, u32[]{:S(2)}, u32[]{:S(2)}) async-start(bf16[4,128,512]{2,1,0:T(8,128)(2,1)} %outgoing_weights.1), calls=%async_computation | async-start | bytes 1048576 | tf_op jit(solution)/shard_map/weights_out/all_to_all | solution.py:796
  8.7 7.2 %copy-start.18 = (bf16[2048,32]{0,1:T(8,128)(2,1)S(1)}, bf16[2048,32]{0,1:T(8,128)(2,1)}, u32[]{:S(2)}) copy-start(bf16[2048,32]{0,1:T(8,128)(2,1)} %param.32) | copy-start | bytes 393220
  10.9 5.2 %copy-start.25 = (bf16[2048,8]{0,1:T(8,128)(2,1)S(1)}, bf16[2048,8]{0,1:T(8,128)(2,1)}, u32[]{:S(2)}) copy-start(bf16[2048,8]{0,1:T(8,128)(2,1)} %param.26) | copy-start | bytes 98308
  10.9 18.0 %collective-permute-start = (bf16[128,1024]{1,0:T(8,128)(2,1)}, bf16[128,1024]{1,0:T(8,128)(2,1)}, u32[]{:S(2)}, u32[]{:S(2)}) collective-permute-start(bf16[128,1024]{1,0:T(8,128)(2,1)} %get-tuple-element.26.refs_0_), channel_id=1, source_target_pairs={{0,12},{4,0},{8,4},{12,8},{1,13},{5,1},{9,5},{13,9},{2,14},{6,2},{... | collective-permute-start | bytes 786440 | tf_op jit(solution)/shard_map/tokens_out/ppermute | solution.py:802
  14.8 37.6 %collective-permute-start.2 = (bf16[128,1024]{1,0:T(8,128)(2,1)}, bf16[128,1024]{1,0:T(8,128)(2,1)}, u32[]{:S(2)}, u32[]{:S(2)}) collective-permute-start(bf16[128,1024]{1,0:T(8,128)(2,1)} %get-tuple-element.26.refs_0_), channel_id=1, source_target_pairs={{0,8},{4,12},{8,0},{12,4},{1,9},{5,13},{9,1},{13,5},{2,10},{6,14},... | collective-permute-start | bytes 786440 | tf_op jit(solution)/shard_map/tokens_out/ppermute | solution.py:802
  14.8 37.6 %collective-permute-start.3 = (bf16[128,1024]{1,0:T(8,128)(2,1)}, bf16[128,1024]{1,0:T(8,128)(2,1)}, u32[]{:S(2)}, u32[]{:S(2)}) collective-permute-start(bf16[128,1024]{1,0:T(8,128)(2,1)} %get-tuple-element.26.refs_0_), channel_id=1, source_target_pairs={{0,4},{4,8},{8,12},{12,0},{1,5},{5,9},{9,13},{13,1},{2,6},{6,10},{... | collective-permute-start | bytes 786440 | tf_op jit(solution)/shard_map/tokens_out/ppermute | solution.py:802
  17.3 1.0 copy-start.16
  17.3 1.0 copy-start.17
  24.2 3.1 %copy-start.2 = (bf16[4,128,512]{2,1,0:T(8,128)(2,1)}, bf16[4,128,512]{2,1,0:T(8,128)(2,1)S(1)}, u32[]{:S(2)}) copy-start(bf16[4,128,512]{2,1,0:T(8,128)(2,1)S(1)} %all-to-all-done) | copy-start | bytes 1572868
  24.2 28.7 %collective-permute-start.7 = (bf16[512,512]{1,0:T(8,128)(2,1)S(1)}, bf16[512,512]{1,0:T(8,128)(2,1)S(1)}, u32[]{:S(2)}, u32[]{:S(2)}) collective-permute-start(bf16[512,512]{1,0:T(8,128)(2,1)S(1)} %bitcast.28), channel_id=1, source_target_pairs={{0,2},{2,0},{1,3},{3,1},{4,6},{6,4},{5,7},{7,5},{8,10},{10,8},{9,1... | collective-permute-start | bytes 1572872 | tf_op jit(solution)/shard_map/ppermute | solution.py:799
  25.7 28.1 %collective-permute-start.8 = (bf16[512,512]{1,0:T(8,128)(2,1)S(1)}, bf16[512,512]{1,0:T(8,128)(2,1)}, u32[]{:S(2)}, u32[]{:S(2)}) collective-permute-start(bf16[512,512]{1,0:T(8,128)(2,1)S(1)} %bitcast.29), channel_id=1, source_target_pairs={{0,16},{16,0},{1,17},{17,1},{2,18},{18,2},{3,19},{19,3},{4,20},{20... | collective-permute-start | bytes 1572872 | tf_op jit(solution)/shard_map/ppermute | solution.py:799
  27.3 48.2 %copy-start.1 = (bf16[1024,256]{1,0:T(8,128)(2,1)}, bf16[1024,256]{1,0:T(8,128)(2,1)S(1)}, u32[]{:S(2)}) copy-start(bf16[1024,256]{1,0:T(8,128)(2,1)S(1)} %pad_maximum_fusion.refs_8_) | copy-start | bytes 1572868
  28.9 28.1 %collective-permute-start.1 = (bf16[512,256]{1,0:T(8,128)(2,1)S(1)}, bf16[512,256]{1,0:T(8,128)(2,1)S(1)}, u32[]{:S(2)}, u32[]{:S(2)}) collective-permute-start(bf16[512,256]{1,0:T(8,128)(2,1)S(1)} %constant_dynamic-slice_fusion), channel_id=1, source_target_pairs={{0,8},{4,12},{8,0},{12,4},{1,9},{5,13},{9,1},{13,5},{2,10},{6,14},... | collective-permute-start | bytes 786440 | tf_op jit(solution)/shard_map/far_out/ppermute | solution.py:802
  40.7 17.9 %copy-start.6 = (bf16[512,2,96]{0,2,1:T(8,128)(2,1)}, bf16[512,2,96]{0,2,1:T(8,128)(2,1)S(1)}, u32[]{:S(2)}) copy-start(bf16[512,2,96]{0,2,1:T(8,128)(2,1)S(1)} %dynamic-slice_bitcast_fusion) | copy-start | bytes 589828
  52.4 10.4 %collective-permute-start.4 = (bf16[128,1024]{1,0:T(8,128)(2,1)}, bf16[128,1024]{1,0:T(8,128)(2,1)S(1)}, u32[]{:S(2)}, u32[]{:S(2)}) collective-permute-start(bf16[128,1024]{1,0:T(8,128)(2,1)} %collective-permute-done.refs_1_), channel_id=1, source_target_pairs={{0,1},{1,0},{2,3},{3,2},{4,5},{5,4},{6,7},{7,6},{8,9},{9,8},{10,11... | collective-permute-start | bytes 786440 | tf_op jit(solution)/shard_map/ppermute | solution.py:799
  52.4 10.4 %collective-permute-start.5 = (bf16[128,1024]{1,0:T(8,128)(2,1)}, bf16[128,1024]{1,0:T(8,128)(2,1)S(1)}, u32[]{:S(2)}, u32[]{:S(2)}) collective-permute-start(bf16[128,1024]{1,0:T(8,128)(2,1)} %collective-permute-done.2.refs_2_), channel_id=1, source_target_pairs={{0,1},{1,0},{2,3},{3,2},{4,5},{5,4},{6,7},{7,6},{8,9},{9,8},{10,11... | collective-permute-start | bytes 786440 | tf_op jit(solution)/shard_map/ppermute | solution.py:799
  52.9 4.1 %copy-start.4 = (bf16[512,512]{1,0:T(8,128)(2,1)}, bf16[512,512]{1,0:T(8,128)(2,1)S(1)}, u32[]{:S(2)}) copy-start(bf16[512,512]{1,0:T(8,128)(2,1)S(1)} %collective-permute-done.7.refs_9_) | copy-start | bytes 1572868
  52.9 9.9 %collective-permute-start.6 = (bf16[128,1024]{1,0:T(8,128)(2,1)}, bf16[128,1024]{1,0:T(8,128)(2,1)S(1)}, u32[]{:S(2)}, u32[]{:S(2)}) collective-permute-start(bf16[128,1024]{1,0:T(8,128)(2,1)} %collective-permute-done.3.refs_3_), channel_id=1, source_target_pairs={{0,1},{1,0},{2,3},{3,2},{4,5},{5,4},{6,7},{7,6},{8,9},{9,8},{10,11... | collective-permute-start | bytes 786440 | tf_op jit(solution)/shard_map/ppermute | solution.py:799
  53.8 9.0 %collective-permute-start.10 = (bf16[256,512]{1,0:T(8,128)(2,1)}, bf16[256,512]{1,0:T(8,128)(2,1)}, u32[]{:S(2)}, u32[]{:S(2)}) collective-permute-start(bf16[256,512]{1,0:T(8,128)(2,1)} %slice.47), channel_id=1, source_target_pairs={{0,16},{16,0},{1,17},{17,1},{2,18},{18,2},{3,19},{19,3},{4,20},{20... | collective-permute-start | bytes 786440 | tf_op jit(solution)/shard_map/ppermute | solution.py:799
  57.0 1.6 %copy-start.14 = (bf16[512,256]{1,0:T(8,128)(2,1)}, bf16[512,256]{1,0:T(8,128)(2,1)S(1)}, u32[]{:S(2)}) copy-start(bf16[512,256]{1,0:T(8,128)(2,1)S(1)} %collective-permute-done.1) | copy-start | bytes 786436
  57.0 8.5 %collective-permute-start.9 = (bf16[256,512]{1,0:T(8,128)(2,1)}, bf16[256,512]{1,0:T(8,128)(2,1)S(1)}, u32[]{:S(2)}, u32[]{:S(2)}) collective-permute-start(bf16[256,512]{1,0:T(8,128)(2,1)} %slice.46), channel_id=1, source_target_pairs={{0,2},{2,0},{1,3},{3,1},{4,6},{6,4},{5,7},{7,5},{8,10},{10,8},{9,1... | collective-permute-start | bytes 786440 | tf_op jit(solution)/shard_map/ppermute | solution.py:799
  62.8 2.8 %copy-start.10 = (bf16[128,1024]{1,0:T(8,128)(2,1)}, bf16[128,1024]{1,0:T(8,128)(2,1)S(1)}, u32[]{:S(2)}) copy-start(bf16[128,1024]{1,0:T(8,128)(2,1)S(1)} %collective-permute-done.4.refs_5_) | copy-start | bytes 786436
  62.8 2.8 %copy-start.11 = (bf16[128,1024]{1,0:T(8,128)(2,1)}, bf16[128,1024]{1,0:T(8,128)(2,1)S(1)}, u32[]{:S(2)}) copy-start(bf16[128,1024]{1,0:T(8,128)(2,1)S(1)} %collective-permute-done.5.refs_6_) | copy-start | bytes 786436
  62.8 2.7 %copy-start.12 = (bf16[128,1024]{1,0:T(8,128)(2,1)}, bf16[128,1024]{1,0:T(8,128)(2,1)S(1)}, u32[]{:S(2)}) copy-start(bf16[128,1024]{1,0:T(8,128)(2,1)S(1)} %collective-permute-done.6.refs_7_) | copy-start | bytes 786436
  71.3 3.6 %copy-start.15 = (bf16[512,256]{1,0:T(8,128)(2,1)S(1)}, bf16[512,256]{1,0:T(8,128)(2,1)}, u32[]{:S(2)}) copy-start(bf16[512,256]{1,0:T(8,128)(2,1)} %copy-done.14) | copy-start | bytes 786436
  71.3 14.9 %all-to-all-start.1 = ((bf16[4,384,128]{2,1,0:T(8,128)(2,1)}), bf16[4,384,128]{2,1,0:T(8,128)(2,1)S(1)}, u32[]{:S(2)}, u32[]{:S(2)}) async-start(bf16[4,384,128]{2,1,0:T(8,128)(2,1)} %get-tuple-element.36), calls=%async_computation.1 | async-start | bytes 786432 | tf_op jit(solution)/shard_map/all_to_all | solution.py:796
  74.9 7.5 %collective-permute-start.19 = (bf16[512,256]{1,0:T(8,128)(2,1)S(1)}, bf16[512,256]{1,0:T(8,128)(2,1)S(1)}, u32[]{:S(2)}, u32[]{:S(2)}) collective-permute-start(bf16[512,256]{1,0:T(8,128)(2,1)S(1)} %copy-done.15), channel_id=1, source_target_pairs={{0,16},{16,0},{1,17},{17,1},{2,18},{18,2},{3,19},{19,3},{4,20},{20... | collective-permute-start | bytes 786440 | tf_op jit(solution)/shard_map/ppermute | solution.py:799
  75.5 23.9 %collective-permute-start.18 = (bf16[1024,256]{1,0:T(8,128)(2,1)S(1)}, bf16[1024,256]{1,0:T(8,128)(2,1)S(1)}, u32[]{:S(2)}, u32[]{:S(2)}) collective-permute-start(bf16[1024,256]{1,0:T(8,128)(2,1)S(1)} %pad_maximum_fusion.refs_8_), channel_id=1, source_target_pairs={{0,2},{2,0},{1,3},{3,1},{4,6},{6,4},{5,7},{7,5},{8,10},{10,8},{9,1... | collective-permute-start | bytes 1572872 | tf_op jit(solution)/shard_map/near_out/ppermute | solution.py:799
  82.4 27.5 %copy-start.5 = (bf16[1024,256]{1,0:T(8,128)(2,1)}, bf16[1024,256]{1,0:T(8,128)(2,1)S(1)}, u32[]{:S(2)}) copy-start(bf16[1024,256]{1,0:T(8,128)(2,1)S(1)} %constant_dynamic-update-slice_fusion.refs_10_) | copy-start | bytes 1572868
  82.4 20.0 %collective-permute-start.20 = (bf16[1024,256]{1,0:T(8,128)(2,1)S(1)}, bf16[1024,256]{1,0:T(8,128)(2,1)S(1)}, u32[]{:S(2)}, u32[]{:S(2)}) collective-permute-start(bf16[1024,256]{1,0:T(8,128)(2,1)S(1)} %constant_dynamic-update-slice_fusion.refs_10_), channel_id=1, source_target_pairs={{0,2},{2,0},{1,3},{3,1},{4,6},{6,4},{5,7},{7,5},{8,10},{10,8},{9,1... | collective-permute-start | bytes 1572872 | tf_op jit(solution)/shard_map/ppermute | solution.py:799
  86.2 7.9 %copy-start.3 = (bf16[4,384,128]{2,1,0:T(8,128)(2,1)}, bf16[4,384,128]{2,1,0:T(8,128)(2,1)S(1)}, u32[]{:S(2)}) copy-start(bf16[4,384,128]{2,1,0:T(8,128)(2,1)S(1)} %all-to-all-done.1.mine_ref) | copy-start | bytes 1179652
  86.2 7.0 %collective-permute-start.14 = (bf16[4,384,128]{2,1,0:T(8,128)(2,1)S(1)}, bf16[4,384,128]{2,1,0:T(8,128)(2,1)S(1)}, u32[]{:S(2)}, u32[]{:S(2)}) collective-permute-start(bf16[4,384,128]{2,1,0:T(8,128)(2,1)S(1)} %all-to-all-done.1.mine_ref), channel_id=1, source_target_pairs={{0,1},{1,0},{2,3},{3,2},{4,5},{5,4},{6,7},{7,6},{8,9},{9,8},{10,11... | collective-permute-start | bytes 1179656 | tf_op jit(solution)/shard_map/ppermute | solution.py:799
  91.7 11.8 %collective-permute-start.11 = (bf16[256,128]{1,0:T(8,128)(2,1)}, bf16[256,128]{1,0:T(8,128)(2,1)S(1)}, u32[]{:S(2)}, u32[]{:S(2)}) collective-permute-start(bf16[256,128]{1,0:T(8,128)(2,1)} %get-tuple-element.33), channel_id=1, source_target_pairs={{0,12},{4,0},{8,4},{12,8},{1,13},{5,1},{9,5},{13,9},{2,14},{6,2},{... | collective-permute-start | bytes 196616 | tf_op jit(solution)/shard_map/ppermute | solution.py:802
  93.2 11.0 %collective-permute-start.12 = (bf16[256,128]{1,0:T(8,128)(2,1)}, bf16[256,128]{1,0:T(8,128)(2,1)S(1)}, u32[]{:S(2)}, u32[]{:S(2)}) collective-permute-start(bf16[256,128]{1,0:T(8,128)(2,1)} %get-tuple-element.34), channel_id=1, source_target_pairs={{0,8},{4,12},{8,0},{12,4},{1,9},{5,13},{9,1},{13,5},{2,10},{6,14},... | collective-permute-start | bytes 196616 | tf_op jit(solution)/shard_map/ppermute | solution.py:802
  93.2 11.0 %collective-permute-start.13 = (bf16[256,128]{1,0:T(8,128)(2,1)}, bf16[256,128]{1,0:T(8,128)(2,1)S(1)}, u32[]{:S(2)}, u32[]{:S(2)}) collective-permute-start(bf16[256,128]{1,0:T(8,128)(2,1)} %get-tuple-element.35), channel_id=1, source_target_pairs={{0,4},{4,8},{8,12},{12,0},{1,5},{5,9},{9,13},{13,1},{2,6},{6,10},{... | collective-permute-start | bytes 196616 | tf_op jit(solution)/shard_map/ppermute | solution.py:802
  99.4 10.5 %copy-start.7 = (bf16[1024,256]{1,0:T(8,128)(2,1)}, bf16[1024,256]{1,0:T(8,128)(2,1)S(1)}, u32[]{:S(2)}) copy-start(bf16[1024,256]{1,0:T(8,128)(2,1)S(1)} %collective-permute-done.18.refs_9_) | copy-start | bytes 1572868
  99.4 5.8 %collective-permute-start.15 = (bf16[256,128]{1,0:T(8,128)(2,1)}, bf16[256,128]{1,0:T(8,128)(2,1)S(1)}, u32[]{:S(2)}, u32[]{:S(2)}) collective-permute-start(bf16[256,128]{1,0:T(8,128)(2,1)} %get-tuple-element.40), channel_id=1, source_target_pairs={{0,12},{4,0},{8,4},{12,8},{1,13},{5,1},{9,5},{13,9},{2,14},{6,2},{... | collective-permute-start | bytes 196616 | tf_op jit(solution)/shard_map/ppermute | solution.py:802
  102.4 7.4 %copy-start.8 = (bf16[1024,256]{1,0:T(8,128)(2,1)}, bf16[1024,256]{1,0:T(8,128)(2,1)S(1)}, u32[]{:S(2)}) copy-start(bf16[1024,256]{1,0:T(8,128)(2,1)S(1)} %collective-permute-done.20.refs_11_) | copy-start | bytes 1572868
  102.4 6.7 %collective-permute-start.16 = (bf16[256,128]{1,0:T(8,128)(2,1)}, bf16[256,128]{1,0:T(8,128)(2,1)S(1)}, u32[]{:S(2)}, u32[]{:S(2)}) collective-permute-start(bf16[256,128]{1,0:T(8,128)(2,1)} %get-tuple-element.41), channel_id=1, source_target_pairs={{0,8},{4,12},{8,0},{12,4},{1,9},{5,13},{9,1},{13,5},{2,10},{6,14},... | collective-permute-start | bytes 196616 | tf_op jit(solution)/shard_map/ppermute | solution.py:802
  103.5 6.4 %copy-start.19 = (bf16[256,128]{1,0:T(8,128)(2,1)}, bf16[256,128]{1,0:T(8,128)(2,1)S(1)}, u32[]{:S(2)}) copy-start(bf16[256,128]{1,0:T(8,128)(2,1)S(1)} %collective-permute-done.11.refs_1_) | copy-start | bytes 196612
  103.5 6.4 %collective-permute-start.17 = (bf16[256,128]{1,0:T(8,128)(2,1)}, bf16[256,128]{1,0:T(8,128)(2,1)S(1)}, u32[]{:S(2)}, u32[]{:S(2)}) collective-permute-start(bf16[256,128]{1,0:T(8,128)(2,1)} %get-tuple-element.42), channel_id=1, source_target_pairs={{0,4},{4,8},{8,12},{12,0},{1,5},{5,9},{9,13},{13,1},{2,6},{6,10},{... | collective-permute-start | bytes 196616 | tf_op jit(solution)/shard_map/ppermute | solution.py:802
  104.2 5.6 %copy-start.20 = (bf16[256,128]{1,0:T(8,128)(2,1)}, bf16[256,128]{1,0:T(8,128)(2,1)S(1)}, u32[]{:S(2)}) copy-start(bf16[256,128]{1,0:T(8,128)(2,1)S(1)} %collective-permute-done.12.refs_2_) | copy-start | bytes 196612
  104.2 5.6 %copy-start.21 = (bf16[256,128]{1,0:T(8,128)(2,1)}, bf16[256,128]{1,0:T(8,128)(2,1)S(1)}, u32[]{:S(2)}) copy-start(bf16[256,128]{1,0:T(8,128)(2,1)S(1)} %collective-permute-done.13.refs_3_) | copy-start | bytes 196612
  105.2 4.7 %copy-start.22 = (bf16[256,128]{1,0:T(8,128)(2,1)}, bf16[256,128]{1,0:T(8,128)(2,1)S(1)}, u32[]{:S(2)}) copy-start(bf16[256,128]{1,0:T(8,128)(2,1)S(1)} %collective-permute-done.15.refs_5_) | copy-start | bytes 196612
  113.9 1.7 %collective-permute-start.21 = (bf16[2,128,512]{2,1,0:T(8,128)(2,1)}, bf16[2,128,512]{2,1,0:T(8,128)(2,1)S(1)}, u32[]{:S(2)}, u32[]{:S(2)}) collective-permute-start(bf16[2,128,512]{2,1,0:T(8,128)(2,1)} %get-tuple-element.44), channel_id=1, source_target_pairs={{0,1},{1,0},{2,3},{3,2},{4,5},{5,4},{6,7},{7,6},{8,9},{9,8},{10,11... | collective-permute-start | bytes 786440 | tf_op jit(solution)/shard_map/ppermute | solution.py:799
  116.7 5.6 %collective-permute-start.22 = (bf16[128,512]{1,0:T(8,128)(2,1)S(1)}, bf16[128,512]{1,0:T(8,128)(2,1)S(1)}, u32[]{:S(2)}, u32[]{:S(2)}) collective-permute-start(bf16[128,512]{1,0:T(8,128)(2,1)S(1)} %dynamic-slice_bitcast_fusion.1), channel_id=1, source_target_pairs={{0,4},{4,0},{8,12},{12,8},{1,5},{5,1},{9,13},{13,9},{2,6},{6,2},{1... | collective-permute-start | bytes 393224 | tf_op jit(solution)/shard_map/ppermute | solution.py:889
  122.4 1.2 collective-permute-start.23
  (8 other events, 6.2 us)

commit v3 on v2

--- a/solution.py
+++ b/solution.py
@@ -7,6 +7,7 @@
 from jax.experimental import pallas as pl
 from jax.experimental.pallas import tpu as pltpu
 from jax.sharding import PartitionSpec as P
+
 
 D = 2048
 HEAD = 128
@@ -71,7 +72,7 @@
 
 
 def delta_terms(query_vectors, key_vectors, value_vectors, beta_gate, log_decay):
-    length, head_count, head_width = query_vectors.shape
+    length, head_count, _ = query_vectors.shape
     nblocks = length // BLOCK
 
     def split_blocks(tensor):
@@ -155,7 +156,6 @@
     kv_width = latent_down.shape[1] // lax.axis_size("tp")
     q_own = lax.dynamic_slice_in_dim(query_down, head_group * q_width, q_width, 1)
     kv_own = lax.dynamic_slice_in_dim(latent_down, head_group * kv_width, kv_width, 1)
-    weights = (query_weight, key_weight, value_weight, q_own, kv_own)
     portion = (
         lax.all_gather(query_weight, ("sp", "fs"), axis=0, tiled=True),
         lax.all_gather(key_weight, ("sp", "fs"), axis=0, tiled=True),
@@ -314,7 +314,7 @@
 
         return lax.fori_loop(0, row_count // span_rows, visit_block, current)
 
-    row_max, row_sum, weighted = lax.cond(
+    _, row_sum, weighted = lax.cond(
         jnp.int32(0) < query_start + token_count, visit_rows, keep_same, start_stats
     )
     latent_heads = (
@@ -365,17 +365,17 @@
     )
 
 
-def kernel_call(body, out_shapes, args, scratch=(), name=None):
-    specs = [pl.BlockSpec(memory_space=pltpu.VMEM) for _ in args]
+def kernel_call(body, out_shapes, args, scratch=(), inside=(True, True)):
+    space = pl.BlockSpec(memory_space=pltpu.VMEM)
+    operand_space, result_space = (pltpu.VMEM if here else pltpu.HBM for here in inside)
     return pl.pallas_call(
         body,
-        out_shape=out_shapes,
-        in_specs=specs,
-        out_specs=jax.tree.map(lambda _: pl.BlockSpec(memory_space=pltpu.VMEM), out_shapes),
+        out_shape=jax.tree.map(lambda leaf: result_space(leaf.shape, leaf.dtype), out_shapes),
+        in_specs=[space] * len(args),
+        out_specs=jax.tree.map(lambda _: space, out_shapes),
         scratch_shapes=scratch,
-        name=name,
-        compiler_params=pltpu.CompilerParams(vmem_limit_bytes=56 * 1024 * 1024),
-    )(*args)
+        compiler_params=pltpu.CompilerParams(vmem_limit_bytes=16 * 1024 * 1024),
+    )(*(pltpu.with_memory_space_constraint(arg, operand_space) for arg in args))
 
 
 def outgoing_weights(mixers, lats, sp_size):
@@ -407,7 +407,7 @@
         body,
         jax.ShapeDtypeStruct((sp_size, half, padded), jnp.bfloat16),
         (*mixers, *lats),
-        name="outgoing_weights",
+        inside=(False, False),
     )
 
 
@@ -429,7 +429,7 @@
                 their_ref[:, at : at + block] = jnp.where(first, high, low)
 
     shape = jax.ShapeDtypeStruct((rows, width // 2), jnp.bfloat16)
-    return kernel_call(body, (shape, shape), (tokens, gain), name="outgoing_tokens")
+    return kernel_call(body, (shape, shape), (tokens, gain))
 
 
 def project(mine, theirs, blocks, extra, sizes):
@@ -442,12 +442,12 @@
     extra_width = extra.shape[1]
     q_stack, kv_stack = 128 // q_cols, 128 // kv_cols
     packed = rows // q_stack + rows // kv_stack
-    lat_width = q_cols + kv_cols
 
     def body(*refs):
         mine_refs, refs = refs[:sp_size], refs[sp_size:]
         their_refs, refs = refs[:sp_size], refs[sp_size:]
-        block_refs, extra_ref, fine_ref, pack_ref, ext_ref, lat_ref = refs[:5], *refs[5:]
+        block_refs, refs = refs[:7], refs[7:]
+        extra_ref, fine_ref, pack_ref, ext_ref, lat_ref = refs
         place, fs_at = lax.axis_index("sp"), lax.axis_index("fs")
         tp_at = lax.axis_index("tp")
         straight = tp_at == lax.axis_index("grp")
@@ -463,15 +463,12 @@
                     one, two = two, one
                 return jnp.where(straight, one, two)
 
-            far = half_of(False, False)
-            cut = block_refs[3].shape[0]
-            value = (
-                dot32(half_of(True, True), block_refs[0][...])
-                + dot32(half_of(True, False), block_refs[1][...])
-                + dot32(half_of(False, True), block_refs[2][...])
-                + dot32(far[:, :cut], block_refs[3][...])
-                + dot32(far[:, cut:], block_refs[4][...])
-            ).astype(jnp.bfloat16)
+            value = dot32(half_of(True, True), block_refs[0][...])
+            for k, (same_grp, same_fs) in enumerate(((True, False), (False, True), (False, False))):
+                lhs = half_of(same_grp, same_fs)
+                value = value + dot32(lhs[:, : middle // 2], block_refs[2 * k + 1][...])
+                value = value + dot32(lhs[:, middle // 2 :], block_refs[2 * k + 2][...])
+            value = value.astype(jnp.bfloat16)
             mine_at = pl.ds(pl.multiple_of(tp_at * part, part), part)
             their_at = pl.ds(pl.multiple_of((1 - tp_at) * part, part), part)
             outer = dot32(mine_refs[o][...], extra_ref[mine_at, :])
@@ -511,11 +508,10 @@
         ),
         (*mine, *theirs, *blocks, extra),
         scratch=(pltpu.VMEM((rows, 128), jnp.bfloat16),),
-        name="project",
-    )
-
-
-def send_by_pair(out_refs, pieces, sp_size, token_count):
+    )
+
+
+def send_by_pair(out_refs, pieces, sp_size):
     place = lax.axis_index("sp")
     for step, out_ref in enumerate(out_refs):
         second = lax.rem(place + step, sp_size) >= sp_size // 2
@@ -613,12 +609,10 @@
         for h in range(heads):
             columns = slice(h * HEAD, (h + 1) * HEAD)
             views = [ref.at[:, columns] for ref in out_refs] if heads > 1 else out_refs
-            send_by_pair(views, pieces[h::heads], sp_size, span // sp_size)
+            send_by_pair(views, pieces[h::heads], sp_size)
 
     shape = jax.ShapeDtypeStruct((seq_count * span // 2, heads * HEAD), jnp.bfloat16)
-    return kernel_call(
-        body, (shape,) * sp_size, (fine, ext, gain, rates), name="delta_mix"
-    )
+    return kernel_call(body, (shape,) * sp_size, (fine, ext, gain, rates), inside=(True, False))
 
 
 def latent_mix(mine, theirs, ext, tables, gains, ups, q_cols, kv_cols, heads):
@@ -683,18 +677,13 @@
                 results.append(dot32(weights.astype(jnp.bfloat16), values) / total)
             joined = jnp.concatenate(results, axis=1).astype(jnp.bfloat16)
             joins.append((joined[: span // 2], joined[span // 2 :]))
-        send_by_pair(out_refs, joins, sp_size, span // sp_size)
+        send_by_pair(out_refs, joins, sp_size)
 
     shape = jax.ShapeDtypeStruct((rows // 2, heads * VDIM), jnp.bfloat16)
-    return kernel_call(
-        body,
-        (shape,) * sp_size,
-        (mine, theirs, ext, *tables, *gains, *ups),
-        name="latent_mix",
-    )
-
-
-def output_partial(delta_all, latent_all, near, near_fs, far, far_fs, sizes):
+    return kernel_call(body, (shape,) * sp_size, (mine, theirs, ext, *tables, *gains, *ups))
+
+
+def output_partial(delta_all, latent_all, near, near_fs, far, sizes):
     seq_count, token_count = sizes
     sp_size = len(delta_all)
     rows, d_width = delta_all[0].shape
@@ -706,7 +695,7 @@
     def body(*refs):
         d_refs, refs = refs[:sp_size], refs[sp_size:]
         l_refs, refs = refs[:sp_size], refs[sp_size:]
-        near_ref, near_fs_ref, far_ref, far_fs_ref, keep_ref, pass_ref, lhs_ref = refs
+        near_ref, near_fs_ref, *far_refs, keep_ref, pass_ref, lhs_ref = refs
         place, fs_at = lax.axis_index("sp"), lax.axis_index("fs")
         grp_at = lax.axis_index("grp")
         for o in range(sp_size):
@@ -725,8 +714,8 @@
             dot32(lhs, near_fs_ref[...]).astype(jnp.bfloat16),
         )
         away = tuple(
-            (dot32(own, ref[:half, :]) + dot32(other, ref[half:, :])).astype(jnp.bfloat16)
-            for ref in (far_ref, far_fs_ref)
+            (dot32(own, far_refs[k][...]) + dot32(other, far_refs[k + 1][...])).astype(jnp.bfloat16)
+            for k in (0, 2)
         )
         straight = place // per_half == lax.axis_index("tp")
         for k in range(2):
@@ -746,9 +735,8 @@
     return kernel_call(
         body,
         (shape, shape),
-        (*delta_all, *latent_all, near, near_fs, far, far_fs),
+        (*delta_all, *latent_all, near, near_fs, *far),
         scratch=(pltpu.VMEM((rows, total), jnp.bfloat16),),
-        name="output_partial",
     )
 
 
@@ -804,35 +792,35 @@
     def from_sp(sends):
         return [sends[0]] + [along(sends[step], step) for step in range(sp_size - 1, 0, -1)]
 
-    with jax.named_scope("weights_out"):
-        outgoing = outgoing_weights(
-            (query_weight, key_weight, value_weight), (query_down, latent_down), sp_size
-        )
-        block = exchange(outgoing, "sp").reshape(-1, outgoing.shape[2])
+    outgoing = outgoing_weights(
+        (query_weight, key_weight, value_weight), (query_down, latent_down), sp_size
+    )
+    block = exchange(outgoing, "sp").reshape(-1, outgoing.shape[2])
     token_rows, outgoing = lax.optimization_barrier((tokens.reshape(rows, width), outgoing))
 
+    own_half, other_half = outgoing_tokens(token_rows, pre_gain[None, :], sp_size)
+    mine = [own_half] + [along(own_half, step) for step in range(sp_size - 1, 0, -1)]
     quarter = delta_out.shape[0] // 2
     near = jnp.concatenate(
         [w[k * quarter : (k + 1) * quarter] for k in range(2) for w in (delta_out, latent_out)]
     )
-    with jax.named_scope("near_out"):
-        near_fs = swap(near, "fs")
-
-    own_half, other_half = outgoing_tokens(token_rows, pre_gain[None, :], sp_size)
-    with jax.named_scope("tokens_out"):
-        mine = from_sp([own_half] * sp_size)
+    near_fs = swap(near, "fs")
+
+    middle = block.shape[0] // 2
+    low, high = block[:middle], block[middle:]
+    low_grp = swap(low, "grp")
+    high_fs = swap(high, "fs")
+    low_fs = swap(low, "fs")
+    high_grp = swap(high, "grp")
+    corner = swap(low_grp, "fs"), swap(high_fs, "grp")
+    blocks = (block, low_fs, high_fs, low_grp, high_grp, *corner)
     theirs = [other_half] + [swap(piece, "tp") for piece in mine[1:]]
 
-    with jax.named_scope("far_out"):
-        far_half = lax.dynamic_slice_in_dim(near, grp_at * 2 * quarter, 2 * quarter, 0)
-        far_half = along(far_half, sp_size // 2)
-
-    middle = block.shape[0] // 2
-    by_fs, by_grp = swap(block, "fs"), swap(block, "grp")
-    blocks = (block, by_fs, by_grp, swap(by_grp[:middle], "fs"), swap(by_fs[middle:], "grp"))
-
-    far = jnp.concatenate([far_half, swap(far_half, "grp")])
-    far_fs = swap(far, "fs")
+    far_own = lax.dynamic_slice_in_dim(near, grp_at * 2 * quarter, 2 * quarter, 0)
+    far_own = along(far_own, sp_size // 2)
+    far_other = swap(far_own, "grp")
+    far = (far_own, far_other, swap(far_own, "fs"))
+    far = (*far, swap(far_other, "fs"))
 
     gate_at = rope_weight.shape[1]
     filler = -(gate_at + 2 * beta_weight.shape[1]) % 128
@@ -847,25 +835,27 @@
     up = lax.dynamic_index_in_dim(up, place, 1, False)
     turn = up[..., NOPE:]
     back = jnp.concatenate([turn[..., ROPE // 2 :], turn[..., : ROPE // 2]], axis=-1)
-    q_up = jnp.concatenate(
-        [a.reshape(up.shape[0], -1) for a in (up[..., :NOPE], turn, back)], axis=1
-    )
+    parts = [a.reshape(up.shape[0], -1) for a in (up[..., :NOPE], turn, back)]
+    q_up = jnp.concatenate(parts, axis=1)
     kv_width = latent_up.shape[1] // sp_size
     kv_up = lax.dynamic_slice_in_dim(latent_up, place * kv_width, kv_width, 1)
     tables = whole_tables(sp_size * token_count, latent_heads)
-    mine[1], extra, q_up, kv_up, far_half = lax.optimization_barrier(
-        (mine[1], extra, q_up, kv_up, far_half)
-    )
+    mine[1], extra, q_up, kv_up = lax.optimization_barrier((mine[1], extra, q_up, kv_up))
 
     fine, lat, ext = project(
-        mine, theirs, blocks, extra, (seq_count, token_count, 3 * heads * HEAD, q_cols, kv_cols)
+        mine,
+        theirs,
+        blocks,
+        extra,
+        (seq_count, token_count, 3 * heads * HEAD, q_cols, kv_cols),
     )
     lat_mine = exchange(lat, "sp")
+    delta_sends = delta_mix(
+        fine, ext, delta_gain[None, :], decay_rate[None, :], gate_at, heads, sp_size
+    )
+    lat_mine, delta_sends = lax.optimization_barrier((lat_mine, delta_sends))
     lat_theirs = swap(lat_mine, "tp")
-
-    delta_all = from_sp(
-        delta_mix(fine, ext, delta_gain[None, :], decay_rate[None, :], gate_at, heads, sp_size)
-    )
+    delta_all = from_sp(delta_sends)
     latent_all = from_sp(
         latent_mix(
             lat_mine,
@@ -881,7 +871,7 @@
     )
 
     keep, onward = output_partial(
-        delta_all, latent_all, near, near_fs, far, far_fs, (seq_count, token_count)
+        delta_all, latent_all, near, near_fs, far, (seq_count, token_count)
     )
     mixed = (keep.astype(f32) + swap(onward, "tp").astype(f32)).astype(bf16)
     side = lax.rem(place, 2)

time: 126 us -> 138 us (1.095)
  waiting for transfers between devices: 41.9 us -> 64.1 us
  Pallas kernels: 23.8 us -> 15.9 us
  starting transfers between devices: 44.3 us -> 37.7 us
  local copies, waits for them, and re-layouts: 11.6 us -> 15 us
    ppermute x10, waiting for transfers between devices: 17.3 us -> 45.9 us  [along(): lax.ppermute(values, 'sp', [(i, (i + step) % sp_size) for i in range(sp_s...]
    ppermute x10, starting transfers between devices: 23.9 us -> 15.2 us  [along(): lax.ppermute(values, 'sp', [(i, (i + step) % sp_size) for i in range(sp_s...]
    all_to_all x2, waiting for transfers between devices: 8.06 us -> 0.01 us  [exchange(): return lax.all_to_all(values, axis, 0, 0, tiled=True)]
    pallas_call x6, Pallas kernels: 23.8 us -> 15.9 us  [kernel_call(): pl.pallas_call(body, out_shape=jax.tree.map(lambda leaf: result_space(lea...]
    ppermute x13 -> x16, starting transfers between devices: 10.4 us -> 12.4 us  [swap(): return lax.ppermute(values, axis, [(0, 1), (1, 0)])]
    unnamed x61 -> x60, local copies, waits for them, and re-layouts: 5.47 us -> 7.51 us
    concatenate x1, other arithmetic: 0.51 us -> 2.52 us  [whole_sequences(): jnp.concatenate([rope_weight, beta_weight, decay_weight, jnp.zeros((width...]
    slice x1, local copies, waits for them, and re-layouts: 0.03 us -> 1.92 us  [whole_sequences(): w[k * quarter:(k + 1) * quarter]]
  transfers between devices with their start and end apart: 26 -> 29, of which waited for: 11 -> 15; matrix products, arithmetic and copies ran while one was open for 7% -> 11% of each run, Pallas kernels for 10% -> 6%
where the time goes in v3:
time: 138 us
  waiting for transfers between devices  64.1 us (46%)
  starting transfers between devices  37.7 us (27%)
  Pallas kernels  15.9 us (12%)
  local copies, waits for them, and re-layouts  15 us (11%)
  other arithmetic  4.65 us (3%)
    ppermute x10, waiting for transfers between devices, along(): lax.ppermute(values, 'sp', [(i, (i + step) % sp_size) for i in range(sp_s...  45.9 us
    pallas_call x6, Pallas kernels, kernel_call(): pl.pallas_call(body, out_shape=jax.tree.map(lambda leaf: result_space(lea...  15.9 us
    ppermute x10, starting transfers between devices, along(): lax.ppermute(values, 'sp', [(i, (i + step) % sp_size) for i in range(sp_s...  15.2 us
    ppermute x16, waiting for transfers between devices, swap(): return lax.ppermute(values, axis, [(0, 1), (1, 0)])  12.6 us
    ppermute x16, starting transfers between devices, swap(): return lax.ppermute(values, axis, [(0, 1), (1, 0)])  12.4 us
    all_to_all x2, starting transfers between devices, exchange(): return lax.all_to_all(values, axis, 0, 0, tiled=True)  10.1 us
    unnamed x60, local copies, waits for them, and re-layouts  7.51 us
    ppermute x1, waiting for transfers between devices, whole_sequences(): lax.ppermute(pick(mixed, 1 - side), 'sp', [(i, i ^ 1) for i in range(sp_s...  5.52 us
  transfers between devices with their start and end apart: 29, of which 15 were waited for; matrix products, arithmetic and copies ran while one was open for 11% of the time, Pallas kernels for 6%

profile of v3, /device:TPU:0, one launch (start us, length us, event | category | flops | bytes accessed | tf_op | source)
XLA Modules:
  0.0 137.8 jit_solution(13335706422123507050)
XLA Ops:
  0.0 2.4 %shard_map.199 = bf16[4,128,512]{2,1,0:T(8,128)(2,1)} custom-call(bf16[256,512]{1,0:T(8,128)(2,1)} %refs_0_.1, bf16[256,512]{1,0:T(8,128)(2,1)} %refs_1_.1, bf16[256,512]{1,0:T(8,128)(2,1)} %refs_2_.1, bf16[256,512]{1,0:T(8,128)(2,1)} %refs_3_.1, bf16[256,256]{1,0:T(8,128)(2,1)} %refs_4_.1), custom_call_target="tpu_custom_call" | custom-call | tf_op jit(solution)/shard_map/pallas_call | solution.py:371
  2.4 6.5 %all-to-all-start = ((bf16[4,128,512]{2,1,0:T(8,128)(2,1)}), bf16[4,128,512]{2,1,0:T(8,128)(2,1)S(1)}, u32[]{:S(2)}, u32[]{:S(2)}) async-start(bf16[4,128,512]{2,1,0:T(8,128)(2,1)} %shard_map.199), calls=%async_computation | async-start | bytes 1048576 | tf_op jit(solution)/shard_map/all_to_all | solution.py:784
  9.2 3.9 %collective-permute-start = (bf16[128,1024]{1,0:T(8,128)(2,1)S(1)}, bf16[128,1024]{1,0:T(8,128)(2,1)S(1)}, u32[]{:S(2)}, u32[]{:S(2)}) collective-permute-start(bf16[128,1024]{1,0:T(8,128)(2,1)S(1)} %get-tuple-element.31.refs_0_), channel_id=1, source_target_pairs={{0,12},{4,0},{8,4},{12,8},{1,13},{5,1},{9,5},{13,9},{2,14},{6,2},{... | collective-permute-start | bytes 786440 | tf_op jit(solution)/shard_map/ppermute | solution.py:790
  13.1 1.1 collective-permute-start.2
  14.5 1.0 copy.26
  15.6 1.0 copy.27
  16.7 2.5 %maximum_maximum_fusion = bf16[2048,128]{1,0:T(8,128)(2,1)} fusion(bf16[2048,8]{1,0:T(8,128)(2,1)} %copy.27, bf16[2048,8]{1,0:T(8,128)(2,1)} %copy.26, bf16[2048,32]{1,0:T(8,128)(2,1)S(1)} %copy.25, bf16[128]{0:T(256)(128)(2,1)S(1)} %pad.14.clone), kind=kLoop, calls=%fused_computation | loop fusion | flops 2097152 | bytes 721152 | tf_op jit(solution)/shard_map/concatenate | solution.py:827
  19.2 2.3 %copy.29 = bf16[512,768]{0,1:T(8,128)(2,1)} copy(bf16[512,768]{1,0:T(8,128)(2,1)} %param.35) | data formatting | bytes 1572864 | tf_op args[14]
  21.5 0.9 dynamic-slice_bitcast_fusion
  22.5 2.8 %collective-permute-done.refs_1_ = bf16[128,1024]{1,0:T(8,128)(2,1)S(1)} collective-permute-done((bf16[128,1024]{1,0:T(8,128)(2,1)S(1)}, bf16[128,1024]{1,0:T(8,128)(2,1)S(1)}, u32[]{:S(2)}, u32[]{:S(2)}) %collective-permute-start) | collective-permute-done | bytes 262176 | tf_op jit(solution)/shard_map/ppermute | solution.py:790
  25.3 20.6 %collective-permute-done.1.refs_2_ = bf16[128,1024]{1,0:T(8,128)(2,1)S(1)} collective-permute-done((bf16[128,1024]{1,0:T(8,128)(2,1)S(1)}, bf16[128,1024]{1,0:T(8,128)(2,1)S(1)}, u32[]{:S(2)}, u32[]{:S(2)}) %collective-permute-start.1) | collective-permute-done | bytes 262176 | tf_op jit(solution)/shard_map/ppermute | solution.py:790
  45.8 0.9 fusion.4
  46.7 1.5 %collective-permute-start.8 = (bf16[256,512]{1,0:T(8,128)(2,1)}, bf16[256,512]{1,0:T(8,128)(2,1)}, u32[]{:S(2)}, u32[]{:S(2)}) collective-permute-start(bf16[256,512]{1,0:T(8,128)(2,1)} %bitcast.11), channel_id=1, source_target_pairs={{0,16},{16,0},{1,17},{17,1},{2,18},{18,2},{3,19},{19,3},{4,20},{20... | collective-permute-start | bytes 786440 | tf_op jit(solution)/shard_map/ppermute | solution.py:787
  48.2 1.5 %collective-permute-start.7 = (bf16[256,512]{1,0:T(8,128)(2,1)}, bf16[256,512]{1,0:T(8,128)(2,1)}, u32[]{:S(2)}, u32[]{:S(2)}) collective-permute-start(bf16[256,512]{1,0:T(8,128)(2,1)} %bitcast.12), channel_id=1, source_target_pairs={{0,2},{2,0},{1,3},{3,1},{4,6},{6,4},{5,7},{7,5},{8,10},{10,8},{9,1... | collective-permute-start | bytes 786440 | tf_op jit(solution)/shard_map/ppermute | solution.py:787
  49.9 0.8 slice-done
  50.6 0.8 copy.30
  51.5 0.7 copy.31
  52.3 1.0 pad_maximum_fusion.1.refs_2_
  54.1 0.7 copy-done.8
  55.7 1.5 %collective-permute-start.10 = (bf16[256,512]{1,0:T(8,128)(2,1)}, bf16[256,512]{1,0:T(8,128)(2,1)}, u32[]{:S(2)}, u32[]{:S(2)}) collective-permute-start(bf16[256,512]{1,0:T(8,128)(2,1)} %collective-permute-done.8.refs_11_), channel_id=1, source_target_pairs={{0,2},{2,0},{1,3},{3,1},{4,6},{6,4},{5,7},{7,5},{8,10},{10,8},{9,1... | collective-permute-start | bytes 786440 | tf_op jit(solution)/shard_map/ppermute | solution.py:787
  57.2 1.5 %collective-permute-start.11 = (bf16[256,512]{1,0:T(8,128)(2,1)}, bf16[256,512]{1,0:T(8,128)(2,1)}, u32[]{:S(2)}, u32[]{:S(2)}) collective-permute-start(bf16[256,512]{1,0:T(8,128)(2,1)} %collective-permute-done.7.refs_10_), channel_id=1, source_target_pairs={{0,16},{16,0},{1,17},{17,1},{2,18},{18,2},{3,19},{19,3},{4,20},{20... | collective-permute-start | bytes 786440 | tf_op jit(solution)/shard_map/ppermute | solution.py:787
  58.7 1.1 copy.28
  59.9 1.9 %fusion.5 = (bf16[256,256]{1,0:T(8,128)(2,1)S(1)}, bf16[256,256]{1,0:T(8,128)(2,1)}, bf16[256,256]{1,0:T(8,128)(2,1)}, bf16[256,256]{1,0:T(8,128)(2,1)}) fusion(bf16[512,256]{1,0:T(8,128)(2,1)} %param.37, bf16[512,256]{1,0:T(8,128)(2,1)} %param.38), kind=kLoop, calls=%fused_computation.21 | loop fusion | bytes 1048576 | tf_op jit(solution)/shard_map/slice | solution.py:805
  61.8 1.2 collective-permute-done.6.refs_9_
  63.0 1.2 collective-permute-done.9.refs_12_
  64.3 3.9 %collective-permute-done.10.refs_13_ = bf16[256,512]{1,0:T(8,128)(2,1)} collective-permute-done((bf16[256,512]{1,0:T(8,128)(2,1)}, bf16[256,512]{1,0:T(8,128)(2,1)}, u32[]{:S(2)}, u32[]{:S(2)}) %collective-permute-start.10) | collective-permute-done | bytes 262176 | tf_op jit(solution)/shard_map/ppermute | solution.py:787
  68.2 0.9 collective-permute-done.11.refs_14_
  69.1 4.0 %shard_map.201 = (bf16[2,256,384]{2,1,0:T(8,128)(2,1)S(1)}, bf16[4,384,128]{2,1,0:T(8,128)(2,1)}, f32[2,256,128]{2,1,0:T(8,128)S(1)}) custom-call(bf16[128,1024]{1,0:T(8,128)(2,1)S(1)} %get-tuple-element.31.refs_0_, bf16[128,1024]{1,0:T(8,128)(2,1)S(1)} %collective-permute-done.refs_1_, bf16[128,1024]{1,0:T(8,128)(2,1)S(1)} %copy-done.3, ...), custom_call_target="tpu_custom_call" | custom-call | tf_op jit(solution)/shard_map/pallas_call | solution.py:371
  73.1 3.6 %all-to-all-start.1 = ((bf16[4,384,128]{2,1,0:T(8,128)(2,1)}), bf16[4,384,128]{2,1,0:T(8,128)(2,1)S(1)}, u32[]{:S(2)}, u32[]{:S(2)}) async-start(bf16[4,384,128]{2,1,0:T(8,128)(2,1)} %get-tuple-element.35), calls=%async_computation.1 | async-start | bytes 786432 | tf_op jit(solution)/shard_map/all_to_all | solution.py:784
  76.8 2.9 %collective-permute-start.20 = (bf16[512,256]{1,0:T(8,128)(2,1)S(1)}, bf16[512,256]{1,0:T(8,128)(2,1)S(1)}, u32[]{:S(2)}, u32[]{:S(2)}) collective-permute-start(bf16[512,256]{1,0:T(8,128)(2,1)S(1)} %constant_dynamic-slice_fusion), channel_id=1, source_target_pairs={{0,8},{4,12},{8,0},{12,4},{1,9},{5,13},{9,1},{13,5},{2,10},{6,14},... | collective-permute-start | bytes 786440 | tf_op jit(solution)/shard_map/ppermute | solution.py:790
  79.7 1.5 %collective-permute-start.19 = (bf16[1024,256]{1,0:T(8,128)(2,1)S(1)}, bf16[1024,256]{1,0:T(8,128)(2,1)S(1)}, u32[]{:S(2)}, u32[]{:S(2)}) collective-permute-start(bf16[1024,256]{1,0:T(8,128)(2,1)S(1)} %pad_maximum_fusion.refs_8_), channel_id=1, source_target_pairs={{0,2},{2,0},{1,3},{3,1},{4,6},{6,4},{5,7},{7,5},{8,10},{10,8},{9,1... | collective-permute-start | bytes 1572872 | tf_op jit(solution)/shard_map/ppermute | solution.py:787
  81.2 18.1 %collective-permute-done.20.refs_10_ = bf16[512,256]{1,0:T(8,128)(2,1)S(1)} collective-permute-done((bf16[512,256]{1,0:T(8,128)(2,1)S(1)}, bf16[512,256]{1,0:T(8,128)(2,1)S(1)}, u32[]{:S(2)}, u32[]{:S(2)}) %collective-permute-start.20) | collective-permute-done | bytes 262176 | tf_op jit(solution)/shard_map/ppermute | solution.py:790
  100.5 4.3 %shard_map.202 = (bf16[256,128]{1,0:T(8,128)(2,1)}, bf16[256,128]{1,0:T(8,128)(2,1)}, bf16[256,128]{1,0:T(8,128)(2,1)}, bf16[256,128]{1,0:T(8,128)(2,1)}) custom-call(bf16[2,256,384]{2,1,0:T(8,128)(2,1)S(1)} %get-tuple-element.36.fine_ref, f32[2,256,128]{2,1,0:T(8,128)S(1)} %get-tuple-element.37.ext_ref, f32[1,128]{1,0:T(1,128)S(1)} %bitcast.36, ...), custom_call_target="tpu_custom_call" | custom-call | tf_op jit(solution)/shard_map/pallas_call | solution.py:371
  104.8 1.5 %collective-permute-start.22 = (bf16[512,256]{1,0:T(8,128)(2,1)S(1)}, bf16[512,256]{1,0:T(8,128)(2,1)S(1)}, u32[]{:S(2)}, u32[]{:S(2)}) collective-permute-start(bf16[512,256]{1,0:T(8,128)(2,1)S(1)} %collective-permute-done.20.refs_10_), channel_id=1, source_target_pairs={{0,2},{2,0},{1,3},{3,1},{4,6},{6,4},{5,7},{7,5},{8,10},{10,8},{9,1... | collective-permute-start | bytes 786440 | tf_op jit(solution)/shard_map/ppermute | solution.py:787
  106.7 1.5 %collective-permute-start.23 = (bf16[512,256]{1,0:T(8,128)(2,1)}, bf16[512,256]{1,0:T(8,128)(2,1)S(1)}, u32[]{:S(2)}, u32[]{:S(2)}) collective-permute-start(bf16[512,256]{1,0:T(8,128)(2,1)} %collective-permute-done.21.refs_11_), channel_id=1, source_target_pairs={{0,2},{2,0},{1,3},{3,1},{4,6},{6,4},{5,7},{7,5},{8,10},{10,8},{9,1... | collective-permute-start | bytes 786440 | tf_op jit(solution)/shard_map/ppermute | solution.py:787
  108.2 1.4 %collective-permute-start.12 = (bf16[256,128]{1,0:T(8,128)(2,1)}, bf16[256,128]{1,0:T(8,128)(2,1)S(1)}, u32[]{:S(2)}, u32[]{:S(2)}) collective-permute-start(bf16[256,128]{1,0:T(8,128)(2,1)} %get-tuple-element.43), channel_id=1, source_target_pairs={{0,12},{4,0},{8,4},{12,8},{1,13},{5,1},{9,5},{13,9},{2,14},{6,2},{... | collective-permute-start | bytes 196616 | tf_op jit(solution)/shard_map/ppermute | solution.py:790
  110.3 3.1 %shard_map.203 = (bf16[256,128]{1,0:T(8,128)(2,1)S(1)}, bf16[256,128]{1,0:T(8,128)(2,1)S(1)}, bf16[256,128]{1,0:T(8,128)(2,1)S(1)}, bf16[256,128]{1,0:T(8,128)(2,1)S(1)}) custom-call(bf16[4,384,128]{2,1,0:T(8,128)(2,1)S(1)} %all-to-all-done.1.mine_ref, bf16[4,384,128]{2,1,0:T(8,128)(2,1)S(1)} %collective-permute-done.15.their_ref, ...), custom_call_target="tpu_custom_call" | custom-call | tf_op jit(solution)/shard_map/pallas_call | solution.py:371
  113.4 0.7 collective-permute-done.22.refs_12_
  114.1 3.8 %collective-permute-start.16 = (bf16[256,128]{1,0:T(8,128)(2,1)S(1)}, bf16[256,128]{1,0:T(8,128)(2,1)S(1)}, u32[]{:S(2)}, u32[]{:S(2)}) collective-permute-start(bf16[256,128]{1,0:T(8,128)(2,1)S(1)} %get-tuple-element.50), channel_id=1, source_target_pairs={{0,12},{4,0},{8,4},{12,8},{1,13},{5,1},{9,5},{13,9},{2,14},{6,2},{... | collective-permute-start | bytes 196616 | tf_op jit(solution)/shard_map/ppermute | solution.py:790
  117.9 1.2 collective-permute-done.23.refs_13_
  119.2 2.0 %collective-permute-start.18 = (bf16[256,128]{1,0:T(8,128)(2,1)S(1)}, bf16[256,128]{1,0:T(8,128)(2,1)S(1)}, u32[]{:S(2)}, u32[]{:S(2)}) collective-permute-start(bf16[256,128]{1,0:T(8,128)(2,1)S(1)} %get-tuple-element.52), channel_id=1, source_target_pairs={{0,4},{4,8},{8,12},{12,0},{1,5},{5,9},{9,13},{13,1},{2,6},{6,10},{... | collective-permute-start | bytes 196616 | tf_op jit(solution)/shard_map/ppermute | solution.py:790
  121.2 4.5 %collective-permute-done.17.refs_6_ = bf16[256,128]{1,0:T(8,128)(2,1)S(1)} collective-permute-done((bf16[256,128]{1,0:T(8,128)(2,1)S(1)}, bf16[256,128]{1,0:T(8,128)(2,1)S(1)}, u32[]{:S(2)}, u32[]{:S(2)}) %collective-permute-start.17) | collective-permute-done | bytes 65568 | tf_op jit(solution)/shard_map/ppermute | solution.py:790
  125.7 1.8 %shard_map.204 = (bf16[2,128,512]{2,1,0:T(8,128)(2,1)S(1)}, bf16[2,128,512]{2,1,0:T(8,128)(2,1)S(1)}) custom-call(bf16[256,128]{1,0:T(8,128)(2,1)S(1)} %copy-done.12, bf16[256,128]{1,0:T(8,128)(2,1)S(1)} %collective-permute-done.12.refs_1_, bf16[256,128]{1,0:T(8,128)(2,1)S(1)} %collective-permute-done.13.refs_2_, ...), custom_call_target="tpu_custom_call" | custom-call | tf_op jit(solution)/shard_map/pallas_call | solution.py:371
  127.6 1.5 %collective-permute-done.24 = bf16[2,128,512]{2,1,0:T(8,128)(2,1)S(1)} collective-permute-done((bf16[2,128,512]{2,1,0:T(8,128)(2,1)S(1)}, bf16[2,128,512]{2,1,0:T(8,128)(2,1)S(1)}, u32[]{:S(2)}, u32[]{:S(2)}) %collective-permute-start.24) | collective-permute-done | bytes 262176 | tf_op jit(solution)/shard_map/ppermute | solution.py:787
  129.3 5.5 %collective-permute-done.25 = bf16[128,512]{1,0:T(8,128)(2,1)S(1)} collective-permute-done((bf16[128,512]{1,0:T(8,128)(2,1)S(1)}, bf16[128,512]{1,0:T(8,128)(2,1)S(1)}, u32[]{:S(2)}, u32[]{:S(2)}) %collective-permute-start.25) | collective-permute-done | bytes 131104 | tf_op jit(solution)/shard_map/ppermute | solution.py:879
  135.0 1.1 collective-permute-done.26
  136.3 0.7 copy-done.26
  137.0 0.8 fusion.1
  (103 shorter events, 5.6 us)
Async XLA Ops:
  0.0 58.7 %copy-start = (bf16[256,1024]{1,0:T(8,128)(2,1)S(1)}, bf16[256,1024]{1,0:T(8,128)(2,1)}, u32[]{:S(2)}) copy-start(bf16[256,1024]{1,0:T(8,128)(2,1)} %param.36) | copy-start | bytes 1572868
  2.4 6.5 %copy-start.1 = (bf16[2,64,2048]{2,1,0:T(8,128)(2,1)S(1)}, bf16[2,64,2048]{2,1,0:T(8,128)(2,1)}, u32[]{:S(2)}) copy-start(bf16[2,64,2048]{2,1,0:T(8,128)(2,1)} %param.21) | copy-start | bytes 1572868
  2.4 6.5 %copy-start.13 = (f32[2048]{0:T(1024)S(1)}, f32[2048]{0:T(1024)}, u32[]{:S(2)}) copy-start(f32[2048]{0:T(1024)} %param.22) | copy-start | bytes 24580
  2.4 43.4 %all-to-all-start = ((bf16[4,128,512]{2,1,0:T(8,128)(2,1)}), bf16[4,128,512]{2,1,0:T(8,128)(2,1)S(1)}, u32[]{:S(2)}, u32[]{:S(2)}) async-start(bf16[4,128,512]{2,1,0:T(8,128)(2,1)} %shard_map.199), calls=%async_computation | async-start | bytes 1048576 | tf_op jit(solution)/shard_map/all_to_all | solution.py:784
  8.9 5.4 %copy-start.23 = (bf16[2048,32]{0,1:T(8,128)(2,1)S(1)}, bf16[2048,32]{0,1:T(8,128)(2,1)}, u32[]{:S(2)}) copy-start(bf16[2048,32]{0,1:T(8,128)(2,1)} %param.32) | copy-start | bytes 393220
  9.2 5.3 %copy-start.24 = (bf16[2048,8]{0,1:T(8,128)(2,1)S(1)}, bf16[2048,8]{0,1:T(8,128)(2,1)}, u32[]{:S(2)}) copy-start(bf16[2048,8]{0,1:T(8,128)(2,1)} %param.26) | copy-start | bytes 98308
  9.2 16.0 %collective-permute-start = (bf16[128,1024]{1,0:T(8,128)(2,1)S(1)}, bf16[128,1024]{1,0:T(8,128)(2,1)S(1)}, u32[]{:S(2)}, u32[]{:S(2)}) collective-permute-start(bf16[128,1024]{1,0:T(8,128)(2,1)S(1)} %get-tuple-element.31.refs_0_), channel_id=1, source_target_pairs={{0,12},{4,0},{8,4},{12,8},{1,13},{5,1},{9,5},{13,9},{2,14},{6,2},{... | collective-permute-start | bytes 786440 | tf_op jit(solution)/shard_map/ppermute | solution.py:790
  13.1 32.7 %collective-permute-start.1 = (bf16[128,1024]{1,0:T(8,128)(2,1)S(1)}, bf16[128,1024]{1,0:T(8,128)(2,1)S(1)}, u32[]{:S(2)}, u32[]{:S(2)}) collective-permute-start(bf16[128,1024]{1,0:T(8,128)(2,1)S(1)} %get-tuple-element.31.refs_0_), channel_id=1, source_target_pairs={{0,8},{4,12},{8,0},{12,4},{1,9},{5,13},{9,1},{13,5},{2,10},{6,14},... | collective-permute-start | bytes 786440 | tf_op jit(solution)/shard_map/ppermute | solution.py:790
  13.1 40.2 %collective-permute-start.2 = (bf16[128,1024]{1,0:T(8,128)(2,1)S(1)}, bf16[128,1024]{1,0:T(8,128)(2,1)S(1)}, u32[]{:S(2)}, u32[]{:S(2)}) collective-permute-start(bf16[128,1024]{1,0:T(8,128)(2,1)S(1)} %get-tuple-element.31.refs_0_), channel_id=1, source_target_pairs={{0,4},{4,8},{8,12},{12,0},{1,5},{5,9},{9,13},{13,1},{2,6},{6,10},{... | collective-permute-start | bytes 786440 | tf_op jit(solution)/shard_map/ppermute | solution.py:790
  22.4 27.3 %copy-start.18 = (bf16[512,2,96]{0,2,1:T(8,128)(2,1)}, bf16[512,2,96]{0,2,1:T(8,128)(2,1)S(1)}, u32[]{:S(2)}) copy-start(bf16[512,2,96]{0,2,1:T(8,128)(2,1)S(1)} %dynamic-slice_bitcast_fusion) | copy-start | bytes 589828
  25.3 28.2 %collective-permute-start.3 = (bf16[128,1024]{1,0:T(8,128)(2,1)S(1)}, bf16[128,1024]{1,0:T(8,128)(2,1)S(1)}, u32[]{:S(2)}, u32[]{:S(2)}) collective-permute-start(bf16[128,1024]{1,0:T(8,128)(2,1)S(1)} %collective-permute-done.refs_1_), channel_id=1, source_target_pairs={{0,1},{1,0},{2,3},{3,2},{4,5},{5,4},{6,7},{7,6},{8,9},{9,8},{10,11... | collective-permute-start | bytes 786440 | tf_op jit(solution)/shard_map/ppermute | solution.py:787
  45.8 8.2 %collective-permute-start.4 = (bf16[128,1024]{1,0:T(8,128)(2,1)S(1)}, bf16[128,1024]{1,0:T(8,128)(2,1)S(1)}, u32[]{:S(2)}, u32[]{:S(2)}) collective-permute-start(bf16[128,1024]{1,0:T(8,128)(2,1)S(1)} %collective-permute-done.1.refs_2_), channel_id=1, source_target_pairs={{0,1},{1,0},{2,3},{3,2},{4,5},{5,4},{6,7},{7,6},{8,9},{9,8},{10,11... | collective-permute-start | bytes 786440 | tf_op jit(solution)/shard_map/ppermute | solution.py:787
  46.7 9.0 %collective-permute-start.8 = (bf16[256,512]{1,0:T(8,128)(2,1)}, bf16[256,512]{1,0:T(8,128)(2,1)}, u32[]{:S(2)}, u32[]{:S(2)}) collective-permute-start(bf16[256,512]{1,0:T(8,128)(2,1)} %bitcast.11), channel_id=1, source_target_pairs={{0,16},{16,0},{1,17},{17,1},{2,18},{18,2},{3,19},{19,3},{4,20},{20... | collective-permute-start | bytes 786440 | tf_op jit(solution)/shard_map/ppermute | solution.py:787
  48.2 9.0 %collective-permute-start.7 = (bf16[256,512]{1,0:T(8,128)(2,1)}, bf16[256,512]{1,0:T(8,128)(2,1)}, u32[]{:S(2)}, u32[]{:S(2)}) collective-permute-start(bf16[256,512]{1,0:T(8,128)(2,1)} %bitcast.12), channel_id=1, source_target_pairs={{0,2},{2,0},{1,3},{3,1},{4,6},{6,4},{5,7},{7,5},{8,10},{10,8},{9,1... | collective-permute-start | bytes 786440 | tf_op jit(solution)/shard_map/ppermute | solution.py:787
  53.3 6.5 %copy-start.4 = (bf16[128,1024]{1,0:T(8,128)(2,1)}, bf16[128,1024]{1,0:T(8,128)(2,1)S(1)}, u32[]{:S(2)}) copy-start(bf16[128,1024]{1,0:T(8,128)(2,1)S(1)} %collective-permute-done.2.refs_3_) | copy-start | bytes 786436
  53.4 8.5 %collective-permute-start.5 = (bf16[128,1024]{1,0:T(8,128)(2,1)S(1)}, bf16[128,1024]{1,0:T(8,128)(2,1)}, u32[]{:S(2)}, u32[]{:S(2)}) collective-permute-start(bf16[128,1024]{1,0:T(8,128)(2,1)S(1)} %collective-permute-done.2.refs_3_), channel_id=1, source_target_pairs={{0,1},{1,0},{2,3},{3,2},{4,5},{5,4},{6,7},{7,6},{8,9},{9,8},{10,11... | collective-permute-start | bytes 786440 | tf_op jit(solution)/shard_map/ppermute | solution.py:787
  53.4 6.4 %copy-start.6 = (bf16[128,1024]{1,0:T(8,128)(2,1)}, bf16[128,1024]{1,0:T(8,128)(2,1)S(1)}, u32[]{:S(2)}) copy-start(bf16[128,1024]{1,0:T(8,128)(2,1)S(1)} %collective-permute-done.3.refs_5_) | copy-start | bytes 786436
  53.5 9.6 %collective-permute-start.6 = (bf16[256,512]{1,0:T(8,128)(2,1)}, bf16[256,512]{1,0:T(8,128)(2,1)}, u32[]{:S(2)}, u32[]{:S(2)}) collective-permute-start(bf16[256,512]{1,0:T(8,128)(2,1)} %bitcast.11), channel_id=1, source_target_pairs={{0,2},{2,0},{1,3},{3,1},{4,6},{6,4},{5,7},{7,5},{8,10},{10,8},{9,1... | collective-permute-start | bytes 786440 | tf_op jit(solution)/shard_map/ppermute | solution.py:787
  54.8 9.5 %collective-permute-start.9 = (bf16[256,512]{1,0:T(8,128)(2,1)}, bf16[256,512]{1,0:T(8,128)(2,1)}, u32[]{:S(2)}, u32[]{:S(2)}) collective-permute-start(bf16[256,512]{1,0:T(8,128)(2,1)} %bitcast.12), channel_id=1, source_target_pairs={{0,16},{16,0},{1,17},{17,1},{2,18},{18,2},{3,19},{19,3},{4,20},{20... | collective-permute-start | bytes 786440 | tf_op jit(solution)/shard_map/ppermute | solution.py:787
  55.7 12.5 %collective-permute-start.10 = (bf16[256,512]{1,0:T(8,128)(2,1)}, bf16[256,512]{1,0:T(8,128)(2,1)}, u32[]{:S(2)}, u32[]{:S(2)}) collective-permute-start(bf16[256,512]{1,0:T(8,128)(2,1)} %collective-permute-done.8.refs_11_), channel_id=1, source_target_pairs={{0,2},{2,0},{1,3},{3,1},{4,6},{6,4},{5,7},{7,5},{8,10},{10,8},{9,1... | collective-permute-start | bytes 786440 | tf_op jit(solution)/shard_map/ppermute | solution.py:787
  57.2 11.8 %collective-permute-start.11 = (bf16[256,512]{1,0:T(8,128)(2,1)}, bf16[256,512]{1,0:T(8,128)(2,1)}, u32[]{:S(2)}, u32[]{:S(2)}) collective-permute-start(bf16[256,512]{1,0:T(8,128)(2,1)} %collective-permute-done.7.refs_10_), channel_id=1, source_target_pairs={{0,16},{16,0},{1,17},{17,1},{2,18},{18,2},{3,19},{19,3},{4,20},{20... | collective-permute-start | bytes 786440 | tf_op jit(solution)/shard_map/ppermute | solution.py:787
  59.9 9.2 %copy-start.3 = (bf16[128,1024]{1,0:T(8,128)(2,1)S(1)}, bf16[128,1024]{1,0:T(8,128)(2,1)}, u32[]{:S(2)}) copy-start(bf16[128,1024]{1,0:T(8,128)(2,1)} %copy-done.2) | copy-start | bytes 786436
  59.9 9.2 %copy-start.5 = (bf16[128,1024]{1,0:T(8,128)(2,1)S(1)}, bf16[128,1024]{1,0:T(8,128)(2,1)}, u32[]{:S(2)}) copy-start(bf16[128,1024]{1,0:T(8,128)(2,1)} %copy-done.4) | copy-start | bytes 786436
  59.9 9.2 %copy-start.7 = (bf16[128,1024]{1,0:T(8,128)(2,1)S(1)}, bf16[128,1024]{1,0:T(8,128)(2,1)}, u32[]{:S(2)}) copy-start(bf16[128,1024]{1,0:T(8,128)(2,1)} %copy-done.6) | copy-start | bytes 786436
  59.9 9.2 %copy-start.9 = (bf16[128,1024]{1,0:T(8,128)(2,1)S(1)}, bf16[128,1024]{1,0:T(8,128)(2,1)}, u32[]{:S(2)}) copy-start(bf16[128,1024]{1,0:T(8,128)(2,1)} %copy-done.8) | copy-start | bytes 786436
  73.1 3.6 %copy-start.21 = (bf16[256,256]{1,0:T(8,128)(2,1)S(1)}, bf16[256,256]{1,0:T(8,128)(2,1)}, u32[]{:S(2)}) copy-start(bf16[256,256]{1,0:T(8,128)(2,1)} %get-tuple-element.67) | copy-start | bytes 393220
  73.1 3.6 %copy-start.22 = (bf16[256,256]{1,0:T(8,128)(2,1)S(1)}, bf16[256,256]{1,0:T(8,128)(2,1)}, u32[]{:S(2)}) copy-start(bf16[256,256]{1,0:T(8,128)(2,1)} %get-tuple-element.68) | copy-start | bytes 393220
  73.1 31.7 %all-to-all-start.1 = ((bf16[4,384,128]{2,1,0:T(8,128)(2,1)}), bf16[4,384,128]{2,1,0:T(8,128)(2,1)S(1)}, u32[]{:S(2)}, u32[]{:S(2)}) async-start(bf16[4,384,128]{2,1,0:T(8,128)(2,1)} %get-tuple-element.35), calls=%async_computation.1 | async-start | bytes 786432 | tf_op jit(solution)/shard_map/all_to_all | solution.py:784
  76.8 22.5 %collective-permute-start.20 = (bf16[512,256]{1,0:T(8,128)(2,1)S(1)}, bf16[512,256]{1,0:T(8,128)(2,1)S(1)}, u32[]{:S(2)}, u32[]{:S(2)}) collective-permute-start(bf16[512,256]{1,0:T(8,128)(2,1)S(1)} %constant_dynamic-slice_fusion), channel_id=1, source_target_pairs={{0,8},{4,12},{8,0},{12,4},{1,9},{5,13},{9,1},{13,5},{2,10},{6,14},... | collective-permute-start | bytes 786440 | tf_op jit(solution)/shard_map/ppermute | solution.py:790
  79.7 34.4 %collective-permute-start.19 = (bf16[1024,256]{1,0:T(8,128)(2,1)S(1)}, bf16[1024,256]{1,0:T(8,128)(2,1)S(1)}, u32[]{:S(2)}, u32[]{:S(2)}) collective-permute-start(bf16[1024,256]{1,0:T(8,128)(2,1)S(1)} %pad_maximum_fusion.refs_8_), channel_id=1, source_target_pairs={{0,2},{2,0},{1,3},{3,1},{4,6},{6,4},{5,7},{7,5},{8,10},{10,8},{9,1... | collective-permute-start | bytes 1572872 | tf_op jit(solution)/shard_map/ppermute | solution.py:787
  99.3 7.4 %collective-permute-start.21 = (bf16[512,256]{1,0:T(8,128)(2,1)S(1)}, bf16[512,256]{1,0:T(8,128)(2,1)}, u32[]{:S(2)}, u32[]{:S(2)}) collective-permute-start(bf16[512,256]{1,0:T(8,128)(2,1)S(1)} %collective-permute-done.20.refs_10_), channel_id=1, source_target_pairs={{0,16},{16,0},{1,17},{17,1},{2,18},{18,2},{3,19},{19,3},{4,20},{20... | collective-permute-start | bytes 786440 | tf_op jit(solution)/shard_map/ppermute | solution.py:787
  100.5 9.1 %copy-start.10 = (f32[256,64]{1,0:T(8,128)S(1)}, f32[256,64]{1,0:T(8,128)}, u32[]{:S(2)}) copy-start(f32[256,64]{1,0:T(8,128)} %constant.51.clone.cos_ref) | copy-start | bytes 196612
  100.5 9.2 %copy-start.11 = (f32[256,64]{1,0:T(8,128)S(1)}, f32[256,64]{1,0:T(8,128)}, u32[]{:S(2)}) copy-start(f32[256,64]{1,0:T(8,128)} %constant.52.clone.sin_ref) | copy-start | bytes 196612
  104.8 4.8 %copy-start.14 = (f32[512]{0:T(512)S(1)}, f32[512]{0:T(512)}, u32[]{:S(2)}) copy-start(f32[512]{0:T(512)} %param.33) | copy-start | bytes 6148
  104.8 4.8 %collective-permute-start.15 = (bf16[4,384,128]{2,1,0:T(8,128)(2,1)S(1)}, bf16[4,384,128]{2,1,0:T(8,128)(2,1)S(1)}, u32[]{:S(2)}, u32[]{:S(2)}) collective-permute-start(bf16[4,384,128]{2,1,0:T(8,128)(2,1)S(1)} %all-to-all-done.1.mine_ref), channel_id=1, source_target_pairs={{0,1},{1,0},{2,3},{3,2},{4,5},{5,4},{6,7},{7,6},{8,9},{9,8},{10,11... | collective-permute-start | bytes 1179656 | tf_op jit(solution)/shard_map/ppermute | solution.py:787
  104.8 9.2 %collective-permute-start.22 = (bf16[512,256]{1,0:T(8,128)(2,1)S(1)}, bf16[512,256]{1,0:T(8,128)(2,1)S(1)}, u32[]{:S(2)}, u32[]{:S(2)}) collective-permute-start(bf16[512,256]{1,0:T(8,128)(2,1)S(1)} %collective-permute-done.20.refs_10_), channel_id=1, source_target_pairs={{0,2},{2,0},{1,3},{3,1},{4,6},{6,4},{5,7},{7,5},{8,10},{10,8},{9,1... | collective-permute-start | bytes 786440 | tf_op jit(solution)/shard_map/ppermute | solution.py:787
  106.7 12.5 %collective-permute-start.23 = (bf16[512,256]{1,0:T(8,128)(2,1)}, bf16[512,256]{1,0:T(8,128)(2,1)S(1)}, u32[]{:S(2)}, u32[]{:S(2)}) collective-permute-start(bf16[512,256]{1,0:T(8,128)(2,1)} %collective-permute-done.21.refs_11_), channel_id=1, source_target_pairs={{0,2},{2,0},{1,3},{3,1},{4,6},{6,4},{5,7},{7,5},{8,10},{10,8},{9,1... | collective-permute-start | bytes 786440 | tf_op jit(solution)/shard_map/ppermute | solution.py:787
  108.2 11.0 %collective-permute-start.12 = (bf16[256,128]{1,0:T(8,128)(2,1)}, bf16[256,128]{1,0:T(8,128)(2,1)S(1)}, u32[]{:S(2)}, u32[]{:S(2)}) collective-permute-start(bf16[256,128]{1,0:T(8,128)(2,1)} %get-tuple-element.43), channel_id=1, source_target_pairs={{0,12},{4,0},{8,4},{12,8},{1,13},{5,1},{9,5},{13,9},{2,14},{6,2},{... | collective-permute-start | bytes 196616 | tf_op jit(solution)/shard_map/ppermute | solution.py:790
  109.6 11.6 %collective-permute-start.13 = (bf16[256,128]{1,0:T(8,128)(2,1)}, bf16[256,128]{1,0:T(8,128)(2,1)S(1)}, u32[]{:S(2)}, u32[]{:S(2)}) collective-permute-start(bf16[256,128]{1,0:T(8,128)(2,1)} %get-tuple-element.44), channel_id=1, source_target_pairs={{0,8},{4,12},{8,0},{12,4},{1,9},{5,13},{9,1},{13,5},{2,10},{6,14},... | collective-permute-start | bytes 196616 | tf_op jit(solution)/shard_map/ppermute | solution.py:790
  110.3 3.8 %copy-start.27 = (bf16[256,128]{1,0:T(8,128)(2,1)S(1)}, bf16[256,128]{1,0:T(8,128)(2,1)}, u32[]{:S(2)}) copy-start(bf16[256,128]{1,0:T(8,128)(2,1)} %get-tuple-element.45) | copy-start | bytes 196612
  110.3 15.4 %copy-start.12 = (bf16[256,128]{1,0:T(8,128)(2,1)S(1)}, bf16[256,128]{1,0:T(8,128)(2,1)}, u32[]{:S(2)}) copy-start(bf16[256,128]{1,0:T(8,128)(2,1)} %get-tuple-element.42.refs_0_) | copy-start | bytes 196612
  114.1 7.1 %collective-permute-start.14 = (bf16[256,128]{1,0:T(8,128)(2,1)S(1)}, bf16[256,128]{1,0:T(8,128)(2,1)S(1)}, u32[]{:S(2)}, u32[]{:S(2)}) collective-permute-start(bf16[256,128]{1,0:T(8,128)(2,1)S(1)} %copy-done.27), channel_id=1, source_target_pairs={{0,4},{4,8},{8,12},{12,0},{1,5},{5,9},{9,13},{13,1},{2,6},{6,10},{... | collective-permute-start | bytes 196616 | tf_op jit(solution)/shard_map/ppermute | solution.py:790
  114.1 7.1 %collective-permute-start.16 = (bf16[256,128]{1,0:T(8,128)(2,1)S(1)}, bf16[256,128]{1,0:T(8,128)(2,1)S(1)}, u32[]{:S(2)}, u32[]{:S(2)}) collective-permute-start(bf16[256,128]{1,0:T(8,128)(2,1)S(1)} %get-tuple-element.50), channel_id=1, source_target_pairs={{0,12},{4,0},{8,4},{12,8},{1,13},{5,1},{9,5},{13,9},{2,14},{6,2},{... | collective-permute-start | bytes 196616 | tf_op jit(solution)/shard_map/ppermute | solution.py:790
  119.2 6.5 %collective-permute-start.17 = (bf16[256,128]{1,0:T(8,128)(2,1)S(1)}, bf16[256,128]{1,0:T(8,128)(2,1)S(1)}, u32[]{:S(2)}, u32[]{:S(2)}) collective-permute-start(bf16[256,128]{1,0:T(8,128)(2,1)S(1)} %get-tuple-element.51), channel_id=1, source_target_pairs={{0,8},{4,12},{8,0},{12,4},{1,9},{5,13},{9,1},{13,5},{2,10},{6,14},... | collective-permute-start | bytes 196616 | tf_op jit(solution)/shard_map/ppermute | solution.py:790
  119.2 6.5 %collective-permute-start.18 = (bf16[256,128]{1,0:T(8,128)(2,1)S(1)}, bf16[256,128]{1,0:T(8,128)(2,1)S(1)}, u32[]{:S(2)}, u32[]{:S(2)}) collective-permute-start(bf16[256,128]{1,0:T(8,128)(2,1)S(1)} %get-tuple-element.52), channel_id=1, source_target_pairs={{0,4},{4,8},{8,12},{12,0},{1,5},{5,9},{9,13},{13,1},{2,6},{6,10},{... | collective-permute-start | bytes 196616 | tf_op jit(solution)/shard_map/ppermute | solution.py:790
  127.5 1.6 %collective-permute-start.24 = (bf16[2,128,512]{2,1,0:T(8,128)(2,1)S(1)}, bf16[2,128,512]{2,1,0:T(8,128)(2,1)S(1)}, u32[]{:S(2)}, u32[]{:S(2)}) collective-permute-start(bf16[2,128,512]{2,1,0:T(8,128)(2,1)S(1)} %get-tuple-element.54), channel_id=1, source_target_pairs={{0,1},{1,0},{2,3},{3,2},{4,5},{5,4},{6,7},{7,6},{8,9},{9,8},{10,11... | collective-permute-start | bytes 786440 | tf_op jit(solution)/shard_map/ppermute | solution.py:787
  129.2 5.6 %collective-permute-start.25 = (bf16[128,512]{1,0:T(8,128)(2,1)S(1)}, bf16[128,512]{1,0:T(8,128)(2,1)S(1)}, u32[]{:S(2)}, u32[]{:S(2)}) collective-permute-start(bf16[128,512]{1,0:T(8,128)(2,1)S(1)} %dynamic-slice_bitcast_fusion.1), channel_id=1, source_target_pairs={{0,4},{4,0},{8,12},{12,8},{1,5},{5,1},{9,13},{13,9},{2,6},{6,2},{1... | collective-permute-start | bytes 393224 | tf_op jit(solution)/shard_map/ppermute | solution.py:879
  135.0 1.2 collective-permute-start.26
  (11 other events, 11.6 us)
